TPU v7x, 256 devices: a whole 4x4x8 slice. The times are simulated.
256 devices in a mesh: sp: 16 (over y, x), tp: 16 (over z, core).
Axes of the slice: x: 4, y: 4, z: 8, core: 2. Of those that a mesh axis runs over, the one named last changes fastest.
Arguments:
- conv_in: bfloat16 [1024, 65536], P('tp', 'sp'), may hold values from -6 to 6
- in_gate: bfloat16 [1024, 65536], P('tp', 'sp'), may hold values from -6 to 6
- out_gate: bfloat16 [1024, 65536], P('tp', 'sp'), may hold values from -6 to 6
- doc_ids: int32 [65536], P('sp'), may hold values from 0 to 7, never falling along the last dimension, each value on 1 to 12288 neighbouring positions
- conv_taps: float32 [1024, 3], P('tp'), may hold values from -3.5 to 3.5
- head_gain: float32 [1024], P('tp'), may hold values from 0.1 to 1.9
- out_proj: bfloat16 [1024, 2048], P('tp'), may hold values from -0.1875 to 0.1875
- resid: bfloat16 [65536, 2048], P(('sp', 'tp')), may hold values from -6 to 6
- norm_gain: float32 [2048], replicated, may hold values from 0.1 to 1.9
- route_ids: int32 [65536, 2], P(('sp', 'tp')), may hold values from 0 to 15, all different within a row; in each aligned block of 128 rows (0 to 127, 128 to 255, ...) at most 32 rows name the same one
- route_weight: float32 [65536, 2], P(('sp', 'tp')), may hold values from 0.1 to 1
- w_gate: bfloat16 [16, 2048, 512], P('sp'), may hold values from -0.125 to 0.125
- w_up: bfloat16 [16, 2048, 512], P('sp'), may hold values from -0.125 to 0.125
- w_down: bfloat16 [16, 512, 2048], P('sp'), may hold values from -0.25 to 0.25
Outputs:
- layer_out: bfloat16 [65536, 2048], P(('sp', 'tp'))
Inputs may be any that keep to these rules, and one draw needn't show every extreme that they name: `doc_ids`: document numbers never fall along the sequence; every number from 0 to 7 is used; no document is longer than 12288 positions and one is exactly that long. `route_ids`: each position names 2 different experts. In every aligned block of 128 positions no expert is named by more than 32 positions, a bound that some block reaches.
All inputs are finite; a program needn't handle non-finite values.
Results may differ from a plain program's by a relative error of at most 0.0051.
Values may be sent and summed in bfloat16 or wider, within the bound.
No kernel may reach another device: no remote copies, remote signals or barrier semaphores. Data moves between devices by JAX's collectives and lax.ppermute only.
A program may use at most 64 MiB of HBM per device.

v0:
```python
import jax
import jax.numpy as jnp
from jax import lax
from jax.sharding import Mesh
from jax.sharding import PartitionSpec as P

HEAD = 64
TP = ("tp_0", "tp_1")
SP_TP = ("sp", "tp_0", "tp_1")


norm_eps = 1e-06


def shifted(value, axis, steps):
    count = lax.axis_size(axis)
    leading, last = (max(0, -steps), min(count, count - steps))
    return lax.ppermute(value, axis, [(source, source + steps) for source in range(leading, last)])


def cut_along(array, dim, length):
    before, after = (array.shape[:dim], array.shape[dim + 1 :])
    return jnp.moveaxis(array.reshape(*before, length, -1, *after), dim, 0)


def joined_along(pieces, dim):
    dims = list(pieces.shape[1:])
    dims[dim] *= pieces.shape[0]
    return jnp.moveaxis(pieces, 0, dim).reshape(dims)


def exchange_in_order(pieces, axes, sequence):
    dims = [lax.axis_size(a) for a in axes]
    pieces = pieces.reshape(*dims, *pieces.shape[1:])
    for k in sequence:
        pieces = lax.all_to_all(pieces, axes[k], split_axis=k, concat_axis=k, tiled=True)
    return pieces.reshape(-1, *pieces.shape[len(axes) :])


def exchange_by_chip(array, groups, sequence, split_dim, concat_dim):
    length = lax.axis_size(groups[0]) * lax.axis_size(groups[1])
    pieces = cut_along(array, split_dim, length)
    return joined_along(exchange_in_order(pieces, groups, sequence), concat_dim)


def slot_places(ids_block, slot, experts):
    flat = ids_block.reshape(-1)
    marks = (flat[:, None] == jnp.arange(experts, dtype=jnp.int32)[None, :]).astype(jnp.int32)
    before = jnp.sum((jnp.cumsum(marks, axis=0) - 1) * marks, axis=1)
    return (flat * slot + before).reshape(ids_block.shape)


def pack_rows(places, normed_rows, total_slots):
    targets = jnp.arange(total_slots, dtype=jnp.int32)
    table = jnp.any(targets[:, None, None] == places[None, :, :], axis=2).astype(jnp.bfloat16)
    return jnp.dot(table, normed_rows, preferred_element_type=jnp.float32).astype(jnp.bfloat16)


def combine_rows(returned, places, weights):
    totals = jnp.zeros((places.shape[0], returned.shape[1]), jnp.float32)
    for choice_k in range(places.shape[1]):
        totals = totals + weights[:, choice_k : choice_k + 1] * returned[
            places[:, choice_k]
        ].astype(jnp.float32)
    return totals


def body(
    conv_in,
    in_gate,
    out_gate,
    doc_ids,
    conv_taps,
    head_gain,
    out_proj,
    resid,
    norm_gain,
    route_ids,
    route_weight,
    w_gate,
    w_up,
    w_down,
):
    gated_in = in_gate.astype(jnp.float32) * conv_in.astype(jnp.float32)
    doc_value = doc_ids.astype(jnp.float32)
    earlier_in, earlier_doc = shifted((gated_in[:, -2:], doc_value[-2:]), "sp", 1)
    padded_in = jnp.concatenate([earlier_in, gated_in], axis=1)
    padded_doc = jnp.concatenate([earlier_doc, doc_value])
    same_one = (padded_doc[1:-1] == doc_value).astype(jnp.float32)
    same_two = (padded_doc[:-2] == doc_value).astype(jnp.float32)
    conv_out = (
        conv_taps[:, 2:3] * gated_in
        + conv_taps[:, 1:2] * (padded_in[:, 1:-1] * same_one)
        + conv_taps[:, 0:1] * (padded_in[:, :-2] * same_two)
    )
    gated_out = out_gate.astype(jnp.float32) * conv_out
    channels = gated_out.shape[0]
    by_head = gated_out.reshape(channels // HEAD, HEAD, -1)
    by_head = by_head * lax.rsqrt(jnp.mean(by_head * by_head, axis=1, keepdims=True) + norm_eps)
    head_normed = (by_head.reshape(channels, -1) * head_gain[:, None]).astype(jnp.bfloat16)
    by_row = exchange_by_chip(head_normed, ("tp_0", "tp_1"), (0, 1), 1, 0)
    rows = resid.shape[0]
    width = resid.shape[1]
    mixed = lax.dot_general(
        by_row,
        lax.all_gather(out_proj, TP, axis=0, tiled=True),
        (((0,), (0,)), ((), ())),
        preferred_element_type=jnp.float32,
    )
    stream = resid.astype(jnp.float32) + mixed
    expert_in = (
        stream * lax.rsqrt(jnp.mean(stream * stream, axis=1, keepdims=True) + norm_eps) * norm_gain
    ).astype(jnp.bfloat16)
    sp_count = lax.axis_size("sp")
    local_experts = w_gate.shape[0]
    experts_total = local_experts * sp_count
    half = rows // 2
    slot = max(2, rows // 8)
    parts = []
    for block_no in range(2):
        block_ids = route_ids[block_no * half : (block_no + 1) * half]
        place = slot_places(block_ids, slot, experts_total)
        send = pack_rows(
            place, expert_in[block_no * half : (block_no + 1) * half], experts_total * slot
        ).reshape(sp_count, local_experts, slot, width)
        arrived = lax.all_to_all(send, "sp", split_axis=0, concat_axis=0, tiled=True)
        gate_part = jnp.einsum(
            "nesd,edf->nesf", arrived, w_gate, preferred_element_type=jnp.float32
        )
        up_part = jnp.einsum("nesd,edf->nesf", arrived, w_up, preferred_element_type=jnp.float32)
        hidden = (jax.nn.silu(gate_part) * up_part).astype(jnp.bfloat16)
        arrived = jnp.einsum(
            "nesf,efd->nesd", hidden, w_down, preferred_element_type=jnp.float32
        ).astype(jnp.bfloat16)
        returned = lax.all_to_all(arrived, "sp", split_axis=0, concat_axis=0, tiled=True).reshape(
            experts_total * slot, width
        )
        parts.append(
            combine_rows(returned, place, route_weight[block_no * half : (block_no + 1) * half])
        )
    mixture = jnp.concatenate(parts, axis=0)
    return (stream + mixture).astype(jnp.bfloat16)


def solution(mesh):
    finer = Mesh(mesh.devices.reshape(mesh.shape["sp"], 8, 2), ("sp", "tp_0", "tp_1"))
    return jax.shard_map(
        body,
        mesh=finer,
        in_specs=(
            P(TP, "sp"),
            P(TP, "sp"),
            P(TP, "sp"),
            P("sp"),
            P(TP, None),
            P(TP),
            P(TP, None),
            P(SP_TP, None),
            P(),
            P(SP_TP, None),
            P(SP_TP, None),
            P("sp", None, None),
            P("sp", None, None),
            P("sp", None, None),
        ),
        out_specs=P(SP_TP, None),
        check_vma=False,
    )
```

profile of v0, /device:TPU:32, one launch (start us, length us, event | category | flops | bytes accessed | tf_op | source)
XLA Modules:
  0.0 229.9 jit_solution(15386730923567032720)
XLA Ops:
  8.1 3.4 %collective-permute-start.1 = (f32[2]{0:T(128)S(1)}, f32[2]{0:T(128)S(1)}, u32[]{:S(2)}, u32[]{:S(2)}) collective-permute-start(f32[2]{0:T(128)S(1)} %slice.117), channel_id=1, source_target_pairs={{0,16},{16,32},{32,48},{48,64},{64,80},{80,96},{96,112},{112,128},... | collective-permute-start | bytes 32 | tf_op jit(solution)/shard_map/ppermute | solution.py:18
  12.9 3.4 %collective-permute-start = (f32[64,2]{1,0:T(8,128)S(1)}, f32[64,2]{1,0:T(8,128)S(1)}, u32[]{:S(2)}, u32[]{:S(2)}) collective-permute-start(f32[64,2]{1,0:T(8,128)S(1)} %slice.114), channel_id=1, source_target_pairs={{0,16},{16,32},{32,48},{48,64},{64,80},{80,96},{96,112},{112,128},... | collective-permute-start | bytes 1544 | tf_op jit(solution)/shard_map/ppermute | solution.py:18
  20.3 8.6 %all-to-all-start = ((bf16[8,2,64,256]{3,2,1,0:T(8,128)(2,1)}), bf16[8,2,64,256]{3,2,1,0:T(8,128)(2,1)S(1)}, u32[]{:S(2)}, u32[]{:S(2)}) async-start(bf16[8,2,64,256]{3,2,1,0:T(8,128)(2,1)} %bitcast.4), calls=%async_computation | async-start | bytes 1048576 | tf_op jit(solution)/shard_map/all_to_all | solution.py:36
  30.5 20.4 %all-to-all-done = bf16[8,2,64,256]{3,2,1,0:T(8,128)(2,1)S(1)} async-done(((bf16[8,2,64,256]{3,2,1,0:T(8,128)(2,1)}), bf16[8,2,64,256]{3,2,1,0:T(8,128)(2,1)S(1)}, u32[]{:S(2)}, u32[]{:S(2)}) %all-to-all-start) | async-done | bytes 524320 | tf_op jit(solution)/shard_map/all_to_all | solution.py:36
  51.0 4.2 %all_to_all.30 = bf16[8,2,64,256]{3,2,0,1:T(8,128)(2,1)S(1)} all-to-all(bf16[8,2,64,256]{3,2,0,1:T(8,128)(2,1)S(1)} %copy.58), channel_id=1, replica_groups=mesh['sp'=16,'tp_0'=8,'tp_1'=2] {'tp_1'}, dimensions={1} | all-to-all | bytes 1048576 | tf_op jit(solution)/shard_map/all_to_all | solution.py:36
  55.3 7.1 %all-gather.2.cloned.1.call-done = bf16[1024,2048]{1,0:T(8,128)(2,1)} async-done(((bf16[64,2048]{1,0:T(8,128)(2,1)}), bf16[1024,2048]{1,0:T(8,128)(2,1)}) %all-gather.2.cloned.1.call-update) | async-done | bytes 4194320 | tf_op jit(solution)/shard_map/all_gather | solution.py:106
  62.4 3.9 %multiply_reduce_fusion = (f32[256]{0:T(256)S(1)}, f32[256,2048]{1,0:T(8,128)S(1)}) fusion(bf16[1024,256]{1,0:T(8,128)(2,1)S(1)} %bitcast.207, bf16[1024,2048]{1,0:T(8,128)(2,1)} %all-gather.2.cloned.1.call-done, bf16[256,2048]{1,0:T(8,128)(2,1)} %param.21), kind=kOutput, calls=%fused_computation.28 | convolution fusion | flops 1075838720 | bytes 7865344 | tf_op jit(solution)/shard_map/dot_general | solution.py:104
  68.6 6.9 %all-to-all-start.2 = ((bf16[16,1,32,2048]{3,2,1,0:T(8,128)(2,1)}), bf16[16,1,32,2048]{3,2,1,0:T(8,128)(2,1)}, u32[]{:S(2)}, u32[]{:S(2)}) async-start(bf16[16,1,32,2048]{3,2,1,0:T(8,128)(2,1)} %bitcast.204), calls=%async_computation.2 | async-start | bytes 4194304 | tf_op jit(solution)/shard_map/all_to_all | solution.py:126
  77.1 2.1 convolution_convert_fusion.1
  79.2 29.7 %all-to-all-done.2 = bf16[16,1,32,2048]{3,2,1,0:T(8,128)(2,1)} async-done(((bf16[16,1,32,2048]{3,2,1,0:T(8,128)(2,1)}), bf16[16,1,32,2048]{3,2,1,0:T(8,128)(2,1)}, u32[]{:S(2)}, u32[]{:S(2)}) %all-to-all-start.2) | async-done | bytes 2097184 | tf_op jit(solution)/shard_map/all_to_all | solution.py:126
  108.9 4.4 %all-to-all-start.4 = ((bf16[16,1,32,2048]{3,2,1,0:T(8,128)(2,1)}), bf16[16,1,32,2048]{3,2,1,0:T(8,128)(2,1)}, u32[]{:S(2)}, u32[]{:S(2)}) async-start(bf16[16,1,32,2048]{3,2,1,0:T(8,128)(2,1)} %bitcast.205), calls=%async_computation.4 | async-start | bytes 4194304 | tf_op jit(solution)/shard_map/all_to_all | solution.py:126
  113.3 3.5 %fusion.17 = f32[16,1,32,512]{3,2,0,1:T(8,128)S(1)} fusion(bf16[1,2048,512]{2,1,0:T(8,128)(2,1)} %param.25, bf16[16,1,32,2048]{3,2,1,0:T(8,128)(2,1)} %all-to-all-done.2), kind=kOutput, calls=%fused_computation.29 | convolution fusion | flops 1073741824 | bytes 5242880 | tf_op jit(solution)/shard_map/nesd,edf->nesf/dot_general | solution.py:127
  116.8 6.0 %fusion = bf16[16,1,32,2048]{3,2,1,0:T(8,128)(2,1)} fusion(bf16[1,512,2048]{2,1,0:T(8,128)(2,1)S(1)} %copy-done, bf16[1,2048,512]{2,1,0:T(8,128)(2,1)} %param.26, bf16[16,1,32,2048]{3,2,1,0:T(8,128)(2,1)} %all-to-all-done.2, f32[16,1,32,512]{3,2,0,1:T(8,128)S(1)} %fusion.17), kind=kOutput, calls=%fused_computation.8 | convolution fusion | flops 2150105088 | bytes 9437184 | tf_op jit(solution)/shard_map/nesf,efd->nesd/dot_general | solution.py:132
  122.8 21.1 %all-to-all-done.4 = bf16[16,1,32,2048]{3,2,1,0:T(8,128)(2,1)} async-done(((bf16[16,1,32,2048]{3,2,1,0:T(8,128)(2,1)}), bf16[16,1,32,2048]{3,2,1,0:T(8,128)(2,1)}, u32[]{:S(2)}, u32[]{:S(2)}) %all-to-all-start.4) | async-done | bytes 2097184 | tf_op jit(solution)/shard_map/all_to_all | solution.py:126
  143.9 4.4 %all-to-all-start.3 = ((bf16[16,1,32,2048]{3,2,1,0:T(8,128)(2,1)}), bf16[16,1,32,2048]{3,2,1,0:T(8,128)(2,1)}, u32[]{:S(2)}, u32[]{:S(2)}) async-start(bf16[16,1,32,2048]{3,2,1,0:T(8,128)(2,1)} %fusion), calls=%async_computation.3 | async-start | bytes 4194304 | tf_op jit(solution)/shard_map/all_to_all | solution.py:135
  148.4 3.5 %fusion.32 = f32[16,1,32,512]{3,2,0,1:T(8,128)S(1)} fusion(bf16[1,2048,512]{2,1,0:T(8,128)(2,1)} %param.25, bf16[16,1,32,2048]{3,2,1,0:T(8,128)(2,1)} %all-to-all-done.4), kind=kOutput, calls=%fused_computation.32 | convolution fusion | flops 1073741824 | bytes 5242880 | tf_op jit(solution)/shard_map/nesd,edf->nesf/dot_general | solution.py:127
  151.9 6.1 %fusion.1 = bf16[16,1,32,2048]{3,2,1,0:T(8,128)(2,1)} fusion(bf16[1,512,2048]{2,1,0:T(8,128)(2,1)S(1)} %copy-done, bf16[1,2048,512]{2,1,0:T(8,128)(2,1)} %param.26, bf16[16,1,32,2048]{3,2,1,0:T(8,128)(2,1)} %all-to-all-done.4, f32[16,1,32,512]{3,2,0,1:T(8,128)S(1)} %fusion.32), kind=kOutput, calls=%fused_computation.9 | convolution fusion | flops 2150105088 | bytes 9437184 | tf_op jit(solution)/shard_map/nesf,efd->nesd/dot_general | solution.py:132
  157.9 20.1 %all-to-all-done.3 = bf16[16,1,32,2048]{3,2,1,0:T(8,128)(2,1)} async-done(((bf16[16,1,32,2048]{3,2,1,0:T(8,128)(2,1)}), bf16[16,1,32,2048]{3,2,1,0:T(8,128)(2,1)}, u32[]{:S(2)}, u32[]{:S(2)}) %all-to-all-start.3) | async-done | bytes 2097184 | tf_op jit(solution)/shard_map/all_to_all | solution.py:135
  178.1 4.6 %all-to-all-start.5 = ((bf16[16,1,32,2048]{3,2,1,0:T(8,128)(2,1)}), bf16[16,1,32,2048]{3,2,1,0:T(8,128)(2,1)}, u32[]{:S(2)}, u32[]{:S(2)}) async-start(bf16[16,1,32,2048]{3,2,1,0:T(8,128)(2,1)} %fusion.1), calls=%async_computation.5 | async-start | bytes 4194304 | tf_op jit(solution)/shard_map/all_to_all | solution.py:135
  183.1 3.3 %gather_fusion = bf16[128,2048]{1,0:T(8,128)(2,1)S(1)} fusion(bf16[512,2048]{1,0:T(8,128)(2,1)} %bitcast.30, s32[1024]{0:T(1024)S(1)} %get-tuple-element.27), kind=kCustom, calls=%fused_computation | custom fusion | bytes 1049088 | tf_op jit(solution)/shard_map/gather | solution.py:62
  186.4 3.3 %gather_fusion.1 = bf16[128,2048]{1,0:T(8,128)(2,1)S(1)} fusion(bf16[512,2048]{1,0:T(8,128)(2,1)} %bitcast.30, s32[1024]{0:T(1024)S(1)} %get-tuple-element.26), kind=kCustom, calls=%fused_computation.1 | custom fusion | bytes 1049088 | tf_op jit(solution)/shard_map/gather | solution.py:62
  189.7 21.9 %all-to-all-done.5 = bf16[16,1,32,2048]{3,2,1,0:T(8,128)(2,1)} async-done(((bf16[16,1,32,2048]{3,2,1,0:T(8,128)(2,1)}), bf16[16,1,32,2048]{3,2,1,0:T(8,128)(2,1)}, u32[]{:S(2)}, u32[]{:S(2)}) %all-to-all-start.5) | async-done | bytes 2097184 | tf_op jit(solution)/shard_map/all_to_all | solution.py:135
  211.7 4.1 %gather_fusion.2 = bf16[128,2048]{1,0:T(8,128)(2,1)} fusion(bf16[512,2048]{1,0:T(8,128)(2,1)} %bitcast.50, s32[1024]{0:T(1024)S(1)} %get-tuple-element.25), kind=kCustom, calls=%fused_computation.2 | custom fusion | bytes 1049088 | tf_op jit(solution)/shard_map/gather | solution.py:62
  215.8 4.1 %gather_fusion.3 = bf16[128,2048]{1,0:T(8,128)(2,1)} fusion(bf16[512,2048]{1,0:T(8,128)(2,1)} %bitcast.50, s32[1024]{0:T(1024)S(1)} %get-tuple-element.24), kind=kCustom, calls=%fused_computation.3 | custom fusion | bytes 1049088 | tf_op jit(solution)/shard_map/gather | solution.py:62
  (78 shorter events, 16.0 us)
Async XLA Ops:
  6.5 110.3 %copy-start = (bf16[1,512,2048]{2,1,0:T(8,128)(2,1)S(1)}, bf16[1,512,2048]{2,1,0:T(8,128)(2,1)}, u32[]{:S(2)}) copy-start(bf16[1,512,2048]{2,1,0:T(8,128)(2,1)} %param.27) | copy-start | bytes 6291460
  6.5 9.8 %copy-start.9 = (f32[64,3]{0,1:T(4,128)S(1)}, f32[64,3]{0,1:T(4,128)}, u32[]{:S(2)}) copy-start(f32[64,3]{0,1:T(4,128)} %param.18) | copy-start | bytes 2308
  6.5 11.3 %copy-start.5 = (bf16[64,4096]{1,0:T(8,128)(2,1)S(1)}, bf16[64,4096]{1,0:T(8,128)(2,1)}, u32[]{:S(2)}) copy-start(bf16[64,4096]{1,0:T(8,128)(2,1)} %param.16) | copy-start | bytes 1572868
  6.5 55.9 %all-gather.2.cloned.1.call-start = ((), (), s32[]{:S(2)}) async-start(), calls=%async_computation.6 | async-start | bytes 4456448 | tf_op jit(solution)/shard_map/all_gather | solution.py:106
  8.1 8.2 %collective-permute-start.1 = (f32[2]{0:T(128)S(1)}, f32[2]{0:T(128)S(1)}, u32[]{:S(2)}, u32[]{:S(2)}) collective-permute-start(f32[2]{0:T(128)S(1)} %slice.117), channel_id=1, source_target_pairs={{0,16},{16,32},{32,48},{48,64},{64,80},{80,96},{96,112},{112,128},... | collective-permute-start | bytes 32 | tf_op jit(solution)/shard_map/ppermute | solution.py:18
  12.9 5.0 %collective-permute-start = (f32[64,2]{1,0:T(8,128)S(1)}, f32[64,2]{1,0:T(8,128)S(1)}, u32[]{:S(2)}, u32[]{:S(2)}) collective-permute-start(f32[64,2]{1,0:T(8,128)S(1)} %slice.114), channel_id=1, source_target_pairs={{0,16},{16,32},{32,48},{48,64},{64,80},{80,96},{96,112},{112,128},... | collective-permute-start | bytes 1544 | tf_op jit(solution)/shard_map/ppermute | solution.py:18
  18.6 0.7 copy-start.10
  19.2 9.7 %copy-start.7 = (s32[256,2]{0,1:T(2,128)S(1)}, s32[256,2]{0,1:T(2,128)}, u32[]{:S(2)}) copy-start(s32[256,2]{0,1:T(2,128)} %param.23) | copy-start | bytes 6148
  20.3 30.6 %all-to-all-start = ((bf16[8,2,64,256]{3,2,1,0:T(8,128)(2,1)}), bf16[8,2,64,256]{3,2,1,0:T(8,128)(2,1)S(1)}, u32[]{:S(2)}, u32[]{:S(2)}) async-start(bf16[8,2,64,256]{3,2,1,0:T(8,128)(2,1)} %bitcast.4), calls=%async_computation | async-start | bytes 1048576 | tf_op jit(solution)/shard_map/all_to_all | solution.py:36
  62.4 3.9 %copy-start.6 = (f32[2048]{0:T(1024)S(1)}, f32[2048]{0:T(1024)}, u32[]{:S(2)}) copy-start(f32[2048]{0:T(1024)} %param.22) | copy-start | bytes 24580
  66.3 2.3 copy-start.1
  68.6 40.3 %all-to-all-start.2 = ((bf16[16,1,32,2048]{3,2,1,0:T(8,128)(2,1)}), bf16[16,1,32,2048]{3,2,1,0:T(8,128)(2,1)}, u32[]{:S(2)}, u32[]{:S(2)}) async-start(bf16[16,1,32,2048]{3,2,1,0:T(8,128)(2,1)} %bitcast.204), calls=%async_computation.2 | async-start | bytes 4194304 | tf_op jit(solution)/shard_map/all_to_all | solution.py:126
  108.9 35.1 %all-to-all-start.4 = ((bf16[16,1,32,2048]{3,2,1,0:T(8,128)(2,1)}), bf16[16,1,32,2048]{3,2,1,0:T(8,128)(2,1)}, u32[]{:S(2)}, u32[]{:S(2)}) async-start(bf16[16,1,32,2048]{3,2,1,0:T(8,128)(2,1)} %bitcast.205), calls=%async_computation.4 | async-start | bytes 4194304 | tf_op jit(solution)/shard_map/all_to_all | solution.py:126
  143.9 34.1 %all-to-all-start.3 = ((bf16[16,1,32,2048]{3,2,1,0:T(8,128)(2,1)}), bf16[16,1,32,2048]{3,2,1,0:T(8,128)(2,1)}, u32[]{:S(2)}, u32[]{:S(2)}) async-start(bf16[16,1,32,2048]{3,2,1,0:T(8,128)(2,1)} %fusion), calls=%async_computation.3 | async-start | bytes 4194304 | tf_op jit(solution)/shard_map/all_to_all | solution.py:135
  157.9 25.2 %copy-start.8 = (f32[256,2]{0,1:T(2,128)S(1)}, f32[256,2]{0,1:T(2,128)}, u32[]{:S(2)}) copy-start(f32[256,2]{0,1:T(2,128)} %param.24) | copy-start | bytes 6148
  178.1 33.6 %all-to-all-start.5 = ((bf16[16,1,32,2048]{3,2,1,0:T(8,128)(2,1)}), bf16[16,1,32,2048]{3,2,1,0:T(8,128)(2,1)}, u32[]{:S(2)}, u32[]{:S(2)}) async-start(bf16[16,1,32,2048]{3,2,1,0:T(8,128)(2,1)} %fusion.1), calls=%async_computation.5 | async-start | bytes 4194304 | tf_op jit(solution)/shard_map/all_to_all | solution.py:135
  219.9 1.0 copy-start.3
  219.9 1.2 copy-start.4
  219.9 1.9 copy-start.2
Sparse Core Ops, SparseCore 0:
  9.2 53.2 all-gather.1
where the time goes:
time: 231 us; the launch traced here: 230 us
  waiting for transfers between devices  123 us (53%)
  starting transfers between devices  35.7 us (15%)
  matrix products  26.9 us (12%)
  local copies, waits for them, and re-layouts  19.6 us (8%)
  between operations  13.7 us (6%)
  other arithmetic  7 us (3%)
  blocking collectives  4.24 us (2%)
    all_to_all x2, waiting for transfers between devices, body(): lax.all_to_all(send, 'sp', split_axis=0, concat_axis=0, tiled=True)  50.8 us
    all_to_all x2, waiting for transfers between devices, body(): lax.all_to_all(arrived, 'sp', split_axis=0, concat_axis=0, tiled=True)  42.1 us
    all_to_all x1, waiting for transfers between devices, exchange_in_order(): lax.all_to_all(pieces, axes[k], split_axis=k, concat_axis=k, tiled=True)  20.4 us
    gather x4, local copies, waits for them, and re-layouts, combine_rows(): returned[places[:, choice_k]].astype(jnp.float32)  14.8 us
    dot_general x2, matrix products, body(): jnp.einsum('nesf,efd->nesd', hidden, w_down, preferred_element_type=jnp.f...  12.1 us
    all_to_all x2, starting transfers between devices, body(): lax.all_to_all(send, 'sp', split_axis=0, concat_axis=0, tiled=True)  11.3 us
    all_to_all x2, starting transfers between devices, body(): lax.all_to_all(arrived, 'sp', split_axis=0, concat_axis=0, tiled=True)  9.05 us
    all_to_all x1, starting transfers between devices, exchange_in_order(): lax.all_to_all(pieces, axes[k], split_axis=k, concat_axis=k, tiled=True)  8.57 us
  transfers between devices with their start and end apart: 8, of which 7 were waited for; matrix products, arithmetic and copies ran while one was open for 16% of the time, Pallas kernels for 0%

commit v1 on v0

v1 whole, which is shorter than its diff:
```python
import functools

import jax
import jax.numpy as jnp
import numpy as np
from jax import lax
from jax.experimental import pallas as pl
from jax.experimental.pallas import tpu as pltpu
from jax.sharding import Mesh
from jax.sharding import PartitionSpec as P


HEAD = 64
EPS = 1e-06
ROWS = 256
HALF = 128
SLOT = 32
CHUNK = 64
WIDTH = 2048
FF = 512
TILE = 512
SP = ("y", "x")
TP = ("z", "c")
CHIP = ("y", "x", "c")

PAIRS = (
    ((1, 2), (3, 2)),
    ((2, 1), (2, 3)),
    ((2, 2), (0, 0)),
    ((0, 2), (2, 0)),
    ((1, 1), (3, 3)),
    ((1, 3), (3, 1)),
    ((1, 0), (3, 0)),
    ((0, 1), (0, 3)),
)
GROUPS = ((0, 1), (2, 3), (4, 5), (6, 7))

VMEM = pl.BlockSpec(memory_space=pltpu.VMEM)
SMEM = pl.BlockSpec(memory_space=pltpu.SMEM)


def permute(value, axes, sizes, move):
    pairs = []
    for i in np.ndindex(*sizes):
        j = tuple(int(v) for v in np.mod(move(*i), sizes))
        pairs.append((int(np.ravel_multi_index(i, sizes)), int(np.ravel_multi_index(j, sizes))))
    return lax.ppermute(value, axes, pairs)


def displaced(value, op, sign, cross=0):
    def move(y, x, c):
        dy, dx = PAIRS[op][c]
        return (y + sign * dy, x + sign * dx, c + cross)

    return permute(value, CHIP, (4, 4, 2), move)


def along_z(value, step):
    return permute(value, "z", (8,), lambda z: (z + step,))


def swap_cores(value):
    return permute(value, "c", (2,), lambda c: (c + 1,))


def after(value, *others):
    return lax.optimization_barrier((value, *others))[0]


def in_hbm(value):
    return pltpu.with_memory_space_constraint(value, pltpu.HBM)


def cost(flops, nbytes):
    return pl.CostEstimate(flops=int(flops), bytes_accessed=int(nbytes), transcendentals=0)


def params(mib, grid=False):
    kwargs = {"dimension_semantics": ("arbitrary",)} if grid else {}
    return pltpu.CompilerParams(vmem_limit_bytes=mib << 20, **kwargs)


def conv_kernel(a_ref, b_ref, o_ref, m1_ref, m2_ref, halo_ref, taps_ref, gain_ref, out_ref, prev):
    @pl.when(pl.program_id(0) == 0)
    def _():
        prev[...] = halo_ref[...]

    lane = lax.broadcasted_iota(jnp.int32, (HEAD, ROWS), 1)
    t0, t1, t2 = taps_ref[:, 0:1], taps_ref[:, 1:2], taps_ref[:, 2:3]
    gain = gain_ref[...]
    g = prev[...]
    p1, p2 = pltpu.roll(g, 1, 1), pltpu.roll(g, 2, 1)
    for t in range(4):
        at = slice(t * ROWS, (t + 1) * ROWS)
        g = a_ref[:, at].astype(jnp.float32) * b_ref[:, at].astype(jnp.float32)
        r1, r2 = pltpu.roll(g, 1, 1), pltpu.roll(g, 2, 1)
        g1 = jnp.where(lane < 1, p1, r1)
        g2 = jnp.where(lane < 2, p2, r2)
        conv = t2 * g + t1 * (g1 * m1_ref[:, at]) + t0 * (g2 * m2_ref[:, at])
        v = o_ref[:, at].astype(jnp.float32) * conv
        ms = jnp.sum(v * v, axis=0, keepdims=True) * (1.0 / HEAD)
        out_ref[t] = (v * lax.rsqrt(ms + EPS) * gain).astype(jnp.bfloat16)
        p1, p2 = r1, r2
    prev[...] = g


def conv(conv_in, in_gate, out_gate, m1, m2, halo, taps, gain):
    wide = pl.BlockSpec((HEAD, 4 * ROWS), lambda i: (0, i))
    thin = pl.BlockSpec((1, 4 * ROWS), lambda i: (0, i))

    def whole(a):
        return pl.BlockSpec(a.shape, lambda i: (0, 0))

    return pl.pallas_call(
        conv_kernel,
        grid=(4,),
        out_shape=jax.ShapeDtypeStruct((16, HEAD, ROWS), jnp.bfloat16),
        in_specs=[wide, wide, wide, thin, thin, whole(halo), whole(taps), whole(gain)],
        out_specs=pl.BlockSpec((4, HEAD, ROWS), lambda i: (i, 0, 0)),
        scratch_shapes=[pltpu.VMEM((HEAD, ROWS), jnp.float32)],
        compiler_params=params(4, True),
        cost_estimate=cost(2e8, 2 << 20),
        name="conv",
    )(in_hbm(conv_in), in_hbm(in_gate), in_hbm(out_gate), m1, m2, halo, taps, gain)


OFFSETS = (0, -1, 1, -2, 2, -3, 3, -4)


def mix_kernel(where_ref, by_row_ref, *refs):
    n_own = len(OFFSETS)
    own = refs[:n_own]
    swapped = refs[n_own : n_own + 2]
    resid_ref, gain_ref, stream_ref, normed_ref, lhs, rhs, kept, total = refs[n_own + 2 :]
    z, c = where_ref[0], where_ref[1]
    step = pl.program_id(0)

    @pl.when(step == 0)
    def _():
        for q, off in enumerate(OFFSETS):
            zz = lax.rem(z + (off + 8), 8)
            lhs[pl.ds(q * 64, 64), :] = by_row_ref[zz * 2 + c]
            lhs[pl.ds(512 + q * 64, 64), :] = by_row_ref[zz * 2 + 1 - c]
        total[...] = jnp.zeros_like(total)

    row = 0
    for ref in (*own, *swapped):
        rhs[pl.ds(row, ref.shape[0]), :] = ref[...]
        row += ref.shape[0]
    mixed = lax.dot_general(
        lhs[...], rhs[...], (((0,), (0,)), ((), ())), preferred_element_type=jnp.float32
    )
    stream = resid_ref[...].astype(jnp.float32) + mixed
    stream_ref[...] = stream
    kept[step] = stream
    total[...] += jnp.broadcast_to(jnp.sum(stream * stream, axis=1, keepdims=True), total.shape)

    @pl.when(step == WIDTH // TILE - 1)
    def _():
        scale = lax.rsqrt(total[:, 0:1] * (1.0 / WIDTH) + EPS)
        for n in range(WIDTH // TILE):
            at = slice(n * TILE, (n + 1) * TILE)
            normed_ref[:, at] = (kept[n] * scale * gain_ref[:, at]).astype(jnp.bfloat16)


def mix(where, by_row, own, swapped, resid, gain):
    def tall(a):
        return pl.BlockSpec((a.shape[0], TILE), lambda i: (0, i))

    return pl.pallas_call(
        mix_kernel,
        grid=(WIDTH // TILE,),
        out_shape=[
            pltpu.HBM((ROWS, WIDTH), jnp.float32),
            jax.ShapeDtypeStruct((ROWS, WIDTH), jnp.bfloat16),
        ],
        in_specs=[SMEM, pl.BlockSpec(by_row.shape, lambda i: (0, 0, 0))]
        + [tall(a) for a in (*own, *swapped, resid)]
        + [pl.BlockSpec(gain.shape, lambda i: (0, 0))],
        out_specs=[
            pl.BlockSpec((ROWS, TILE), lambda i: (0, i)),
            pl.BlockSpec((ROWS, WIDTH), lambda i: (0, 0)),
        ],
        scratch_shapes=[
            pltpu.VMEM((1024, ROWS), jnp.bfloat16),
            pltpu.VMEM((1024, TILE), jnp.bfloat16),
            pltpu.VMEM((WIDTH // TILE, ROWS, TILE), jnp.float32),
            pltpu.VMEM((ROWS, 128), jnp.float32),
        ],
        compiler_params=params(16, True),
        cost_estimate=cost(1.1e9, 8 << 20),
        name="mix",
    )(where, by_row, *own, *swapped, in_hbm(resid), gain)


def pack_kernel(mine_ref, theirs_ref, mine_at_ref, theirs_at_ref, *refs):
    outs, table = refs[: len(PAIRS)], refs[len(PAIRS)]

    @pl.when(pl.program_id(0) == 0)
    def _():
        slot = lax.broadcasted_iota(jnp.int32, (CHUNK, ROWS), 0)
        for half, ref in enumerate((mine_at_ref, theirs_at_ref)):
            for k in range(len(PAIRS)):
                hit = slot == ref[k : k + 1, :]
                table[half, pl.ds(k * CHUNK, CHUNK), :] = jnp.where(hit, 1.0, 0.0).astype(
                    jnp.bfloat16
                )

    for half, ref in enumerate((mine_ref, theirs_ref)):
        packed = jnp.dot(table[half], ref[...], preferred_element_type=jnp.float32)
        packed = packed.astype(jnp.bfloat16)
        for k, out in enumerate(outs):
            out[pl.ds(half * CHUNK, CHUNK), :] = packed[k * CHUNK : (k + 1) * CHUNK]


def pack(mine, theirs, mine_at, theirs_at):
    block = pl.BlockSpec((ROWS, TILE), lambda i: (0, i))
    at = pl.BlockSpec(mine_at.shape, lambda i: (0, 0))
    n = len(PAIRS)
    return pl.pallas_call(
        pack_kernel,
        grid=(WIDTH // TILE,),
        out_shape=[jax.ShapeDtypeStruct((2 * CHUNK, WIDTH), jnp.bfloat16)] * n,
        in_specs=[block, block, at, at],
        out_specs=[pl.BlockSpec((2 * CHUNK, TILE), lambda i: (0, i))] * n,
        scratch_shapes=[pltpu.VMEM((2, n * CHUNK, ROWS), jnp.bfloat16)],
        compiler_params=params(12, True),
        cost_estimate=cost(1.1e9, 6 << 20),
        name="pack",
    )(mine, theirs, mine_at, theirs_at)


def expert_kernel(n, *refs):
    bufs, (wg, wu, wd) = refs[:n], refs[n : n + 3]
    outs, rows = refs[n + 3 : -1], refs[-1]
    row = 0
    for ref in bufs:
        rows[pl.ds(row, ref.shape[0]), :] = ref[...]
        row += ref.shape[0]
    x = rows[...]
    g = jnp.dot(x, wg[...], preferred_element_type=jnp.float32)
    u = jnp.dot(x, wu[...], preferred_element_type=jnp.float32)
    h = (g / (1.0 + jnp.exp(-g)) * u).astype(jnp.bfloat16)
    for n0 in range(0, WIDTH, TILE):
        at = slice(n0, n0 + TILE)
        y = jnp.dot(h, wd[:, at], preferred_element_type=jnp.float32).astype(jnp.bfloat16)
        row = 0
        for ref in outs:
            ref[:, at] = y[row : row + ref.shape[0]]
            row += ref.shape[0]


def experts(bufs, wg, wu, wd, apart):
    rows = sum(b.shape[0] for b in bufs)
    size = CHUNK if apart else 2 * CHUNK
    n_out = rows // size
    return pl.pallas_call(
        functools.partial(expert_kernel, len(bufs)),
        out_shape=[jax.ShapeDtypeStruct((size, WIDTH), jnp.bfloat16)] * n_out,
        in_specs=[VMEM] * (len(bufs) + 3),
        out_specs=[VMEM] * n_out,
        scratch_shapes=[pltpu.VMEM((rows, WIDTH), jnp.bfloat16)],
        compiler_params=params(18),
        cost_estimate=cost(6.0 * rows * WIDTH * FF, 8 << 20),
        name="experts",
    )(*bufs, wg, wu, wd)


def weighted(place, weight, first, count):
    slot = lax.broadcasted_iota(jnp.int32, (ROWS, count), 1) + first
    table = jnp.where(place[:, 0:1] == slot, weight[:, 0:1], 0.0) + jnp.where(
        place[:, 1:2] == slot, weight[:, 1:2], 0.0
    )
    high = table.astype(jnp.bfloat16)
    return high, (table - high.astype(jnp.float32)).astype(jnp.bfloat16)


def apply(tables, rows):
    return sum(jnp.dot(t, rows, preferred_element_type=jnp.float32) for t in tables)


def gather_kernel(n, acc_ref, place_ref, weight_ref, place2_ref, weight2_ref, *refs):
    bufs = refs[:n]
    mine_ref, theirs_ref, mine, theirs = refs[n:]
    for i, ref in enumerate(bufs):
        mine[pl.ds(i * CHUNK, CHUNK), :] = ref[:CHUNK]
        theirs[pl.ds(i * CHUNK, CHUNK), :] = ref[CHUNK:]
    count = n * CHUNK
    own = weighted(place_ref[...], weight_ref[...], 0, count)
    mine_ref[...] = acc_ref[...] + apply(own, mine[...])
    other = weighted(place2_ref[...], weight2_ref[...], 0, count)
    theirs_ref[...] = apply(other, theirs[...])


def gather(acc, place, weight, place2, weight2, bufs):
    n = len(bufs)
    block = pl.BlockSpec((ROWS, TILE), lambda i: (0, i))
    pair = pl.BlockSpec((ROWS, 2), lambda i: (0, 0))
    return pl.pallas_call(
        functools.partial(gather_kernel, n),
        grid=(WIDTH // TILE,),
        out_shape=[
            pltpu.HBM((ROWS, WIDTH), jnp.float32),
            jax.ShapeDtypeStruct((ROWS, WIDTH), jnp.float32),
        ],
        in_specs=[block] + [pair] * 4 + [pl.BlockSpec((2 * CHUNK, TILE), lambda i: (0, i))] * n,
        out_specs=[block, block],
        scratch_shapes=[pltpu.VMEM((n * CHUNK, TILE), jnp.bfloat16)] * 2,
        compiler_params=params(14, True),
        cost_estimate=cost(8.0 * ROWS * n * CHUNK * WIDTH, 10 << 20),
        name="gather",
    )(in_hbm(acc), place, weight, place2, weight2, *bufs)


def finish_kernel(first, n, acc_ref, more_ref, place_ref, weight_ref, *refs):
    bufs, out_ref, rows = refs[:n], refs[n], refs[n + 1]
    for i, ref in enumerate(bufs):
        rows[pl.ds(i * CHUNK, CHUNK), :] = ref[...]
    half = n // 2 * CHUNK
    mine = weighted(place_ref[...], weight_ref[...], first, half)
    theirs = weighted(place_ref[...], weight_ref[...], first + 8 * CHUNK, half)
    total = acc_ref[...] + more_ref[...]
    total = total + apply(mine, rows[:half]) + apply(theirs, rows[half:])
    out_ref[...] = total.astype(out_ref.dtype)


def finish(first, acc, more, place, weight, bufs):
    n = len(bufs)
    block = pl.BlockSpec((ROWS, TILE), lambda i: (0, i))
    pair = pl.BlockSpec((ROWS, 2), lambda i: (0, 0))
    return pl.pallas_call(
        functools.partial(finish_kernel, first, n),
        grid=(WIDTH // TILE,),
        out_shape=jax.ShapeDtypeStruct((ROWS, WIDTH), jnp.bfloat16),
        in_specs=[block, block, pair, pair]
        + [pl.BlockSpec((CHUNK, TILE), lambda i: (0, i))] * n,
        out_specs=block,
        scratch_shapes=[pltpu.VMEM((n * CHUNK, TILE), jnp.bfloat16)],
        compiler_params=params(12, True),
        cost_estimate=cost(4.0 * ROWS * n * CHUNK * WIDTH, 6 << 20),
        name="finish",
    )(in_hbm(acc), more, place, weight, *bufs)


def places(ids, expert_of):
    at0 = ids[0:1] == expert_of[:, None]
    at1 = ids[1:2] == expert_of[:, None]
    named = at0 | at1
    position = np.arange(ROWS)
    earlier = (position[:, None] < position[None, :]) & (
        position[:, None] // HALF == position[None, :] // HALF
    )
    rank = jnp.dot(
        named.astype(jnp.bfloat16),
        jnp.asarray(earlier, jnp.bfloat16),
        preferred_element_type=jnp.float32,
    ).astype(jnp.int32)
    in_chunk = rank + jnp.asarray(position // HALF * SLOT, jnp.int32)[None]
    rows = jnp.where(named, in_chunk, -1)
    count = expert_of.shape[0]
    in_all = in_chunk + 1 + jnp.arange(count, dtype=jnp.int32)[:, None] * CHUNK
    place = jnp.stack(
        [jnp.sum(jnp.where(at, in_all, 0), axis=0) - 1 for at in (at0, at1)], axis=1
    )
    return rows, place


def body(
    conv_in,
    in_gate,
    out_gate,
    doc_ids,
    conv_taps,
    head_gain,
    out_proj,
    resid,
    norm_gain,
    route_ids,
    route_weight,
    w_gate,
    w_up,
    w_down,
):
    y, x, z, c = (lax.axis_index(a) for a in ("y", "x", "z", "c"))

    last = in_gate[:, -2:].astype(jnp.float32) * conv_in[:, -2:].astype(jnp.float32)
    doc_value = doc_ids.astype(jnp.float32)
    tail = jnp.concatenate([last, doc_value[None, -2:]], axis=0)
    halo = lax.ppermute(tail, SP, [(i, i + 1) for i in range(15)])

    plus, minus = [out_proj], [out_proj]
    plus.append(along_z(out_proj, 1))
    minus.append(along_z(out_proj, -1))

    doc_before = jnp.concatenate([halo[HEAD], doc_value])
    same_one = (doc_before[1:-1] == doc_value).astype(jnp.float32)[None]
    same_two = (doc_before[:-2] == doc_value).astype(jnp.float32)[None]
    before = jnp.pad(halo[:HEAD], ((0, 0), (ROWS - 2, 0)))
    head_normed = conv(
        conv_in, in_gate, out_gate, same_one, same_two, before, conv_taps, head_gain[:, None]
    )
    by_row = lax.all_to_all(head_normed, TP, split_axis=0, concat_axis=0, tiled=True)

    plus[1], minus[1] = after(plus[1], head_normed), after(minus[1], head_normed)
    for _ in range(2, 5):
        plus.append(along_z(plus[-1], 1))
    for _ in range(2, 4):
        minus.append(along_z(minus[-1], -1))
    own = [out_proj, plus[1], minus[1], plus[2], minus[2], plus[3], minus[3], plus[4]]
    swapped = [
        swap_cores(jnp.concatenate(own[:5], axis=0)),
        swap_cores(jnp.concatenate(own[5:], axis=0)),
    ]

    routes = jnp.concatenate([route_ids.astype(jnp.float32), route_weight], axis=1).T
    routes = after(routes, head_normed)
    other = swap_cores(routes)
    table = np.array(PAIRS, np.int32)
    first_core = jnp.asarray(table[:, 0])
    second_core = jnp.asarray(table[:, 1])
    mine_d = jnp.where(c == 0, first_core, second_core)
    theirs_d = jnp.where(c == 0, second_core, first_core)

    def numbers(d):
        return ((y + d[:, 0]) % 4) * 4 + (x + d[:, 1]) % 4

    experts_mine = numbers(mine_d)
    rows_mine, place = places(
        route_ids.T, jnp.concatenate([experts_mine, numbers(theirs_d)])
    )
    rows_theirs, place_theirs = places(other[:2].astype(jnp.int32), experts_mine)
    weight_theirs = other[2:].T

    where = jnp.stack([z, c]).astype(jnp.int32)
    stream, normed = mix(where, by_row, own, swapped, resid, norm_gain[None])
    sends = pack(normed, swap_cores(normed), rows_mine[:8], rows_theirs)
    arrived = [displaced(s, k, 1) for k, s in enumerate(sends)]

    wg, wu, wd = w_gate[0], w_up[0], w_down[0]
    back = []
    for n, group in enumerate(GROUPS):
        final = n == len(GROUPS) - 1
        inputs = [arrived[k] for k in group]
        results = experts(inputs, wg, wu, wd, final)
        if final:
            back += [displaced(results[2 * i], k, -1) for i, k in enumerate(group)]
            back += [displaced(results[2 * i + 1], k, -1, 1) for i, k in enumerate(group)]
        else:
            back += [displaced(r, k, -1) for r, k in zip(results, group)]
    total, partial = gather(
        stream, place, route_weight, place_theirs, weight_theirs, back[:6]
    )
    more = swap_cores(partial)
    return finish(6 * CHUNK, total, more, place, route_weight, back[6:])


def solution(mesh):
    finer = Mesh(mesh.devices.reshape(4, 4, 8, 2), ("y", "x", "z", "c"))
    every = SP + TP
    return jax.shard_map(
        body,
        mesh=finer,
        in_specs=(
            P(TP, SP),
            P(TP, SP),
            P(TP, SP),
            P(SP),
            P(TP, None),
            P(TP),
            P(TP, None),
            P(every, None),
            P(),
            P(every, None),
            P(every, None),
            P(SP, None, None),
            P(SP, None, None),
            P(SP, None, None),
        ),
        out_specs=P(every, None),
        check_vma=False,
    )
```

time: 231 us -> 228 us (0.987)
  the two profiles are of different devices: /device:TPU:32 before, /device:TPU:1 now
where the time goes in v1:
time: 228 us; the launch traced here: 227 us
  waiting for transfers between devices  101 us (44%)
  starting transfers between devices  73.7 us (32%)
  Pallas kernels  33.1 us (15%)
  local copies, waits for them, and re-layouts  9.76 us (4%)
  other arithmetic  7.22 us (3%)
    ppermute x30, waiting for transfers between devices, permute(): return lax.ppermute(value, axes, pairs)  89.9 us
    ppermute x30, starting transfers between devices, permute(): return lax.ppermute(value, axes, pairs)  62.8 us
    all_to_all x1, waiting for transfers between devices, body(): lax.all_to_all(head_normed, TP, split_axis=0, concat_axis=0, tiled=True)  11.6 us
    pallas_call x4, Pallas kernels, experts(): pl.pallas_call(functools.partial(expert_kernel, len(bufs)), out_shape=[ja...  10.2 us
    all_to_all x1, starting transfers between devices, body(): lax.all_to_all(head_normed, TP, split_axis=0, concat_axis=0, tiled=True)  7.75 us
    unnamed x56, local copies, waits for them, and re-layouts  7.52 us
    pallas_call x1, Pallas kernels, gather(): pl.pallas_call(functools.partial(gather_kernel, n), grid=(WIDTH // TILE,)...  6.05 us
    pallas_call x1, Pallas kernels, mix(): pl.pallas_call(mix_kernel, grid=(WIDTH // TILE,), out_shape=[pltpu.HBM((R...  5.53 us
  transfers between devices with their start and end apart: 32, of which 15 were waited for; matrix products, arithmetic and copies ran while one was open for 7% of the time, Pallas kernels for 6%

profile of v1, /device:TPU:1, one launch (start us, length us, event | category | flops | bytes accessed | tf_op | source)
XLA Modules:
  0.0 227.2 jit_solution(15800205089923078622)
XLA Ops:
  0.0 6.4 %collective-permute-start.2 = (bf16[64,2048]{1,0:T(8,128)(2,1)}, bf16[64,2048]{1,0:T(8,128)(2,1)S(1)}, u32[]{:S(2)}, u32[]{:S(2)}) collective-permute-start(bf16[64,2048]{1,0:T(8,128)(2,1)} %refs_0_.1), channel_id=1, source_target_pairs={{0,14},{2,0},{4,2},{6,4},{8,6},{10,8},{12,10},{14,12},{1,15},{3,1}... | collective-permute-start | bytes 786440 | tf_op jit(solution)/shard_map/ppermute | solution.py:47
  8.0 3.1 %collective-permute-start = (f32[65,2]{1,0:T(8,128)S(1)}, f32[65,2]{1,0:T(8,128)S(1)}, u32[]{:S(2)}, u32[]{:S(2)}) collective-permute-start(f32[65,2]{1,0:T(8,128)S(1)} %pad_maximum_fusion.1), channel_id=1, source_target_pairs={{0,16},{16,32},{32,48},{48,64},{64,80},{80,96},{96,112},{112,128},... | collective-permute-start | bytes 1568 | tf_op jit(solution)/shard_map/ppermute | solution.py:389
  17.1 4.0 %conv.1 = bf16[16,64,256]{2,1,0:T(8,128)(2,1)} custom-call(bf16[64,4096]{1,0:T(8,128)(2,1)} %a_ref.1, bf16[64,4096]{1,0:T(8,128)(2,1)} %b_ref.1, bf16[64,4096]{1,0:T(8,128)(2,1)} %o_ref.1, f32[1,4096]{1,0:T(1,128)S(1)} %bitcast.48, f32[1,4096]{1,0:T(1,128)S(1)} %bitcast.47, f32[64,256]{1,0:T(8,128)S(1)} %pad.4.halo_ref, f32[64,3]{1,0:T(8,128)S(1)} %copy.49.taps_ref, ...), custom_call_target="tpu_custom_call" | custom-call | flops 200000000 | bytes 2097152 | tf_op jit(solution)/shard_map/conv/pallas_call | solution.py:114
  25.5 3.6 %collective-permute-done.3.refs_3_ = bf16[64,2048]{1,0:T(8,128)(2,1)S(1)} collective-permute-done((bf16[64,2048]{1,0:T(8,128)(2,1)S(1)}, bf16[64,2048]{1,0:T(8,128)(2,1)S(1)}, u32[]{:S(2)}, u32[]{:S(2)}) %collective-permute-start.3) | collective-permute-done | bytes 262176 | tf_op jit(solution)/shard_map/ppermute | solution.py:47
  32.6 3.0 %collective-permute-start.6 = (bf16[64,2048]{1,0:T(8,128)(2,1)S(1)}, bf16[64,2048]{1,0:T(8,128)(2,1)}, u32[]{:S(2)}, u32[]{:S(2)}) collective-permute-start(bf16[64,2048]{1,0:T(8,128)(2,1)S(1)} %collective-permute-done.4.refs_4_), channel_id=1, source_target_pairs={{0,14},{2,0},{4,2},{6,4},{8,6},{10,8},{12,10},{14,12},{1,15},{3,1}... | collective-permute-start | bytes 786440 | tf_op jit(solution)/shard_map/ppermute | solution.py:47
  36.9 7.8 %all-to-all-start = ((bf16[16,64,256]{2,1,0:T(8,128)(2,1)}), bf16[16,64,256]{2,1,0:T(8,128)(2,1)S(1)}, u32[]{:S(2)}, u32[]{:S(2)}) async-start(bf16[16,64,256]{2,1,0:T(8,128)(2,1)} %conv.1), calls=%async_computation | async-start | bytes 1048576 | tf_op jit(solution)/shard_map/all_to_all | solution.py:402
  50.3 11.6 %all-to-all-done.by_row_ref = bf16[16,64,256]{2,1,0:T(8,128)(2,1)S(1)} async-done(((bf16[16,64,256]{2,1,0:T(8,128)(2,1)}), bf16[16,64,256]{2,1,0:T(8,128)(2,1)S(1)}, u32[]{:S(2)}, u32[]{:S(2)}) %all-to-all-start) | async-done | bytes 524320 | tf_op jit(solution)/shard_map/all_to_all | solution.py:402
  62.0 5.5 %mix.1 = (f32[256,2048]{1,0:T(8,128)}, bf16[256,2048]{1,0:T(8,128)(2,1)S(1)}) custom-call(s32[2]{0:T(128)S(1)} %pad_add_fusion.2.where_ref, bf16[16,64,256]{2,1,0:T(8,128)(2,1)S(1)} %all-to-all-done.by_row_ref, bf16[64,2048]{1,0:T(8,128)(2,1)S(1)} %copy-done.5, bf16[64,2048]{1,0:T(8,128)(2,1)S(1)} %collective-permute-done.1.refs_1_, ...), custom_call_target="tpu_custom_call" | custom-call | flops 1100000000 | bytes 8388608 | tf_op jit(solution)/shard_map/mix/pallas_call | solution.py:170
  74.1 4.9 %collective-permute-start.12 = (bf16[128,2048]{1,0:T(8,128)(2,1)S(1)}, bf16[128,2048]{1,0:T(8,128)(2,1)S(1)}, u32[]{:S(2)}, u32[]{:S(2)}) collective-permute-start(bf16[128,2048]{1,0:T(8,128)(2,1)S(1)} %get-tuple-element.35), channel_id=1, source_target_pairs={{0,96},{1,225},{16,112},{17,241},{32,64},{33,193},{48,80},{49,209}... | collective-permute-start | bytes 1572872 | tf_op jit(solution)/shard_map/ppermute | solution.py:47
  83.8 7.0 %collective-permute-done.12.refs_0_ = bf16[128,2048]{1,0:T(8,128)(2,1)S(1)} collective-permute-done((bf16[128,2048]{1,0:T(8,128)(2,1)S(1)}, bf16[128,2048]{1,0:T(8,128)(2,1)S(1)}, u32[]{:S(2)}, u32[]{:S(2)}) %collective-permute-start.12) | collective-permute-done | bytes 524320 | tf_op jit(solution)/shard_map/ppermute | solution.py:47
  90.8 5.6 %collective-permute-start.21 = (bf16[128,2048]{1,0:T(8,128)(2,1)S(1)}, bf16[128,2048]{1,0:T(8,128)(2,1)S(1)}, u32[]{:S(2)}, u32[]{:S(2)}) collective-permute-start(bf16[128,2048]{1,0:T(8,128)(2,1)S(1)} %get-tuple-element.44), channel_id=1, source_target_pairs={{0,112},{1,209},{16,64},{17,225},{32,80},{33,241},{48,96},{49,193}... | collective-permute-start | bytes 1572872 | tf_op jit(solution)/shard_map/ppermute | solution.py:47
  96.4 18.4 %collective-permute-done.13.refs_1_ = bf16[128,2048]{1,0:T(8,128)(2,1)S(1)} collective-permute-done((bf16[128,2048]{1,0:T(8,128)(2,1)S(1)}, bf16[128,2048]{1,0:T(8,128)(2,1)S(1)}, u32[]{:S(2)}, u32[]{:S(2)}) %collective-permute-start.13) | collective-permute-done | bytes 524320 | tf_op jit(solution)/shard_map/ppermute | solution.py:47
  117.5 4.8 %collective-permute-start.15 = (bf16[128,2048]{1,0:T(8,128)(2,1)}, bf16[128,2048]{1,0:T(8,128)(2,1)}, u32[]{:S(2)}, u32[]{:S(2)}) collective-permute-start(bf16[128,2048]{1,0:T(8,128)(2,1)} %get-tuple-element.38), channel_id=1, source_target_pairs={{0,176},{1,145},{16,128},{17,161},{32,144},{33,177},{48,160},{49,1... | collective-permute-start | bytes 1572872 | tf_op jit(solution)/shard_map/ppermute | solution.py:47
  122.3 17.7 %collective-permute-done.17.refs_1_ = bf16[128,2048]{1,0:T(8,128)(2,1)S(1)} collective-permute-done((bf16[128,2048]{1,0:T(8,128)(2,1)S(1)}, bf16[128,2048]{1,0:T(8,128)(2,1)S(1)}, u32[]{:S(2)}, u32[]{:S(2)}) %collective-permute-start.17) | collective-permute-done | bytes 524320 | tf_op jit(solution)/shard_map/ppermute | solution.py:47
  140.0 2.8 %experts.5 = (bf16[128,2048]{1,0:T(8,128)(2,1)}, bf16[128,2048]{1,0:T(8,128)(2,1)}) custom-call(bf16[128,2048]{1,0:T(8,128)(2,1)S(1)} %collective-permute-done.16.refs_0_, bf16[128,2048]{1,0:T(8,128)(2,1)S(1)} %collective-permute-done.17.refs_1_, bf16[2048,512]{1,0:T(8,128)(2,1)S(1)} %bitcast.36, bf16[2048,512]{1,0:T(8,128)(2,1)S(1)} %bitcast.40, ...), custom_call_target="tpu_custom_call" | custom-call | flops 1610612736 | bytes 8388608 | tf_op jit(solution)/shard_map/experts/pallas_call | solution.py:257
  142.8 5.4 %collective-permute-start.18 = (bf16[128,2048]{1,0:T(8,128)(2,1)}, bf16[128,2048]{1,0:T(8,128)(2,1)}, u32[]{:S(2)}, u32[]{:S(2)}) collective-permute-start(bf16[128,2048]{1,0:T(8,128)(2,1)} %get-tuple-element.41), channel_id=1, source_target_pairs={{0,160},{1,1},{16,176},{17,17},{32,128},{33,33},{48,144},{49,49},{... | collective-permute-start | bytes 1572872 | tf_op jit(solution)/shard_map/ppermute | solution.py:47
  148.2 3.6 %collective-permute-start.19 = (bf16[128,2048]{1,0:T(8,128)(2,1)}, bf16[128,2048]{1,0:T(8,128)(2,1)}, u32[]{:S(2)}, u32[]{:S(2)}) collective-permute-start(bf16[128,2048]{1,0:T(8,128)(2,1)} %get-tuple-element.42), channel_id=1, source_target_pairs={{0,32},{1,129},{16,48},{17,145},{32,0},{33,161},{48,16},{49,177},{... | collective-permute-start | bytes 1572872 | tf_op jit(solution)/shard_map/ppermute | solution.py:47
  157.7 18.0 %collective-permute-done.19.refs_3_ = bf16[128,2048]{1,0:T(8,128)(2,1)} collective-permute-done((bf16[128,2048]{1,0:T(8,128)(2,1)}, bf16[128,2048]{1,0:T(8,128)(2,1)}, u32[]{:S(2)}, u32[]{:S(2)}) %collective-permute-start.19) | collective-permute-done | bytes 524320 | tf_op jit(solution)/shard_map/ppermute | solution.py:47
  175.7 4.1 %collective-permute-done.22.refs_4_ = bf16[128,2048]{1,0:T(8,128)(2,1)} collective-permute-done((bf16[128,2048]{1,0:T(8,128)(2,1)}, bf16[128,2048]{1,0:T(8,128)(2,1)}, u32[]{:S(2)}, u32[]{:S(2)}) %collective-permute-start.22) | collective-permute-done | bytes 524320 | tf_op jit(solution)/shard_map/ppermute | solution.py:47
  180.9 6.0 %gather.1 = (f32[256,2048]{1,0:T(8,128)}, f32[256,2048]{1,0:T(8,128)S(1)}) custom-call(f32[256,2048]{1,0:T(8,128)} %get-tuple-element.32.acc_ref, s32[256,2]{1,0:T(8,128)S(1)} %copy.52.place_ref, f32[256,2]{1,0:T(8,128)S(1)} %copy.53.weight_ref, s32[256,2]{1,0:T(8,128)S(1)} %copy.54.place2_ref, f32[256,2]{1,0:T(8,128)S(1)} %get-tuple-element.61.weight2_ref, ...), custom_call_target="tpu_custom_call" | custom-call | flops 1610612736 | bytes 10485760 | tf_op jit(solution)/shard_map/gather/pallas_call | solution.py:299
  186.9 9.4 %collective-permute-start.25 = (bf16[128,2048]{1,0:T(8,128)(2,1)S(1)}, bf16[128,2048]{1,0:T(8,128)(2,1)S(1)}, u32[]{:S(2)}, u32[]{:S(2)}) collective-permute-start(bf16[128,2048]{1,0:T(8,128)(2,1)S(1)} %copy-done.8), channel_id=1, source_target_pairs={{0,64},{1,193},{16,80},{17,209},{32,96},{33,225},{48,112},{49,241}... | collective-permute-start | bytes 1572872 | tf_op jit(solution)/shard_map/ppermute | solution.py:47
  196.3 9.5 %collective-permute-done.25.refs_0_ = bf16[128,2048]{1,0:T(8,128)(2,1)S(1)} collective-permute-done((bf16[128,2048]{1,0:T(8,128)(2,1)S(1)}, bf16[128,2048]{1,0:T(8,128)(2,1)S(1)}, u32[]{:S(2)}, u32[]{:S(2)}) %collective-permute-start.25) | collective-permute-done | bytes 524320 | tf_op jit(solution)/shard_map/ppermute | solution.py:47
  217.6 3.1 %collective-permute-done.29.refs_2_ = bf16[64,2048]{1,0:T(8,128)(2,1)S(1)} collective-permute-done((bf16[64,2048]{1,0:T(8,128)(2,1)S(1)}, bf16[64,2048]{1,0:T(8,128)(2,1)S(1)}, u32[]{:S(2)}, u32[]{:S(2)}) %collective-permute-start.29) | collective-permute-done | bytes 262176 | tf_op jit(solution)/shard_map/ppermute | solution.py:47
  222.3 4.9 %finish.1 = bf16[256,2048]{1,0:T(8,128)(2,1)} custom-call(f32[256,2048]{1,0:T(8,128)} %get-tuple-element.47.acc_ref, f32[256,2048]{1,0:T(8,128)S(1)} %collective-permute-done.24.more_ref, s32[256,2]{1,0:T(8,128)S(1)} %copy.52.place_ref, f32[256,2]{1,0:T(8,128)S(1)} %copy.53.weight_ref, bf16[64,2048]{1,0:T(8,128)(2,1)S(1)} %collective-permute-done.27.refs_0_, ...), custom_call_target="tpu_custom_call" | custom-call | flops 536870912 | bytes 6291456 | tf_op jit(solution)/shard_map/finish/pallas_call | solution.py:331
  (140 shorter events, 56.6 us)
Async XLA Ops:
  0.0 21.2 %collective-permute-start.2 = (bf16[64,2048]{1,0:T(8,128)(2,1)}, bf16[64,2048]{1,0:T(8,128)(2,1)S(1)}, u32[]{:S(2)}, u32[]{:S(2)}) collective-permute-start(bf16[64,2048]{1,0:T(8,128)(2,1)} %refs_0_.1), channel_id=1, source_target_pairs={{0,14},{2,0},{4,2},{6,4},{8,6},{10,8},{12,10},{14,12},{1,15},{3,1}... | collective-permute-start | bytes 786440 | tf_op jit(solution)/shard_map/ppermute | solution.py:47
  6.4 14.8 %collective-permute-start.1 = (bf16[64,2048]{1,0:T(8,128)(2,1)}, bf16[64,2048]{1,0:T(8,128)(2,1)S(1)}, u32[]{:S(2)}, u32[]{:S(2)}) collective-permute-start(bf16[64,2048]{1,0:T(8,128)(2,1)} %refs_0_.1), channel_id=1, source_target_pairs={{0,2},{2,4},{4,6},{6,8},{8,10},{10,12},{12,14},{14,0},{1,3},{3,5},... | collective-permute-start | bytes 786440 | tf_op jit(solution)/shard_map/ppermute | solution.py:47
  8.0 8.9 %collective-permute-start = (f32[65,2]{1,0:T(8,128)S(1)}, f32[65,2]{1,0:T(8,128)S(1)}, u32[]{:S(2)}, u32[]{:S(2)}) collective-permute-start(f32[65,2]{1,0:T(8,128)S(1)} %pad_maximum_fusion.1), channel_id=1, source_target_pairs={{0,16},{16,32},{32,48},{48,64},{64,80},{80,96},{96,112},{112,128},... | collective-permute-start | bytes 1568 | tf_op jit(solution)/shard_map/ppermute | solution.py:389
  21.3 8.5 %collective-permute-start.4 = (bf16[64,2048]{1,0:T(8,128)(2,1)S(1)}, bf16[64,2048]{1,0:T(8,128)(2,1)S(1)}, u32[]{:S(2)}, u32[]{:S(2)}) collective-permute-start(bf16[64,2048]{1,0:T(8,128)(2,1)S(1)} %collective-permute-done.2.refs_2_), channel_id=1, source_target_pairs={{0,14},{2,0},{4,2},{6,4},{8,6},{10,8},{12,10},{14,12},{1,15},{3,1}... | collective-permute-start | bytes 786440 | tf_op jit(solution)/shard_map/ppermute | solution.py:47
  30.5 31.3 %collective-permute-start.8 = (bf16[320,2048]{1,0:T(8,128)(2,1)}, bf16[320,2048]{1,0:T(8,128)(2,1)S(1)}, u32[]{:S(2)}, u32[]{:S(2)}) collective-permute-start(bf16[320,2048]{1,0:T(8,128)(2,1)} %constant_dynamic-update-slice_fusion), channel_id=1, source_target_pairs={{0,1},{1,0},{2,3},{3,2},{4,5},{5,4},{6,7},{7,6},{8,9},{9,8},{10,11... | collective-permute-start | bytes 3932168 | tf_op jit(solution)/shard_map/ppermute | solution.py:47
  32.6 12.1 %collective-permute-start.6 = (bf16[64,2048]{1,0:T(8,128)(2,1)S(1)}, bf16[64,2048]{1,0:T(8,128)(2,1)}, u32[]{:S(2)}, u32[]{:S(2)}) collective-permute-start(bf16[64,2048]{1,0:T(8,128)(2,1)S(1)} %collective-permute-done.4.refs_4_), channel_id=1, source_target_pairs={{0,14},{2,0},{4,2},{6,4},{8,6},{10,8},{12,10},{14,12},{1,15},{3,1}... | collective-permute-start | bytes 786440 | tf_op jit(solution)/shard_map/ppermute | solution.py:47
  36.1 8.7 %collective-permute-start.7 = (bf16[64,2048]{1,0:T(8,128)(2,1)S(1)}, bf16[64,2048]{1,0:T(8,128)(2,1)}, u32[]{:S(2)}, u32[]{:S(2)}) collective-permute-start(bf16[64,2048]{1,0:T(8,128)(2,1)S(1)} %collective-permute-done.5.refs_5_), channel_id=1, source_target_pairs={{0,2},{2,4},{4,6},{6,8},{8,10},{10,12},{12,14},{14,0},{1,3},{3,5},... | collective-permute-start | bytes 786440 | tf_op jit(solution)/shard_map/ppermute | solution.py:47
  36.9 25.0 %all-to-all-start = ((bf16[16,64,256]{2,1,0:T(8,128)(2,1)}), bf16[16,64,256]{2,1,0:T(8,128)(2,1)S(1)}, u32[]{:S(2)}, u32[]{:S(2)}) async-start(bf16[16,64,256]{2,1,0:T(8,128)(2,1)} %conv.1), calls=%async_computation | async-start | bytes 1048576 | tf_op jit(solution)/shard_map/all_to_all | solution.py:402
  46.8 15.1 %collective-permute-start.9 = (bf16[192,2048]{1,0:T(8,128)(2,1)}, bf16[192,2048]{1,0:T(8,128)(2,1)}, u32[]{:S(2)}, u32[]{:S(2)}) collective-permute-start(bf16[192,2048]{1,0:T(8,128)(2,1)} %pad_maximum_fusion), channel_id=1, source_target_pairs={{0,1},{1,0},{2,3},{3,2},{4,5},{5,4},{6,7},{7,6},{8,9},{9,8},{10,11... | collective-permute-start | bytes 2359304 | tf_op jit(solution)/shard_map/ppermute | solution.py:47
  74.1 16.7 %collective-permute-start.12 = (bf16[128,2048]{1,0:T(8,128)(2,1)S(1)}, bf16[128,2048]{1,0:T(8,128)(2,1)S(1)}, u32[]{:S(2)}, u32[]{:S(2)}) collective-permute-start(bf16[128,2048]{1,0:T(8,128)(2,1)S(1)} %get-tuple-element.35), channel_id=1, source_target_pairs={{0,96},{1,225},{16,112},{17,241},{32,64},{33,193},{48,80},{49,209}... | collective-permute-start | bytes 1572872 | tf_op jit(solution)/shard_map/ppermute | solution.py:47
  79.0 35.8 %collective-permute-start.13 = (bf16[128,2048]{1,0:T(8,128)(2,1)S(1)}, bf16[128,2048]{1,0:T(8,128)(2,1)S(1)}, u32[]{:S(2)}, u32[]{:S(2)}) collective-permute-start(bf16[128,2048]{1,0:T(8,128)(2,1)S(1)} %get-tuple-element.36), channel_id=1, source_target_pairs={{0,144},{1,177},{16,160},{17,129},{32,176},{33,145},{48,128},{49,1... | collective-permute-start | bytes 1572872 | tf_op jit(solution)/shard_map/ppermute | solution.py:47
  80.2 37.3 %collective-permute-start.16 = (bf16[128,2048]{1,0:T(8,128)(2,1)S(1)}, bf16[128,2048]{1,0:T(8,128)(2,1)S(1)}, u32[]{:S(2)}, u32[]{:S(2)}) collective-permute-start(bf16[128,2048]{1,0:T(8,128)(2,1)S(1)} %get-tuple-element.39), channel_id=1, source_target_pairs={{0,160},{1,1},{16,176},{17,17},{32,128},{33,33},{48,144},{49,49},{... | collective-permute-start | bytes 1572872 | tf_op jit(solution)/shard_map/ppermute | solution.py:47
  81.1 58.9 %collective-permute-start.17 = (bf16[128,2048]{1,0:T(8,128)(2,1)S(1)}, bf16[128,2048]{1,0:T(8,128)(2,1)S(1)}, u32[]{:S(2)}, u32[]{:S(2)}) collective-permute-start(bf16[128,2048]{1,0:T(8,128)(2,1)S(1)} %get-tuple-element.40), channel_id=1, source_target_pairs={{0,32},{1,129},{16,48},{17,145},{32,0},{33,161},{48,16},{49,177},{... | collective-permute-start | bytes 1572872 | tf_op jit(solution)/shard_map/ppermute | solution.py:47
  83.8 64.4 %collective-permute-start.20 = (bf16[128,2048]{1,0:T(8,128)(2,1)S(1)}, bf16[128,2048]{1,0:T(8,128)(2,1)S(1)}, u32[]{:S(2)}, u32[]{:S(2)}) collective-permute-start(bf16[128,2048]{1,0:T(8,128)(2,1)S(1)} %get-tuple-element.43), channel_id=1, source_target_pairs={{0,80},{1,241},{16,96},{17,193},{32,112},{33,209},{48,64},{49,225}... | collective-permute-start | bytes 1572872 | tf_op jit(solution)/shard_map/ppermute | solution.py:47
  90.8 60.9 %collective-permute-start.21 = (bf16[128,2048]{1,0:T(8,128)(2,1)S(1)}, bf16[128,2048]{1,0:T(8,128)(2,1)S(1)}, u32[]{:S(2)}, u32[]{:S(2)}) collective-permute-start(bf16[128,2048]{1,0:T(8,128)(2,1)S(1)} %get-tuple-element.44), channel_id=1, source_target_pairs={{0,112},{1,209},{16,64},{17,225},{32,80},{33,241},{48,96},{49,193}... | collective-permute-start | bytes 1572872 | tf_op jit(solution)/shard_map/ppermute | solution.py:47
  117.5 37.1 %collective-permute-start.14 = (bf16[128,2048]{1,0:T(8,128)(2,1)S(1)}, bf16[128,2048]{1,0:T(8,128)(2,1)S(1)}, u32[]{:S(2)}, u32[]{:S(2)}) collective-permute-start(bf16[128,2048]{1,0:T(8,128)(2,1)S(1)} %get-tuple-element.37), channel_id=1, source_target_pairs={{0,224},{1,97},{16,240},{17,113},{32,192},{33,65},{48,208},{49,81}... | collective-permute-start | bytes 1572872 | tf_op jit(solution)/shard_map/ppermute | solution.py:47
  117.5 40.2 %collective-permute-start.15 = (bf16[128,2048]{1,0:T(8,128)(2,1)}, bf16[128,2048]{1,0:T(8,128)(2,1)}, u32[]{:S(2)}, u32[]{:S(2)}) collective-permute-start(bf16[128,2048]{1,0:T(8,128)(2,1)} %get-tuple-element.38), channel_id=1, source_target_pairs={{0,176},{1,145},{16,128},{17,161},{32,144},{33,177},{48,160},{49,1... | collective-permute-start | bytes 1572872 | tf_op jit(solution)/shard_map/ppermute | solution.py:47
  142.8 14.9 %collective-permute-start.18 = (bf16[128,2048]{1,0:T(8,128)(2,1)}, bf16[128,2048]{1,0:T(8,128)(2,1)}, u32[]{:S(2)}, u32[]{:S(2)}) collective-permute-start(bf16[128,2048]{1,0:T(8,128)(2,1)} %get-tuple-element.41), channel_id=1, source_target_pairs={{0,160},{1,1},{16,176},{17,17},{32,128},{33,33},{48,144},{49,49},{... | collective-permute-start | bytes 1572872 | tf_op jit(solution)/shard_map/ppermute | solution.py:47
  148.2 27.5 %collective-permute-start.19 = (bf16[128,2048]{1,0:T(8,128)(2,1)}, bf16[128,2048]{1,0:T(8,128)(2,1)}, u32[]{:S(2)}, u32[]{:S(2)}) collective-permute-start(bf16[128,2048]{1,0:T(8,128)(2,1)} %get-tuple-element.42), channel_id=1, source_target_pairs={{0,32},{1,129},{16,48},{17,145},{32,0},{33,161},{48,16},{49,177},{... | collective-permute-start | bytes 1572872 | tf_op jit(solution)/shard_map/ppermute | solution.py:47
  154.5 25.3 %collective-permute-start.22 = (bf16[128,2048]{1,0:T(8,128)(2,1)}, bf16[128,2048]{1,0:T(8,128)(2,1)}, u32[]{:S(2)}, u32[]{:S(2)}) collective-permute-start(bf16[128,2048]{1,0:T(8,128)(2,1)} %get-tuple-element.45), channel_id=1, source_target_pairs={{0,240},{1,81},{16,192},{17,97},{32,208},{33,113},{48,224},{49,65}... | collective-permute-start | bytes 1572872 | tf_op jit(solution)/shard_map/ppermute | solution.py:47
  155.4 24.4 %collective-permute-start.23 = (bf16[128,2048]{1,0:T(8,128)(2,1)}, bf16[128,2048]{1,0:T(8,128)(2,1)}, u32[]{:S(2)}, u32[]{:S(2)}) collective-permute-start(bf16[128,2048]{1,0:T(8,128)(2,1)} %get-tuple-element.46), channel_id=1, source_target_pairs={{0,208},{1,113},{16,224},{17,65},{32,240},{33,81},{48,192},{49,97}... | collective-permute-start | bytes 1572872 | tf_op jit(solution)/shard_map/ppermute | solution.py:47
  186.9 35.4 %collective-permute-start.24 = (f32[256,2048]{1,0:T(8,128)S(1)}, f32[256,2048]{1,0:T(8,128)S(1)}, u32[]{:S(2)}, u32[]{:S(2)}) collective-permute-start(f32[256,2048]{1,0:T(8,128)S(1)} %get-tuple-element.48), channel_id=1, source_target_pairs={{0,1},{1,0},{2,3},{3,2},{4,5},{5,4},{6,7},{7,6},{8,9},{9,8},{10,11... | collective-permute-start | bytes 6291464 | tf_op jit(solution)/shard_map/ppermute | solution.py:47
  186.9 18.9 %collective-permute-start.25 = (bf16[128,2048]{1,0:T(8,128)(2,1)S(1)}, bf16[128,2048]{1,0:T(8,128)(2,1)S(1)}, u32[]{:S(2)}, u32[]{:S(2)}) collective-permute-start(bf16[128,2048]{1,0:T(8,128)(2,1)S(1)} %copy-done.8), channel_id=1, source_target_pairs={{0,64},{1,193},{16,80},{17,209},{32,96},{33,225},{48,112},{49,241}... | collective-permute-start | bytes 1572872 | tf_op jit(solution)/shard_map/ppermute | solution.py:47
  196.3 11.5 %collective-permute-start.26 = (bf16[128,2048]{1,0:T(8,128)(2,1)S(1)}, bf16[128,2048]{1,0:T(8,128)(2,1)S(1)}, u32[]{:S(2)}, u32[]{:S(2)}) collective-permute-start(bf16[128,2048]{1,0:T(8,128)(2,1)S(1)} %get-tuple-element.50), channel_id=1, source_target_pairs={{0,16},{1,49},{16,32},{17,1},{32,48},{33,17},{48,0},{49,33},{64,80... | collective-permute-start | bytes 1572872 | tf_op jit(solution)/shard_map/ppermute | solution.py:47
  (33 other events, 407.6 us)

commit v2 on v1

--- a/solution.py
+++ b/solution.py
@@ -24,15 +24,17 @@
 CHIP = ("y", "x", "c")
 
 PAIRS = (
-    ((1, 2), (3, 2)),
-    ((2, 1), (2, 3)),
-    ((2, 2), (0, 0)),
-    ((0, 2), (2, 0)),
-    ((1, 1), (3, 3)),
-    ((1, 3), (3, 1)),
+    ((0, 0), (0, 0)),
+    ((1, 1), (0, 2)),
+    ((1, 3), (1, 1)),
+    ((0, 2), (1, 3)),
+    ((0, 1), (0, 3)),
+    ((0, 3), (0, 1)),
     ((1, 0), (3, 0)),
-    ((0, 1), (0, 3)),
+    ((3, 0), (1, 0)),
 )
+EXPERTS_AT = np.array([[a, (b[0] + 2, b[1] + 2)] for a, b in PAIRS], np.int32) % 4
+assert len({tuple(d) for pair in EXPERTS_AT.tolist() for d in pair}) == 16
 GROUPS = ((0, 1), (2, 3), (4, 5), (6, 7))
 
 VMEM = pl.BlockSpec(memory_space=pltpu.VMEM)
@@ -52,7 +54,13 @@
         dy, dx = PAIRS[op][c]
         return (y + sign * dy, x + sign * dx, c + cross)
 
+    if op == 0 and not cross:
+        return value
     return permute(value, CHIP, (4, 4, 2), move)
+
+
+def hosted(value):
+    return permute(value, CHIP, (4, 4, 2), lambda y, x, c: (y - 2 * c, x - 2 * c, c))
 
 
 def along_z(value, step):
@@ -289,7 +297,7 @@
     own = weighted(place_ref[...], weight_ref[...], 0, count)
     mine_ref[...] = acc_ref[...] + apply(own, mine[...])
     other = weighted(place2_ref[...], weight2_ref[...], 0, count)
-    theirs_ref[...] = apply(other, theirs[...])
+    theirs_ref[...] = apply(other, theirs[...]).astype(jnp.bfloat16)
 
 
 def gather(acc, place, weight, place2, weight2, bufs):
@@ -301,7 +309,7 @@
         grid=(WIDTH // TILE,),
         out_shape=[
             pltpu.HBM((ROWS, WIDTH), jnp.float32),
-            jax.ShapeDtypeStruct((ROWS, WIDTH), jnp.float32),
+            jax.ShapeDtypeStruct((ROWS, WIDTH), jnp.bfloat16),
         ],
         in_specs=[block] + [pair] * 4 + [pl.BlockSpec((2 * CHUNK, TILE), lambda i: (0, i))] * n,
         out_specs=[block, block],
@@ -319,7 +327,7 @@
     half = n // 2 * CHUNK
     mine = weighted(place_ref[...], weight_ref[...], first, half)
     theirs = weighted(place_ref[...], weight_ref[...], first + 8 * CHUNK, half)
-    total = acc_ref[...] + more_ref[...]
+    total = acc_ref[...] + more_ref[...].astype(jnp.float32)
     total = total + apply(mine, rows[:half]) + apply(theirs, rows[half:])
     out_ref[...] = total.astype(out_ref.dtype)
 
@@ -383,6 +391,10 @@
 ):
     y, x, z, c = (lax.axis_index(a) for a in ("y", "x", "z", "c"))
 
+    wg = hosted(w_gate[0])
+    wu = hosted(w_up[0])
+    wd = hosted(w_down[0])
+
     last = in_gate[:, -2:].astype(jnp.float32) * conv_in[:, -2:].astype(jnp.float32)
     doc_value = doc_ids.astype(jnp.float32)
     tail = jnp.concatenate([last, doc_value[None, -2:]], axis=0)
@@ -415,9 +427,8 @@
     routes = jnp.concatenate([route_ids.astype(jnp.float32), route_weight], axis=1).T
     routes = after(routes, head_normed)
     other = swap_cores(routes)
-    table = np.array(PAIRS, np.int32)
-    first_core = jnp.asarray(table[:, 0])
-    second_core = jnp.asarray(table[:, 1])
+    first_core = jnp.asarray(EXPERTS_AT[:, 0])
+    second_core = jnp.asarray(EXPERTS_AT[:, 1])
     mine_d = jnp.where(c == 0, first_core, second_core)
     theirs_d = jnp.where(c == 0, second_core, first_core)
 
@@ -433,10 +444,10 @@
 
     where = jnp.stack([z, c]).astype(jnp.int32)
     stream, normed = mix(where, by_row, own, swapped, resid, norm_gain[None])
-    sends = pack(normed, swap_cores(normed), rows_mine[:8], rows_theirs)
+    normed_theirs = swap_cores(normed)
+    sends = pack(normed, normed_theirs, rows_mine[:8], rows_theirs)
     arrived = [displaced(s, k, 1) for k, s in enumerate(sends)]
 
-    wg, wu, wd = w_gate[0], w_up[0], w_down[0]
     back = []
     for n, group in enumerate(GROUPS):
         final = n == len(GROUPS) - 1

time: 228 us -> 232 us (1.018)
  waiting for transfers between devices: 101 us -> 70.5 us
  starting transfers between devices: 73.7 us -> 93.6 us
  Pallas kernels: 33.1 us -> 42.1 us
  local copies, waits for them, and re-layouts: 9.76 us -> 12.2 us
    ppermute x30 -> x31, waiting for transfers between devices: 89.9 us -> 70.5 us  [permute(): return lax.ppermute(value, axes, pairs)]
    ppermute x30 -> x31, starting transfers between devices: 62.8 us -> 81.7 us  [permute(): return lax.ppermute(value, axes, pairs)]
    all_to_all x1, waiting for transfers between devices: 11.6 us -> 0.01 us  [body(): lax.all_to_all(head_normed, TP, split_axis=0, concat_axis=0, tiled=True)]
    pallas_call x4, Pallas kernels: 10.2 us -> 19.2 us  [experts(): pl.pallas_call(functools.partial(expert_kernel, len(bufs)), out_shape=[ja...]
    unnamed x56 -> x42, local copies, waits for them, and re-layouts: 7.52 us -> 8.48 us
  transfers between devices with their start and end apart: 32 -> 33, of which waited for: 15 -> 13; matrix products, arithmetic and copies ran while one was open for 7% -> 8% of each run, Pallas kernels for 6% -> 14%
where the time goes in v2:
time: 232 us; the launch traced here: 229 us
  starting transfers between devices  93.6 us (40%)
  waiting for transfers between devices  70.5 us (30%)
  Pallas kernels  42.1 us (18%)
  local copies, waits for them, and re-layouts  12.2 us (5%)
  other arithmetic  7.88 us (3%)
  matrix products  2.5 us (1%)
    ppermute x31, starting transfers between devices, permute(): return lax.ppermute(value, axes, pairs)  81.7 us
    ppermute x31, waiting for transfers between devices, permute(): return lax.ppermute(value, axes, pairs)  70.5 us
    pallas_call x4, Pallas kernels, experts(): pl.pallas_call(functools.partial(expert_kernel, len(bufs)), out_shape=[ja...  19.2 us
    all_to_all x1, starting transfers between devices, body(): lax.all_to_all(head_normed, TP, split_axis=0, concat_axis=0, tiled=True)  8.76 us
    unnamed x42, local copies, waits for them, and re-layouts  8.48 us
    pallas_call x1, Pallas kernels, gather(): pl.pallas_call(functools.partial(gather_kernel, n), grid=(WIDTH // TILE,)...  5.92 us
    pallas_call x1, Pallas kernels, mix(): pl.pallas_call(mix_kernel, grid=(WIDTH // TILE,), out_shape=[pltpu.HBM((R...  5.76 us
    pallas_call x1, Pallas kernels, finish(): pl.pallas_call(functools.partial(finish_kernel, first, n), grid=(WIDTH //...  4.85 us
  transfers between devices with their start and end apart: 33, of which 13 were waited for; matrix products, arithmetic and copies ran while one was open for 8% of the time, Pallas kernels for 14%

profile of v2, /device:TPU:1, one launch (start us, length us, event | category | flops | bytes accessed | tf_op | source)
XLA Modules:
  0.0 229.2 jit_solution(6848771706357002726)
XLA Ops:
  2.5 3.9 %collective-permute-start.2 = (bf16[64,2048]{1,0:T(8,128)(2,1)}, bf16[64,2048]{1,0:T(8,128)(2,1)S(1)}, u32[]{:S(2)}, u32[]{:S(2)}) collective-permute-start(bf16[64,2048]{1,0:T(8,128)(2,1)} %refs_0_.1), channel_id=1, source_target_pairs={{0,14},{2,0},{4,2},{6,4},{8,6},{10,8},{12,10},{14,12},{1,15},{3,1}... | collective-permute-start | bytes 786440 | tf_op jit(solution)/shard_map/ppermute | solution.py:49
  11.2 7.0 %collective-permute-start.13 = (bf16[2048,512]{1,0:T(8,128)(2,1)}, bf16[2048,512]{1,0:T(8,128)(2,1)S(1)}, u32[]{:S(2)}, u32[]{:S(2)}) collective-permute-start(bf16[2048,512]{1,0:T(8,128)(2,1)} %bitcast.49), channel_id=1, source_target_pairs={{0,0},{1,161},{16,16},{17,177},{32,32},{33,129},{48,48},{49,145},{... | collective-permute-start | bytes 6291464 | tf_op jit(solution)/shard_map/ppermute | solution.py:49
  25.7 4.0 %conv.1 = bf16[16,64,256]{2,1,0:T(8,128)(2,1)} custom-call(bf16[64,4096]{1,0:T(8,128)(2,1)} %a_ref.1, bf16[64,4096]{1,0:T(8,128)(2,1)} %b_ref.1, bf16[64,4096]{1,0:T(8,128)(2,1)} %o_ref.1, f32[1,4096]{1,0:T(1,128)S(1)} %bitcast.36, f32[1,4096]{1,0:T(1,128)S(1)} %bitcast.35, f32[64,256]{1,0:T(8,128)S(1)} %pad.4.halo_ref, f32[64,3]{1,0:T(8,128)S(1)} %copy.49.taps_ref, ...), custom_call_target="tpu_custom_call" | custom-call | flops 200000000 | bytes 2097152 | tf_op jit(solution)/shard_map/conv/pallas_call | solution.py:122
  38.8 12.6 %collective-permute-start.8 = (bf16[320,2048]{1,0:T(8,128)(2,1)}, bf16[320,2048]{1,0:T(8,128)(2,1)}, u32[]{:S(2)}, u32[]{:S(2)}) collective-permute-start(bf16[320,2048]{1,0:T(8,128)(2,1)} %constant_dynamic-update-slice_fusion), channel_id=1, source_target_pairs={{0,1},{1,0},{2,3},{3,2},{4,5},{5,4},{6,7},{7,6},{8,9},{9,8},{10,11... | collective-permute-start | bytes 3932168 | tf_op jit(solution)/shard_map/ppermute | solution.py:49
  55.0 8.8 %all-to-all-start = ((bf16[16,64,256]{2,1,0:T(8,128)(2,1)}), bf16[16,64,256]{2,1,0:T(8,128)(2,1)S(1)}, u32[]{:S(2)}, u32[]{:S(2)}) async-start(bf16[16,64,256]{2,1,0:T(8,128)(2,1)} %conv.1), calls=%async_computation | async-start | bytes 1048576 | tf_op jit(solution)/shard_map/all_to_all | solution.py:414
  63.7 7.0 %collective-permute-start.15 = (bf16[512,2048]{1,0:T(8,128)(2,1)}, bf16[512,2048]{1,0:T(8,128)(2,1)}, u32[]{:S(2)}, u32[]{:S(2)}) collective-permute-start(bf16[512,2048]{1,0:T(8,128)(2,1)} %bitcast.51), channel_id=1, source_target_pairs={{0,0},{1,161},{16,16},{17,177},{32,32},{33,129},{48,48},{49,145},{... | collective-permute-start | bytes 6291464 | tf_op jit(solution)/shard_map/ppermute | solution.py:49
  72.8 10.3 %collective-permute-start.9 = (bf16[192,2048]{1,0:T(8,128)(2,1)}, bf16[192,2048]{1,0:T(8,128)(2,1)}, u32[]{:S(2)}, u32[]{:S(2)}) collective-permute-start(bf16[192,2048]{1,0:T(8,128)(2,1)} %pad_maximum_fusion), channel_id=1, source_target_pairs={{0,1},{1,0},{2,3},{3,2},{4,5},{5,4},{6,7},{7,6},{8,9},{9,8},{10,11... | collective-permute-start | bytes 2359304 | tf_op jit(solution)/shard_map/ppermute | solution.py:49
  88.6 5.8 %mix.1 = (f32[256,2048]{1,0:T(8,128)}, bf16[256,2048]{1,0:T(8,128)(2,1)S(1)}) custom-call(s32[2]{0:T(128)S(1)} %pad_add_fusion.2.where_ref, bf16[16,64,256]{2,1,0:T(8,128)(2,1)S(1)} %all-to-all-done.by_row_ref, bf16[64,2048]{1,0:T(8,128)(2,1)S(1)} %copy-done, bf16[64,2048]{1,0:T(8,128)(2,1)S(1)} %collective-permute-done.1.refs_1_, ...), custom_call_target="tpu_custom_call" | custom-call | flops 1100000000 | bytes 8388608 | tf_op jit(solution)/shard_map/mix/pallas_call | solution.py:178
  108.4 5.7 %collective-permute-done.21.refs_0_ = bf16[128,2048]{1,0:T(8,128)(2,1)S(1)} collective-permute-done((bf16[128,2048]{1,0:T(8,128)(2,1)S(1)}, bf16[128,2048]{1,0:T(8,128)(2,1)S(1)}, u32[]{:S(2)}, u32[]{:S(2)}) %collective-permute-start.21) | collective-permute-done | bytes 524320 | tf_op jit(solution)/shard_map/ppermute | solution.py:49
  114.1 5.4 %collective-permute-done.22.refs_1_ = bf16[128,2048]{1,0:T(8,128)(2,1)S(1)} collective-permute-done((bf16[128,2048]{1,0:T(8,128)(2,1)S(1)}, bf16[128,2048]{1,0:T(8,128)(2,1)S(1)}, u32[]{:S(2)}, u32[]{:S(2)}) %collective-permute-start.22) | collective-permute-done | bytes 524320 | tf_op jit(solution)/shard_map/ppermute | solution.py:49
  119.5 5.1 %experts.6 = (bf16[128,2048]{1,0:T(8,128)(2,1)}, bf16[128,2048]{1,0:T(8,128)(2,1)}) custom-call(bf16[128,2048]{1,0:T(8,128)(2,1)S(1)} %collective-permute-done.21.refs_0_, bf16[128,2048]{1,0:T(8,128)(2,1)S(1)} %collective-permute-done.22.refs_1_, bf16[2048,512]{1,0:T(8,128)(2,1)S(1)} %collective-permute-done.13.refs_2_, ...), custom_call_target="tpu_custom_call" | custom-call | flops 1610612736 | bytes 8388608 | tf_op jit(solution)/shard_map/experts/pallas_call | solution.py:265
  127.2 12.9 %collective-permute-done.17.refs_0_ = bf16[128,2048]{1,0:T(8,128)(2,1)S(1)} collective-permute-done((bf16[128,2048]{1,0:T(8,128)(2,1)S(1)}, bf16[128,2048]{1,0:T(8,128)(2,1)S(1)}, u32[]{:S(2)}, u32[]{:S(2)}) %collective-permute-start.17) | collective-permute-done | bytes 524320 | tf_op jit(solution)/shard_map/ppermute | solution.py:49
  140.2 5.1 %experts.5 = (bf16[128,2048]{1,0:T(8,128)(2,1)}, bf16[128,2048]{1,0:T(8,128)(2,1)}) custom-call(bf16[128,2048]{1,0:T(8,128)(2,1)S(1)} %collective-permute-done.17.refs_0_, bf16[128,2048]{1,0:T(8,128)(2,1)S(1)} %collective-permute-done.18.refs_1_, bf16[2048,512]{1,0:T(8,128)(2,1)S(1)} %collective-permute-done.13.refs_2_, ...), custom_call_target="tpu_custom_call" | custom-call | flops 1610612736 | bytes 8388608 | tf_op jit(solution)/shard_map/experts/pallas_call | solution.py:265
  145.3 4.4 %collective-permute-start.20 = (bf16[128,2048]{1,0:T(8,128)(2,1)}, bf16[128,2048]{1,0:T(8,128)(2,1)}, u32[]{:S(2)}, u32[]{:S(2)}) collective-permute-start(bf16[128,2048]{1,0:T(8,128)(2,1)} %get-tuple-element.42), channel_id=1, source_target_pairs={{0,32},{1,209},{16,48},{17,225},{32,0},{33,241},{48,16},{49,193},{... | collective-permute-start | bytes 1572872 | tf_op jit(solution)/shard_map/ppermute | solution.py:49
  149.6 4.9 %experts.4 = (bf16[128,2048]{1,0:T(8,128)(2,1)S(1)}, bf16[128,2048]{1,0:T(8,128)(2,1)}) custom-call(bf16[128,2048]{1,0:T(8,128)(2,1)S(1)} %get-tuple-element.35.refs_0_, bf16[128,2048]{1,0:T(8,128)(2,1)S(1)} %collective-permute-done.12.refs_1_, bf16[2048,512]{1,0:T(8,128)(2,1)S(1)} %collective-permute-done.13.refs_2_, ...), custom_call_target="tpu_custom_call" | custom-call | flops 1610612736 | bytes 8388608 | tf_op jit(solution)/shard_map/experts/pallas_call | solution.py:265
  155.9 11.1 %collective-permute-done.19.refs_2_ = bf16[128,2048]{1,0:T(8,128)(2,1)} collective-permute-done((bf16[128,2048]{1,0:T(8,128)(2,1)}, bf16[128,2048]{1,0:T(8,128)(2,1)}, u32[]{:S(2)}, u32[]{:S(2)}) %collective-permute-start.19) | collective-permute-done | bytes 524320 | tf_op jit(solution)/shard_map/ppermute | solution.py:49
  167.0 9.1 %collective-permute-done.16.refs_1_ = bf16[128,2048]{1,0:T(8,128)(2,1)} collective-permute-done((bf16[128,2048]{1,0:T(8,128)(2,1)}, bf16[128,2048]{1,0:T(8,128)(2,1)}, u32[]{:S(2)}, u32[]{:S(2)}) %collective-permute-start.16) | collective-permute-done | bytes 524320 | tf_op jit(solution)/shard_map/ppermute | solution.py:49
  177.2 5.9 %gather.1 = (f32[256,2048]{1,0:T(8,128)}, bf16[256,2048]{1,0:T(8,128)(2,1)S(1)}) custom-call(f32[256,2048]{1,0:T(8,128)} %get-tuple-element.32.acc_ref, s32[256,2]{1,0:T(8,128)S(1)} %copy.52.place_ref, f32[256,2]{1,0:T(8,128)S(1)} %copy.53.weight_ref, s32[256,2]{1,0:T(8,128)S(1)} %copy.54.place2_ref, f32[256,2]{1,0:T(8,128)S(1)} %get-tuple-element.61.weight2_ref, ...), custom_call_target="tpu_custom_call" | custom-call | flops 1610612736 | bytes 10485760 | tf_op jit(solution)/shard_map/gather/pallas_call | solution.py:307
  183.1 4.8 %collective-permute-start.25 = (bf16[256,2048]{1,0:T(8,128)(2,1)S(1)}, bf16[256,2048]{1,0:T(8,128)(2,1)S(1)}, u32[]{:S(2)}, u32[]{:S(2)}) collective-permute-start(bf16[256,2048]{1,0:T(8,128)(2,1)S(1)} %get-tuple-element.48), channel_id=1, source_target_pairs={{0,1},{1,0},{2,3},{3,2},{4,5},{5,4},{6,7},{7,6},{8,9},{9,8},{10,11... | collective-permute-start | bytes 3145736 | tf_op jit(solution)/shard_map/ppermute | solution.py:49
  187.9 4.4 %collective-permute-start.26 = (bf16[128,2048]{1,0:T(8,128)(2,1)S(1)}, bf16[128,2048]{1,0:T(8,128)(2,1)S(1)}, u32[]{:S(2)}, u32[]{:S(2)}) collective-permute-start(bf16[128,2048]{1,0:T(8,128)(2,1)S(1)} %copy-done.5), channel_id=1, source_target_pairs={{0,64},{1,193},{16,80},{17,209},{32,96},{33,225},{48,112},{49,241}... | collective-permute-start | bytes 1572872 | tf_op jit(solution)/shard_map/ppermute | solution.py:49
  192.4 10.9 %collective-permute-done.26.refs_0_ = bf16[128,2048]{1,0:T(8,128)(2,1)S(1)} collective-permute-done((bf16[128,2048]{1,0:T(8,128)(2,1)S(1)}, bf16[128,2048]{1,0:T(8,128)(2,1)S(1)}, u32[]{:S(2)}, u32[]{:S(2)}) %collective-permute-start.26) | collective-permute-done | bytes 524320 | tf_op jit(solution)/shard_map/ppermute | solution.py:49
  205.0 4.1 %experts.7 = (bf16[64,2048]{1,0:T(8,128)(2,1)S(1)}, bf16[64,2048]{1,0:T(8,128)(2,1)S(1)}, bf16[64,2048]{1,0:T(8,128)(2,1)S(1)}, bf16[64,2048]{1,0:T(8,128)(2,1)S(1)}) custom-call(bf16[128,2048]{1,0:T(8,128)(2,1)S(1)} %collective-permute-done.26.refs_0_, bf16[128,2048]{1,0:T(8,128)(2,1)S(1)} %collective-permute-done.27.refs_1_, ...), custom_call_target="tpu_custom_call" | custom-call | flops 1610612736 | bytes 8388608 | tf_op jit(solution)/shard_map/experts/pallas_call | solution.py:265
  217.7 5.1 %collective-permute-done.30.refs_2_ = bf16[64,2048]{1,0:T(8,128)(2,1)S(1)} collective-permute-done((bf16[64,2048]{1,0:T(8,128)(2,1)S(1)}, bf16[64,2048]{1,0:T(8,128)(2,1)S(1)}, u32[]{:S(2)}, u32[]{:S(2)}) %collective-permute-start.30) | collective-permute-done | bytes 262176 | tf_op jit(solution)/shard_map/ppermute | solution.py:49
  224.3 4.8 %finish.1 = bf16[256,2048]{1,0:T(8,128)(2,1)} custom-call(f32[256,2048]{1,0:T(8,128)} %get-tuple-element.47.acc_ref, bf16[256,2048]{1,0:T(8,128)(2,1)S(1)} %collective-permute-done.25.more_ref, s32[256,2]{1,0:T(8,128)S(1)} %copy.52.place_ref, f32[256,2]{1,0:T(8,128)S(1)} %copy.53.weight_ref, bf16[64,2048]{1,0:T(8,128)(2,1)S(1)} %collective-permute-done.28.refs_0_, ...), custom_call_target="tpu_custom_call" | custom-call | flops 536870912 | bytes 6291456 | tf_op jit(solution)/shard_map/finish/pallas_call | solution.py:339
  (128 shorter events, 65.6 us)
Async XLA Ops:
  0.0 29.8 %collective-permute-start.1 = (bf16[64,2048]{1,0:T(8,128)(2,1)}, bf16[64,2048]{1,0:T(8,128)(2,1)S(1)}, u32[]{:S(2)}, u32[]{:S(2)}) collective-permute-start(bf16[64,2048]{1,0:T(8,128)(2,1)} %refs_0_.1), channel_id=1, source_target_pairs={{0,2},{2,4},{4,6},{6,8},{8,10},{10,12},{12,14},{14,0},{1,3},{3,5},... | collective-permute-start | bytes 786440 | tf_op jit(solution)/shard_map/ppermute | solution.py:49
  2.5 28.1 %collective-permute-start.2 = (bf16[64,2048]{1,0:T(8,128)(2,1)}, bf16[64,2048]{1,0:T(8,128)(2,1)S(1)}, u32[]{:S(2)}, u32[]{:S(2)}) collective-permute-start(bf16[64,2048]{1,0:T(8,128)(2,1)} %refs_0_.1), channel_id=1, source_target_pairs={{0,14},{2,0},{4,2},{6,4},{8,6},{10,8},{12,10},{14,12},{1,15},{3,1}... | collective-permute-start | bytes 786440 | tf_op jit(solution)/shard_map/ppermute | solution.py:49
  8.0 17.5 %collective-permute-start = (f32[65,2]{1,0:T(8,128)S(1)}, f32[65,2]{1,0:T(8,128)S(1)}, u32[]{:S(2)}, u32[]{:S(2)}) collective-permute-start(f32[65,2]{1,0:T(8,128)S(1)} %pad_maximum_fusion.1), channel_id=1, source_target_pairs={{0,16},{16,32},{32,48},{48,64},{64,80},{80,96},{96,112},{112,128},... | collective-permute-start | bytes 1568 | tf_op jit(solution)/shard_map/ppermute | solution.py:401
  11.2 92.3 %collective-permute-start.13 = (bf16[2048,512]{1,0:T(8,128)(2,1)}, bf16[2048,512]{1,0:T(8,128)(2,1)S(1)}, u32[]{:S(2)}, u32[]{:S(2)}) collective-permute-start(bf16[2048,512]{1,0:T(8,128)(2,1)} %bitcast.49), channel_id=1, source_target_pairs={{0,0},{1,161},{16,16},{17,177},{32,32},{33,129},{48,48},{49,145},{... | collective-permute-start | bytes 6291464 | tf_op jit(solution)/shard_map/ppermute | solution.py:49
  18.2 86.5 %collective-permute-start.14 = (bf16[2048,512]{1,0:T(8,128)(2,1)}, bf16[2048,512]{1,0:T(8,128)(2,1)}, u32[]{:S(2)}, u32[]{:S(2)}) collective-permute-start(bf16[2048,512]{1,0:T(8,128)(2,1)} %bitcast.50), channel_id=1, source_target_pairs={{0,0},{1,161},{16,16},{17,177},{32,32},{33,129},{48,48},{49,145},{... | collective-permute-start | bytes 6291464 | tf_op jit(solution)/shard_map/ppermute | solution.py:49
  36.3 18.1 %collective-permute-start.5 = (bf16[64,2048]{1,0:T(8,128)(2,1)S(1)}, bf16[64,2048]{1,0:T(8,128)(2,1)}, u32[]{:S(2)}, u32[]{:S(2)}) collective-permute-start(bf16[64,2048]{1,0:T(8,128)(2,1)S(1)} %collective-permute-done.3.refs_3_), channel_id=1, source_target_pairs={{0,2},{2,4},{4,6},{6,8},{8,10},{10,12},{12,14},{14,0},{1,3},{3,5},... | collective-permute-start | bytes 786440 | tf_op jit(solution)/shard_map/ppermute | solution.py:49
  38.8 48.8 %collective-permute-start.8 = (bf16[320,2048]{1,0:T(8,128)(2,1)}, bf16[320,2048]{1,0:T(8,128)(2,1)}, u32[]{:S(2)}, u32[]{:S(2)}) collective-permute-start(bf16[320,2048]{1,0:T(8,128)(2,1)} %constant_dynamic-update-slice_fusion), channel_id=1, source_target_pairs={{0,1},{1,0},{2,3},{3,2},{4,5},{5,4},{6,7},{7,6},{8,9},{9,8},{10,11... | collective-permute-start | bytes 3932168 | tf_op jit(solution)/shard_map/ppermute | solution.py:49
  54.4 16.4 %collective-permute-start.7 = (bf16[64,2048]{1,0:T(8,128)(2,1)}, bf16[64,2048]{1,0:T(8,128)(2,1)}, u32[]{:S(2)}, u32[]{:S(2)}) collective-permute-start(bf16[64,2048]{1,0:T(8,128)(2,1)} %collective-permute-done.5.refs_5_), channel_id=1, source_target_pairs={{0,2},{2,4},{4,6},{6,8},{8,10},{10,12},{12,14},{14,0},{1,3},{3,5},... | collective-permute-start | bytes 786440 | tf_op jit(solution)/shard_map/ppermute | solution.py:49
  55.0 32.6 %all-to-all-start = ((bf16[16,64,256]{2,1,0:T(8,128)(2,1)}), bf16[16,64,256]{2,1,0:T(8,128)(2,1)S(1)}, u32[]{:S(2)}, u32[]{:S(2)}) async-start(bf16[16,64,256]{2,1,0:T(8,128)(2,1)} %conv.1), calls=%async_computation | async-start | bytes 1048576 | tf_op jit(solution)/shard_map/all_to_all | solution.py:414
  63.7 44.1 %collective-permute-start.15 = (bf16[512,2048]{1,0:T(8,128)(2,1)}, bf16[512,2048]{1,0:T(8,128)(2,1)}, u32[]{:S(2)}, u32[]{:S(2)}) collective-permute-start(bf16[512,2048]{1,0:T(8,128)(2,1)} %bitcast.51), channel_id=1, source_target_pairs={{0,0},{1,161},{16,16},{17,177},{32,32},{33,129},{48,48},{49,145},{... | collective-permute-start | bytes 6291464 | tf_op jit(solution)/shard_map/ppermute | solution.py:49
  72.8 14.8 %collective-permute-start.9 = (bf16[192,2048]{1,0:T(8,128)(2,1)}, bf16[192,2048]{1,0:T(8,128)(2,1)}, u32[]{:S(2)}, u32[]{:S(2)}) collective-permute-start(bf16[192,2048]{1,0:T(8,128)(2,1)} %pad_maximum_fusion), channel_id=1, source_target_pairs={{0,1},{1,0},{2,3},{3,2},{4,5},{5,4},{6,7},{7,6},{8,9},{9,8},{10,11... | collective-permute-start | bytes 2359304 | tf_op jit(solution)/shard_map/ppermute | solution.py:49
  100.9 13.1 %collective-permute-start.21 = (bf16[128,2048]{1,0:T(8,128)(2,1)S(1)}, bf16[128,2048]{1,0:T(8,128)(2,1)S(1)}, u32[]{:S(2)}, u32[]{:S(2)}) collective-permute-start(bf16[128,2048]{1,0:T(8,128)(2,1)S(1)} %get-tuple-element.43), channel_id=1, source_target_pairs={{0,16},{1,49},{16,32},{17,1},{32,48},{33,17},{48,0},{49,33},{64,80... | collective-permute-start | bytes 1572872 | tf_op jit(solution)/shard_map/ppermute | solution.py:49
  103.4 16.0 %collective-permute-start.22 = (bf16[128,2048]{1,0:T(8,128)(2,1)S(1)}, bf16[128,2048]{1,0:T(8,128)(2,1)S(1)}, u32[]{:S(2)}, u32[]{:S(2)}) collective-permute-start(bf16[128,2048]{1,0:T(8,128)(2,1)S(1)} %get-tuple-element.44), channel_id=1, source_target_pairs={{0,48},{1,17},{16,0},{17,33},{32,16},{33,49},{48,32},{49,1},{64,11... | collective-permute-start | bytes 1572872 | tf_op jit(solution)/shard_map/ppermute | solution.py:49
  103.4 36.7 %collective-permute-start.17 = (bf16[128,2048]{1,0:T(8,128)(2,1)S(1)}, bf16[128,2048]{1,0:T(8,128)(2,1)S(1)}, u32[]{:S(2)}, u32[]{:S(2)}) collective-permute-start(bf16[128,2048]{1,0:T(8,128)(2,1)S(1)} %get-tuple-element.39), channel_id=1, source_target_pairs={{0,112},{1,81},{16,64},{17,97},{32,80},{33,113},{48,96},{49,65},{6... | collective-permute-start | bytes 1572872 | tf_op jit(solution)/shard_map/ppermute | solution.py:49
  104.7 35.5 %collective-permute-start.18 = (bf16[128,2048]{1,0:T(8,128)(2,1)S(1)}, bf16[128,2048]{1,0:T(8,128)(2,1)S(1)}, u32[]{:S(2)}, u32[]{:S(2)}) collective-permute-start(bf16[128,2048]{1,0:T(8,128)(2,1)S(1)} %get-tuple-element.40), channel_id=1, source_target_pairs={{0,32},{1,113},{16,48},{17,65},{32,0},{33,81},{48,16},{49,97},{64,... | collective-permute-start | bytes 1572872 | tf_op jit(solution)/shard_map/ppermute | solution.py:49
  107.9 41.8 %collective-permute-start.12 = (bf16[128,2048]{1,0:T(8,128)(2,1)S(1)}, bf16[128,2048]{1,0:T(8,128)(2,1)S(1)}, u32[]{:S(2)}, u32[]{:S(2)}) collective-permute-start(bf16[128,2048]{1,0:T(8,128)(2,1)S(1)} %get-tuple-element.36), channel_id=1, source_target_pairs={{0,80},{1,33},{16,96},{17,49},{32,112},{33,1},{48,64},{49,17},{64,... | collective-permute-start | bytes 1572872 | tf_op jit(solution)/shard_map/ppermute | solution.py:49
  124.5 31.4 %collective-permute-start.23 = (bf16[128,2048]{1,0:T(8,128)(2,1)}, bf16[128,2048]{1,0:T(8,128)(2,1)}, u32[]{:S(2)}, u32[]{:S(2)}) collective-permute-start(bf16[128,2048]{1,0:T(8,128)(2,1)} %get-tuple-element.45), channel_id=1, source_target_pairs={{0,48},{1,17},{16,0},{17,33},{32,16},{33,49},{48,32},{49,1},{64,11... | collective-permute-start | bytes 1572872 | tf_op jit(solution)/shard_map/ppermute | solution.py:49
  124.5 31.4 %collective-permute-start.24 = (bf16[128,2048]{1,0:T(8,128)(2,1)}, bf16[128,2048]{1,0:T(8,128)(2,1)}, u32[]{:S(2)}, u32[]{:S(2)}) collective-permute-start(bf16[128,2048]{1,0:T(8,128)(2,1)} %get-tuple-element.46), channel_id=1, source_target_pairs={{0,16},{1,49},{16,32},{17,1},{32,48},{33,17},{48,0},{49,33},{64,80... | collective-permute-start | bytes 1572872 | tf_op jit(solution)/shard_map/ppermute | solution.py:49
  145.3 21.8 %collective-permute-start.19 = (bf16[128,2048]{1,0:T(8,128)(2,1)}, bf16[128,2048]{1,0:T(8,128)(2,1)}, u32[]{:S(2)}, u32[]{:S(2)}) collective-permute-start(bf16[128,2048]{1,0:T(8,128)(2,1)} %get-tuple-element.41), channel_id=1, source_target_pairs={{0,208},{1,241},{16,224},{17,193},{32,240},{33,209},{48,192},{49,2... | collective-permute-start | bytes 1572872 | tf_op jit(solution)/shard_map/ppermute | solution.py:49
  145.3 21.8 %collective-permute-start.20 = (bf16[128,2048]{1,0:T(8,128)(2,1)}, bf16[128,2048]{1,0:T(8,128)(2,1)}, u32[]{:S(2)}, u32[]{:S(2)}) collective-permute-start(bf16[128,2048]{1,0:T(8,128)(2,1)} %get-tuple-element.42), channel_id=1, source_target_pairs={{0,32},{1,209},{16,48},{17,225},{32,0},{33,241},{48,16},{49,193},{... | collective-permute-start | bytes 1572872 | tf_op jit(solution)/shard_map/ppermute | solution.py:49
  155.3 20.8 %collective-permute-start.16 = (bf16[128,2048]{1,0:T(8,128)(2,1)}, bf16[128,2048]{1,0:T(8,128)(2,1)}, u32[]{:S(2)}, u32[]{:S(2)}) collective-permute-start(bf16[128,2048]{1,0:T(8,128)(2,1)} %get-tuple-element.38), channel_id=1, source_target_pairs={{0,240},{1,33},{16,192},{17,49},{32,208},{33,1},{48,224},{49,17},{... | collective-permute-start | bytes 1572872 | tf_op jit(solution)/shard_map/ppermute | solution.py:49
  183.1 41.2 %collective-permute-start.25 = (bf16[256,2048]{1,0:T(8,128)(2,1)S(1)}, bf16[256,2048]{1,0:T(8,128)(2,1)S(1)}, u32[]{:S(2)}, u32[]{:S(2)}) collective-permute-start(bf16[256,2048]{1,0:T(8,128)(2,1)S(1)} %get-tuple-element.48), channel_id=1, source_target_pairs={{0,1},{1,0},{2,3},{3,2},{4,5},{5,4},{6,7},{7,6},{8,9},{9,8},{10,11... | collective-permute-start | bytes 3145736 | tf_op jit(solution)/shard_map/ppermute | solution.py:49
  187.9 15.3 %collective-permute-start.26 = (bf16[128,2048]{1,0:T(8,128)(2,1)S(1)}, bf16[128,2048]{1,0:T(8,128)(2,1)S(1)}, u32[]{:S(2)}, u32[]{:S(2)}) collective-permute-start(bf16[128,2048]{1,0:T(8,128)(2,1)S(1)} %copy-done.5), channel_id=1, source_target_pairs={{0,64},{1,193},{16,80},{17,209},{32,96},{33,225},{48,112},{49,241}... | collective-permute-start | bytes 1572872 | tf_op jit(solution)/shard_map/ppermute | solution.py:49
  192.3 12.7 %collective-permute-start.27 = (bf16[128,2048]{1,0:T(8,128)(2,1)S(1)}, bf16[128,2048]{1,0:T(8,128)(2,1)S(1)}, u32[]{:S(2)}, u32[]{:S(2)}) collective-permute-start(bf16[128,2048]{1,0:T(8,128)(2,1)S(1)} %get-tuple-element.50), channel_id=1, source_target_pairs={{0,192},{1,65},{16,208},{17,81},{32,224},{33,97},{48,240},{49,113}... | collective-permute-start | bytes 1572872 | tf_op jit(solution)/shard_map/ppermute | solution.py:49
  (27 other events, 271.9 us)

commit v3 on v2

v3 whole, which is shorter than its diff:
```python
import functools

import jax
import jax.numpy as jnp
import numpy as np
from jax import lax
from jax.experimental import pallas as pl
from jax.experimental.pallas import tpu as pltpu
from jax.sharding import Mesh
from jax.sharding import PartitionSpec as P


HEAD = 64
EPS = 1e-06
ROWS = 256
HALF = 128
SLOT = 32
CHUNK = 64
WIDTH = 2048
FF = 512
TILE = 512
SP = ("y", "x")
TP = ("z", "c")
CHIP = ("y", "x", "c")

PAIRS = (
    ((0, 1), (0, 3)),
    ((1, 0), (3, 0)),
    ((0, 3), (0, 1)),
    ((3, 0), (1, 0)),
    ((1, 1), (0, 2)),
    ((1, 3), (1, 1)),
    ((0, 2), (1, 3)),
    ((0, 0), (0, 0)),
)
LOCAL = 7
EXPERTS_AT = np.array([[a, (b[0] + 2, b[1] + 2)] for a, b in PAIRS], np.int32) % 4
assert len({tuple(d) for pair in EXPERTS_AT.tolist() for d in pair}) == 16
GROUPS = ((0, 1, 2, 3), (4, 7), (5, 6))

VMEM = pl.BlockSpec(memory_space=pltpu.VMEM)
SMEM = pl.BlockSpec(memory_space=pltpu.SMEM)


def permute(value, axes, sizes, move):
    pairs = []
    for i in np.ndindex(*sizes):
        j = tuple(int(v) for v in np.mod(move(*i), sizes))
        pairs.append((int(np.ravel_multi_index(i, sizes)), int(np.ravel_multi_index(j, sizes))))
    return lax.ppermute(value, axes, pairs)


def displaced(value, op, sign, cross=0):
    def move(y, x, c):
        dy, dx = PAIRS[op][c]
        return (y + sign * dy, x + sign * dx, c + cross)

    if op == LOCAL and not cross:
        return value
    return permute(value, CHIP, (4, 4, 2), move)


def hosted(value):
    return permute(value, CHIP, (4, 4, 2), lambda y, x, c: (y - 2 * c, x - 2 * c, c))


def along_z(value, step):
    return permute(value, "z", (8,), lambda z: (z + step,))


def swap_cores(value):
    return permute(value, "c", (2,), lambda c: (c + 1,))


def in_hbm(value):
    return pltpu.with_memory_space_constraint(value, pltpu.HBM)


def cost(flops, nbytes):
    return pl.CostEstimate(flops=int(flops), bytes_accessed=int(nbytes), transcendentals=0)


def params(mib, grid=False):
    kwargs = {"dimension_semantics": ("arbitrary",)} if grid else {}
    return pltpu.CompilerParams(vmem_limit_bytes=mib << 20, **kwargs)


def tail_kernel(a_ref, b_ref, doc_ref, out_ref):
    out_ref[:HEAD] = a_ref[...].astype(jnp.float32) * b_ref[...].astype(jnp.float32)
    out_ref[HEAD:] = jnp.broadcast_to(doc_ref[...].astype(jnp.float32), (8, 128))


def tail(conv_in, in_gate, docs):
    at = conv_in.shape[1] // 128 - 1
    wide = pl.BlockSpec((HEAD, 128), lambda i: (0, at))
    return pl.pallas_call(
        tail_kernel,
        grid=(1,),
        out_shape=jax.ShapeDtypeStruct((HEAD + 8, 128), jnp.float32),
        in_specs=[wide, wide, pl.BlockSpec((1, 128), lambda i: (0, at))],
        out_specs=pl.BlockSpec((HEAD + 8, 128), lambda i: (0, 0)),
        compiler_params=params(2, True),
        cost_estimate=cost(1e4, 1e5),
        name="tail",
    )(in_hbm(conv_in), in_hbm(in_gate), docs)


def conv_kernel(a_ref, b_ref, o_ref, doc_ref, halo_ref, small_ref, out_ref, prev):
    @pl.when(pl.program_id(0) == 0)
    def _():
        prev[:, :128] = halo_ref[...]
        prev[:, 128:] = halo_ref[...]

    lane = lax.broadcasted_iota(jnp.int32, (HEAD, ROWS), 1)
    small = small_ref[...].T
    t0, t1, t2, gain = (small[:HEAD, k : k + 1] for k in range(4))
    g, d = prev[:HEAD], prev[HEAD:]
    p1, p2 = pltpu.roll(g, 1, 1), pltpu.roll(g, 2, 1)
    d1, d2 = pltpu.roll(d, 1, 1), pltpu.roll(d, 2, 1)
    for t in range(4):
        at = slice(t * ROWS, (t + 1) * ROWS)
        g = a_ref[:, at].astype(jnp.float32) * b_ref[:, at].astype(jnp.float32)
        d = jnp.broadcast_to(doc_ref[:, at].astype(jnp.float32), (8, ROWS))
        r1, r2 = pltpu.roll(g, 1, 1), pltpu.roll(g, 2, 1)
        e1, e2 = pltpu.roll(d, 1, 1), pltpu.roll(d, 2, 1)
        m1 = jnp.where(jnp.where(lane[:8] < 1, d1, e1) == d, 1.0, 0.0)[0:1]
        m2 = jnp.where(jnp.where(lane[:8] < 2, d2, e2) == d, 1.0, 0.0)[0:1]
        g1 = jnp.where(lane < 1, p1, r1)
        g2 = jnp.where(lane < 2, p2, r2)
        conv = t2 * g + t1 * (g1 * m1) + t0 * (g2 * m2)
        v = o_ref[:, at].astype(jnp.float32) * conv
        ms = jnp.sum(v * v, axis=0, keepdims=True) * (1.0 / HEAD)
        out_ref[t] = (v * lax.rsqrt(ms + EPS) * gain).astype(jnp.bfloat16)
        p1, p2, d1, d2 = r1, r2, e1, e2
    prev[:HEAD] = g
    prev[HEAD:] = d


def conv(conv_in, in_gate, out_gate, docs, halo, small):
    wide = pl.BlockSpec((HEAD, 4 * ROWS), lambda i: (0, i))

    def whole(a):
        return pl.BlockSpec(a.shape, lambda i: (0, 0))

    return pl.pallas_call(
        conv_kernel,
        grid=(4,),
        out_shape=jax.ShapeDtypeStruct((16, HEAD, ROWS), jnp.bfloat16),
        in_specs=[wide] * 3
        + [pl.BlockSpec((1, 4 * ROWS), lambda i: (0, i)), whole(halo), whole(small)],
        out_specs=pl.BlockSpec((4, HEAD, ROWS), lambda i: (i, 0, 0)),
        scratch_shapes=[pltpu.VMEM((HEAD + 8, ROWS), jnp.float32)],
        compiler_params=params(4, True),
        cost_estimate=cost(2e8, 2 << 20),
        name="conv",
    )(in_hbm(conv_in), in_hbm(in_gate), in_hbm(out_gate), docs, halo, small)


def route_kernel(where_ref, mine_ref, other_ref, rows_ref, weights_ref, rows2_ref, weights2_ref):
    y, x, c = where_ref[0], where_ref[1], where_ref[3]
    n = len(PAIRS)
    lane = lax.broadcasted_iota(jnp.int32, (ROWS, ROWS), 1)
    line = lax.broadcasted_iota(jnp.int32, (ROWS, ROWS), 0)
    same = (line < HALF) == (lane < HALF)
    earlier = jnp.where((line < lane) & same, 1.0, 0.0).astype(jnp.bfloat16)
    base = jnp.where(lane[:1] < HALF, 0, SLOT)

    def places(route, sets, rows_out, weights_out):
        count = n * len(sets)
        line = lax.broadcasted_iota(jnp.int32, (count, ROWS), 0)
        number = jnp.zeros((count, ROWS), jnp.int32)
        for s, core in enumerate(sets):
            for k in range(n):
                dy = jnp.where(core == 0, int(EXPERTS_AT[k, 0, 0]), int(EXPERTS_AT[k, 1, 0]))
                dx = jnp.where(core == 0, int(EXPERTS_AT[k, 0, 1]), int(EXPERTS_AT[k, 1, 1]))
                e = lax.rem(y + dy, 4) * 4 + lax.rem(x + dx, 4)
                number = jnp.where(line == s * n + k, e, number)
        number = number.astype(jnp.float32)
        at0, at1 = number == route[0:1], number == route[1:2]
        named = jnp.where(at0 | at1, 1.0, 0.0)
        rank = jnp.dot(named.astype(jnp.bfloat16), earlier, preferred_element_type=jnp.float32)
        rows_out[...] = jnp.where(named > 0.0, rank.astype(jnp.int32) + base, -1)
        weights_out[...] = jnp.where(at0, route[2:3], 0.0) + jnp.where(at1, route[3:4], 0.0)

    places(mine_ref[...], (c, 1 - c), rows_ref, weights_ref)
    places(other_ref[...], (c,), rows2_ref, weights2_ref)


def route(where, mine, other):
    n = len(PAIRS)
    return pl.pallas_call(
        route_kernel,
        out_shape=[
            jax.ShapeDtypeStruct((count, ROWS), dtype)
            for count in (2 * n, n)
            for dtype in (jnp.int32, jnp.float32)
        ],
        in_specs=[SMEM, VMEM, VMEM],
        out_specs=[VMEM] * 4,
        compiler_params=params(2),
        cost_estimate=cost(1e7, 1e5),
        name="route",
    )(where, mine, other)


OFFSETS = (0, -1, 1, -2, 2, -3, 3, -4)


def mix_kernel(where_ref, by_row_ref, *refs):
    n_own = len(OFFSETS)
    own = refs[:n_own]
    swapped = refs[n_own : 2 * n_own]
    resid_ref, gain_ref, stream_ref, normed_ref, lhs, rhs, kept, total = refs[2 * n_own :]
    z, c = where_ref[2], where_ref[3]
    step = pl.program_id(0)

    @pl.when(step == 0)
    def _():
        for q, off in enumerate(OFFSETS):
            zz = lax.rem(z + (off + 8), 8)
            lhs[pl.ds(q * 64, 64), :] = by_row_ref[zz * 2 + c]
            lhs[pl.ds(512 + q * 64, 64), :] = by_row_ref[zz * 2 + 1 - c]
        total[...] = jnp.zeros_like(total)

    row = 0
    for ref in (*own, *swapped):
        rhs[pl.ds(row, ref.shape[0]), :] = ref[...]
        row += ref.shape[0]
    mixed = lax.dot_general(
        lhs[...], rhs[...], (((0,), (0,)), ((), ())), preferred_element_type=jnp.float32
    )
    stream = resid_ref[...].astype(jnp.float32) + mixed
    stream_ref[...] = stream
    kept[step] = stream
    total[...] += jnp.broadcast_to(jnp.sum(stream * stream, axis=1, keepdims=True), total.shape)

    @pl.when(step == WIDTH // TILE - 1)
    def _():
        scale = lax.rsqrt(total[:, 0:1] * (1.0 / WIDTH) + EPS)
        for n in range(WIDTH // TILE):
            at = slice(n * TILE, (n + 1) * TILE)
            normed_ref[:, at] = (kept[n] * scale * gain_ref[:, at]).astype(jnp.bfloat16)


def mix(where, by_row, own, swapped, resid, gain):
    def tall(a):
        return pl.BlockSpec((a.shape[0], TILE), lambda i: (0, i))

    return pl.pallas_call(
        mix_kernel,
        grid=(WIDTH // TILE,),
        out_shape=[
            pltpu.HBM((ROWS, WIDTH), jnp.float32),
            jax.ShapeDtypeStruct((ROWS, WIDTH), jnp.bfloat16),
        ],
        in_specs=[SMEM, pl.BlockSpec(by_row.shape, lambda i: (0, 0, 0))]
        + [tall(a) for a in (*own, *swapped, resid)]
        + [pl.BlockSpec(gain.shape, lambda i: (0, 0))],
        out_specs=[
            pl.BlockSpec((ROWS, TILE), lambda i: (0, i)),
            pl.BlockSpec((ROWS, WIDTH), lambda i: (0, 0)),
        ],
        scratch_shapes=[
            pltpu.VMEM((1024, ROWS), jnp.bfloat16),
            pltpu.VMEM((1024, TILE), jnp.bfloat16),
            pltpu.VMEM((WIDTH // TILE, ROWS, TILE), jnp.float32),
            pltpu.VMEM((ROWS, 128), jnp.float32),
        ],
        compiler_params=params(16, True),
        cost_estimate=cost(1.1e9, 8 << 20),
        name="mix",
    )(where, by_row, *own, *swapped, in_hbm(resid), gain)


def pack_kernel(mine_ref, theirs_ref, mine_at_ref, theirs_at_ref, *refs):
    outs, table = refs[: len(PAIRS)], refs[len(PAIRS)]

    @pl.when(pl.program_id(0) == 0)
    def _():
        slot = lax.broadcasted_iota(jnp.int32, (CHUNK, ROWS), 0)
        for half, ref in enumerate((mine_at_ref, theirs_at_ref)):
            for k in range(len(PAIRS)):
                hit = slot == ref[k : k + 1, :]
                table[half, pl.ds(k * CHUNK, CHUNK), :] = jnp.where(hit, 1.0, 0.0).astype(
                    jnp.bfloat16
                )

    for half, ref in enumerate((mine_ref, theirs_ref)):
        packed = jnp.dot(table[half], ref[...], preferred_element_type=jnp.float32)
        packed = packed.astype(jnp.bfloat16)
        for k, out in enumerate(outs):
            out[pl.ds(half * CHUNK, CHUNK), :] = packed[k * CHUNK : (k + 1) * CHUNK]


def pack(mine, theirs, mine_at, theirs_at):
    block = pl.BlockSpec((ROWS, TILE), lambda i: (0, i))
    at = pl.BlockSpec(mine_at.shape, lambda i: (0, 0))
    n = len(PAIRS)
    return pl.pallas_call(
        pack_kernel,
        grid=(WIDTH // TILE,),
        out_shape=[jax.ShapeDtypeStruct((2 * CHUNK, WIDTH), jnp.bfloat16)] * n,
        in_specs=[block, block, at, at],
        out_specs=[pl.BlockSpec((2 * CHUNK, TILE), lambda i: (0, i))] * n,
        scratch_shapes=[pltpu.VMEM((2, n * CHUNK, ROWS), jnp.bfloat16)],
        compiler_params=params(12, True),
        cost_estimate=cost(1.1e9, 6 << 20),
        name="pack",
    )(mine, theirs, mine_at, theirs_at)


def expert_kernel(n, *refs):
    bufs, (wg, wu, wd) = refs[:n], refs[n : n + 3]
    outs, rows = refs[n + 3 : -1], refs[-1]
    row = 0
    for ref in bufs:
        rows[pl.ds(row, ref.shape[0]), :] = ref[...]
        row += ref.shape[0]
    x = rows[...]
    g = jnp.dot(x, wg[...], preferred_element_type=jnp.float32)
    u = jnp.dot(x, wu[...], preferred_element_type=jnp.float32)
    h = (g / (1.0 + jnp.exp(-g)) * u).astype(jnp.bfloat16)
    for n0 in range(0, WIDTH, TILE):
        at = slice(n0, n0 + TILE)
        y = jnp.dot(h, wd[:, at], preferred_element_type=jnp.float32).astype(jnp.bfloat16)
        row = 0
        for ref in outs:
            ref[:, at] = y[row : row + ref.shape[0]]
            row += ref.shape[0]


def experts(bufs, wg, wu, wd, apart):
    rows = sum(b.shape[0] for b in bufs)
    size = CHUNK if apart else 2 * CHUNK
    n_out = rows // size
    return pl.pallas_call(
        functools.partial(expert_kernel, len(bufs)),
        out_shape=[jax.ShapeDtypeStruct((size, WIDTH), jnp.bfloat16)] * n_out,
        in_specs=[VMEM] * (len(bufs) + 3),
        out_specs=[VMEM] * n_out,
        scratch_shapes=[pltpu.VMEM((rows, WIDTH), jnp.bfloat16)],
        compiler_params=params(24),
        cost_estimate=cost(6.0 * rows * WIDTH * FF, 8 << 20),
        name="experts",
    )(*bufs, wg, wu, wd)


def tables(rows_ref, weights_ref, chunks, high, low):
    slot = lax.broadcasted_iota(jnp.int32, (CHUNK, ROWS), 0)
    for i, k in enumerate(chunks):
        table = jnp.where(slot == rows_ref[k : k + 1, :], weights_ref[k : k + 1, :], 0.0)
        top = table.astype(jnp.bfloat16)
        high[pl.ds(i * CHUNK, CHUNK), :] = top
        low[pl.ds(i * CHUNK, CHUNK), :] = (table - top.astype(jnp.float32)).astype(jnp.bfloat16)


def apply(high, low, rows):
    numbers = (((0,), (0,)), ((), ()))
    return sum(
        lax.dot_general(t[...], rows[...], numbers, preferred_element_type=jnp.float32)
        for t in (high, low)
    )


def gather_kernel(chunks, acc_ref, rows_ref, weights_ref, rows2_ref, weights2_ref, *refs):
    n = len(chunks)
    bufs = refs[:n]
    mine_ref, theirs_ref, mine, theirs, high, low, high2, low2 = refs[n:]

    @pl.when(pl.program_id(0) == 0)
    def _():
        tables(rows_ref, weights_ref, chunks, high, low)
        tables(rows2_ref, weights2_ref, chunks, high2, low2)

    for i, ref in enumerate(bufs):
        mine[pl.ds(i * CHUNK, CHUNK), :] = ref[:CHUNK]
        theirs[pl.ds(i * CHUNK, CHUNK), :] = ref[CHUNK:]
    mine_ref[...] = acc_ref[...] + apply(high, low, mine)
    theirs_ref[...] = apply(high2, low2, theirs).astype(jnp.bfloat16)


def gather(chunks, acc, rows, weights, rows2, weights2, bufs):
    n = len(chunks)
    block = pl.BlockSpec((ROWS, TILE), lambda i: (0, i))

    def whole(a):
        return pl.BlockSpec(a.shape, lambda i: (0, 0))

    return pl.pallas_call(
        functools.partial(gather_kernel, chunks),
        grid=(WIDTH // TILE,),
        out_shape=[
            pltpu.HBM((ROWS, WIDTH), jnp.float32),
            jax.ShapeDtypeStruct((ROWS, WIDTH), jnp.bfloat16),
        ],
        in_specs=[block]
        + [whole(a) for a in (rows, weights, rows2, weights2)]
        + [pl.BlockSpec((2 * CHUNK, TILE), lambda i: (0, i))] * n,
        out_specs=[block, block],
        scratch_shapes=[pltpu.VMEM((n * CHUNK, TILE), jnp.bfloat16)] * 2
        + [pltpu.VMEM((n * CHUNK, ROWS), jnp.bfloat16)] * 4,
        compiler_params=params(14, True),
        cost_estimate=cost(8.0 * ROWS * n * CHUNK * WIDTH, 10 << 20),
        name="gather",
    )(in_hbm(acc), rows, weights, rows2, weights2, *bufs)


def finish_kernel(chunks, acc_ref, more_ref, rows_ref, weights_ref, *refs):
    n = len(chunks)
    bufs = refs[:n]
    out_ref, rows, high, low = refs[n:]

    @pl.when(pl.program_id(0) == 0)
    def _():
        tables(rows_ref, weights_ref, chunks, high, low)

    for i, ref in enumerate(bufs):
        rows[pl.ds(i * CHUNK, CHUNK), :] = ref[...]
    total = acc_ref[...] + more_ref[...].astype(jnp.float32) + apply(high, low, rows)
    out_ref[...] = total.astype(out_ref.dtype)


def finish(chunks, acc, more, rows, weights, bufs):
    n = len(chunks)
    block = pl.BlockSpec((ROWS, TILE), lambda i: (0, i))

    def whole(a):
        return pl.BlockSpec(a.shape, lambda i: (0, 0))

    return pl.pallas_call(
        functools.partial(finish_kernel, chunks),
        grid=(WIDTH // TILE,),
        out_shape=jax.ShapeDtypeStruct((ROWS, WIDTH), jnp.bfloat16),
        in_specs=[block, block, whole(rows), whole(weights)]
        + [pl.BlockSpec((CHUNK, TILE), lambda i: (0, i))] * n,
        out_specs=block,
        scratch_shapes=[pltpu.VMEM((n * CHUNK, TILE), jnp.bfloat16)]
        + [pltpu.VMEM((n * CHUNK, ROWS), jnp.bfloat16)] * 2,
        compiler_params=params(12, True),
        cost_estimate=cost(4.0 * ROWS * n * CHUNK * WIDTH, 6 << 20),
        name="finish",
    )(in_hbm(acc), more, rows, weights, *bufs)


def body(
    conv_in,
    in_gate,
    out_gate,
    doc_ids,
    conv_taps,
    head_gain,
    out_proj,
    resid,
    norm_gain,
    route_ids,
    route_weight,
    w_gate,
    w_up,
    w_down,
):
    y, x, z, c = (lax.axis_index(a) for a in ("y", "x", "z", "c"))

    wg = hosted(w_gate[0])
    wu = hosted(w_up[0])
    wd = hosted(w_down[0])

    plus, minus = [out_proj], [out_proj]
    plus.append(along_z(out_proj, 1))
    minus.append(along_z(out_proj, -1))

    docs = doc_ids[None]
    last = tail(conv_in, in_gate, docs)
    halo = lax.ppermute(last, SP, [(i, i + 1) for i in range(15)])
    small = jnp.pad(jnp.concatenate([conv_taps.T, head_gain[None]]), ((0, 4), (0, 128 - HEAD)))
    head_normed = conv(conv_in, in_gate, out_gate, docs, halo, small)
    by_row = lax.all_to_all(head_normed, TP, split_axis=0, concat_axis=0, tiled=True)

    for _ in range(2, 5):
        plus.append(along_z(plus[-1], 1))
    for _ in range(2, 4):
        minus.append(along_z(minus[-1], -1))
    own = [out_proj, plus[1], minus[1], plus[2], minus[2], plus[3], minus[3], plus[4]]
    swapped = [swap_cores(w) for w in own]

    where = jnp.stack([y, x, z, c]).astype(jnp.int32)
    routes = jnp.concatenate([route_ids.astype(jnp.float32), route_weight], axis=1).T
    routes_other = swap_cores(routes)
    rows, weights, rows_other, weights_other = route(where, routes, routes_other)

    stream, normed = mix(where, by_row, own, swapped, resid, norm_gain[None])
    normed_other = swap_cores(normed)
    sends = pack(normed, normed_other, rows[: len(PAIRS)], rows_other)
    arrived = [displaced(s, k, 1) for k, s in enumerate(sends)]

    back, cross = {}, {}
    for n, group in enumerate(GROUPS):
        apart = n > 0
        inputs = [arrived[k] for k in group]
        results = experts(inputs, wg, wu, wd, apart)
        for i, k in enumerate(group):
            if apart:
                back[k] = displaced(results[2 * i], k, -1)
                cross[k] = displaced(results[2 * i + 1], k, -1, 1)
            else:
                back[k] = displaced(results[i], k, -1)
    near = GROUPS[0]
    far = [k for group in GROUPS[1:] for k in group]
    total, partial = gather(
        near, stream, rows, weights, rows_other, weights_other, [back[k] for k in near]
    )
    more = swap_cores(partial)
    chunks = tuple(far) + tuple(len(PAIRS) + k for k in far)
    return finish(
        chunks, total, more, rows, weights, [back[k] for k in far] + [cross[k] for k in far]
    )


def solution(mesh):
    finer = Mesh(mesh.devices.reshape(4, 4, 8, 2), ("y", "x", "z", "c"))
    every = SP + TP
    return jax.shard_map(
        body,
        mesh=finer,
        in_specs=(
            P(TP, SP),
            P(TP, SP),
            P(TP, SP),
            P(SP),
            P(TP, None),
            P(TP),
            P(TP, None),
            P(every, None),
            P(),
            P(every, None),
            P(every, None),
            P(SP, None, None),
            P(SP, None, None),
            P(SP, None, None),
        ),
        out_specs=P(every, None),
        check_vma=False,
    )
```

time: 232 us -> 212 us (0.914)
  waiting for transfers between devices: 70.5 us -> 42.8 us
  starting transfers between devices: 93.6 us -> 119 us
  other arithmetic: 7.88 us -> 0.8 us
  Pallas kernels: 42.1 us -> 36.7 us
  matrix products: 2.5 us -> 0 us
  local copies, waits for them, and re-layouts: 12.2 us -> 9.79 us
    ppermute x31 -> x39, starting transfers between devices: 81.7 us -> 111 us  [permute(): return lax.ppermute(value, axes, pairs)]
    ppermute x31 -> x39, waiting for transfers between devices: 70.5 us -> 42.8 us  [permute(): return lax.ppermute(value, axes, pairs)]
    pallas_call x4 -> x3, Pallas kernels: 19.2 us -> 13.9 us  [experts(): pl.pallas_call(functools.partial(expert_kernel, len(bufs)), out_shape=[ja...]
    all_to_all x1, starting transfers between devices: 8.76 us -> 4.75 us  [body(): lax.all_to_all(head_normed, TP, split_axis=0, concat_axis=0, tiled=True)]
    dot_general x2 -> x0, matrix products: 2.5 us -> none  [places(): jnp.dot(named.astype(jnp.bfloat16), jnp.asarray(earlier, jnp.bfloat16), p...]
    unnamed x42 -> x32, local copies, waits for them, and re-layouts: 8.48 us -> 9.79 us
    pallas_call x2 -> x4, Pallas kernels: 10.8 us -> 10.7 us  [the longest x1 4.64 us: gather(): pl.pallas_call(functools.partial(gather_kernel, chunks), grid=(WIDTH // T...]
  transfers between devices with their start and end apart: 33 -> 41, of which waited for: 13 -> 13; matrix products, arithmetic and copies ran while one was open for 8% -> 0% of each run, Pallas kernels for 14% -> 13%
where the time goes in v3:
time: 212 us; the launch traced here: 209 us
  starting transfers between devices  119 us (56%)
  waiting for transfers between devices  42.8 us (20%)
  Pallas kernels  36.7 us (17%)
  local copies, waits for them, and re-layouts  9.79 us (5%)
    ppermute x39, starting transfers between devices, permute(): return lax.ppermute(value, axes, pairs)  111 us
    ppermute x39, waiting for transfers between devices, permute(): return lax.ppermute(value, axes, pairs)  42.8 us
    pallas_call x3, Pallas kernels, experts(): pl.pallas_call(functools.partial(expert_kernel, len(bufs)), out_shape=[ja...  13.9 us
    unnamed x32, local copies, waits for them, and re-layouts  9.79 us
    pallas_call x1, Pallas kernels, mix(): pl.pallas_call(mix_kernel, grid=(WIDTH // TILE,), out_shape=[pltpu.HBM((R...  5.57 us
    all_to_all x1, starting transfers between devices, body(): lax.all_to_all(head_normed, TP, split_axis=0, concat_axis=0, tiled=True)  4.75 us
    pallas_call x1, Pallas kernels, gather(): pl.pallas_call(functools.partial(gather_kernel, chunks), grid=(WIDTH // T...  4.64 us
    pallas_call x1, Pallas kernels, finish(): pl.pallas_call(functools.partial(finish_kernel, chunks), grid=(WIDTH // T...  4.56 us
  transfers between devices with their start and end apart: 41, of which 13 were waited for; matrix products, arithmetic and copies ran while one was open for 0% of the time, Pallas kernels for 13%

profile of v3, /device:TPU:1, one launch (start us, length us, event | category | flops | bytes accessed | tf_op | source)
XLA Modules:
  0.0 208.8 jit_solution(4381638223490704760)
XLA Ops:
  0.0 6.4 %collective-permute-start.2 = (bf16[64,2048]{1,0:T(8,128)(2,1)}, bf16[64,2048]{1,0:T(8,128)(2,1)S(1)}, u32[]{:S(2)}, u32[]{:S(2)}) collective-permute-start(bf16[64,2048]{1,0:T(8,128)(2,1)} %refs_0_.1), channel_id=1, source_target_pairs={{0,14},{2,0},{4,2},{6,4},{8,6},{10,8},{12,10},{14,12},{1,15},{3,1}... | collective-permute-start | bytes 786440 | tf_op jit(solution)/shard_map/ppermute | solution.py:50
  13.2 3.3 %collective-permute-start.4 = (bf16[64,2048]{1,0:T(8,128)(2,1)S(1)}, bf16[64,2048]{1,0:T(8,128)(2,1)}, u32[]{:S(2)}, u32[]{:S(2)}) collective-permute-start(bf16[64,2048]{1,0:T(8,128)(2,1)S(1)} %collective-permute-done.2.refs_2_), channel_id=1, source_target_pairs={{0,14},{2,0},{4,2},{6,4},{8,6},{10,8},{12,10},{14,12},{1,15},{3,1}... | collective-permute-start | bytes 786440 | tf_op jit(solution)/shard_map/ppermute | solution.py:50
  18.3 4.1 %conv.1 = bf16[16,64,256]{2,1,0:T(8,128)(2,1)} custom-call(bf16[64,4096]{1,0:T(8,128)(2,1)} %a_ref.3, bf16[64,4096]{1,0:T(8,128)(2,1)} %b_ref.3, bf16[64,4096]{1,0:T(8,128)(2,1)} %o_ref.1, s32[1,4096]{1,0:T(1,128)S(1)} %bitcast.14, f32[72,128]{1,0:T(8,128)S(1)} %collective-permute-done.halo_ref, f32[8,128]{1,0:T(8,128)S(1)} %select_maximum_fusion.small_ref), custom_call_target="tpu_custom_call" | custom-call | flops 200000000 | bytes 2097152 | tf_op jit(solution)/shard_map/conv/pallas_call | solution.py:145
  22.4 4.7 %all-to-all-start = ((bf16[16,64,256]{2,1,0:T(8,128)(2,1)}), bf16[16,64,256]{2,1,0:T(8,128)(2,1)S(1)}, u32[]{:S(2)}, u32[]{:S(2)}) async-start(bf16[16,64,256]{2,1,0:T(8,128)(2,1)} %conv.1), calls=%async_computation | async-start | bytes 1048576 | tf_op jit(solution)/shard_map/all_to_all | solution.py:476
  28.1 7.3 %collective-permute-start.22 = (bf16[2048,512]{1,0:T(8,128)(2,1)}, bf16[2048,512]{1,0:T(8,128)(2,1)S(1)}, u32[]{:S(2)}, u32[]{:S(2)}) collective-permute-start(bf16[2048,512]{1,0:T(8,128)(2,1)} %bitcast.18), channel_id=1, source_target_pairs={{0,0},{1,161},{16,16},{17,177},{32,32},{33,129},{48,48},{49,145},{... | collective-permute-start | bytes 6291464 | tf_op jit(solution)/shard_map/ppermute | solution.py:50
  41.0 10.5 %collective-permute-start.11 = (bf16[64,2048]{1,0:T(8,128)(2,1)}, bf16[64,2048]{1,0:T(8,128)(2,1)S(1)}, u32[]{:S(2)}, u32[]{:S(2)}) collective-permute-start(bf16[64,2048]{1,0:T(8,128)(2,1)} %collective-permute-done.3.refs_3_), channel_id=1, source_target_pairs={{0,1},{1,0},{2,3},{3,2},{4,5},{5,4},{6,7},{7,6},{8,9},{9,8},{10,11... | collective-permute-start | bytes 786440 | tf_op jit(solution)/shard_map/ppermute | solution.py:50
  51.5 3.5 %collective-permute-start.14 = (bf16[64,2048]{1,0:T(8,128)(2,1)S(1)}, bf16[64,2048]{1,0:T(8,128)(2,1)S(1)}, u32[]{:S(2)}, u32[]{:S(2)}) collective-permute-start(bf16[64,2048]{1,0:T(8,128)(2,1)S(1)} %collective-permute-done.6.refs_6_), channel_id=1, source_target_pairs={{0,1},{1,0},{2,3},{3,2},{4,5},{5,4},{6,7},{7,6},{8,9},{9,8},{10,11... | collective-permute-start | bytes 786440 | tf_op jit(solution)/shard_map/ppermute | solution.py:50
  57.3 7.3 %collective-permute-start.24 = (bf16[512,2048]{1,0:T(8,128)(2,1)}, bf16[512,2048]{1,0:T(8,128)(2,1)}, u32[]{:S(2)}, u32[]{:S(2)}) collective-permute-start(bf16[512,2048]{1,0:T(8,128)(2,1)} %bitcast.20), channel_id=1, source_target_pairs={{0,0},{1,161},{16,16},{17,177},{32,32},{33,129},{48,48},{49,145},{... | collective-permute-start | bytes 6291464 | tf_op jit(solution)/shard_map/ppermute | solution.py:50
  65.3 12.0 %collective-permute-start.13 = (bf16[64,2048]{1,0:T(8,128)(2,1)}, bf16[64,2048]{1,0:T(8,128)(2,1)}, u32[]{:S(2)}, u32[]{:S(2)}) collective-permute-start(bf16[64,2048]{1,0:T(8,128)(2,1)} %collective-permute-done.5.refs_5_), channel_id=1, source_target_pairs={{0,1},{1,0},{2,3},{3,2},{4,5},{5,4},{6,7},{7,6},{8,9},{9,8},{10,11... | collective-permute-start | bytes 786440 | tf_op jit(solution)/shard_map/ppermute | solution.py:50
  84.0 5.6 %mix.1 = (f32[256,2048]{1,0:T(8,128)}, bf16[256,2048]{1,0:T(8,128)(2,1)S(1)}) custom-call(s32[4]{0:T(128)S(1)} %pad_add_fusion.where_ref, bf16[16,64,256]{2,1,0:T(8,128)(2,1)S(1)} %all-to-all-done.by_row_ref, bf16[64,2048]{1,0:T(8,128)(2,1)S(1)} %copy-done, bf16[64,2048]{1,0:T(8,128)(2,1)S(1)} %collective-permute-done.1.refs_1_, ...), custom_call_target="tpu_custom_call" | custom-call | flops 1100000000 | bytes 8388608 | tf_op jit(solution)/shard_map/mix/pallas_call | solution.py:249
  100.8 8.3 %collective-permute-done.24.refs_6_.refs_4_ = bf16[512,2048]{1,0:T(8,128)(2,1)} collective-permute-done((bf16[512,2048]{1,0:T(8,128)(2,1)}, bf16[512,2048]{1,0:T(8,128)(2,1)}, u32[]{:S(2)}, u32[]{:S(2)}) %collective-permute-start.24) | collective-permute-done | bytes 2097184 | tf_op jit(solution)/shard_map/ppermute | solution.py:50
  109.1 6.7 %collective-permute-done.18.refs_0_ = bf16[128,2048]{1,0:T(8,128)(2,1)S(1)} collective-permute-done((bf16[128,2048]{1,0:T(8,128)(2,1)S(1)}, bf16[128,2048]{1,0:T(8,128)(2,1)S(1)}, u32[]{:S(2)}, u32[]{:S(2)}) %collective-permute-start.18) | collective-permute-done | bytes 524320 | tf_op jit(solution)/shard_map/ppermute | solution.py:50
  116.6 5.7 %experts.3 = (bf16[128,2048]{1,0:T(8,128)(2,1)S(1)}, bf16[128,2048]{1,0:T(8,128)(2,1)S(1)}, bf16[128,2048]{1,0:T(8,128)(2,1)S(1)}, bf16[128,2048]{1,0:T(8,128)(2,1)S(1)}) custom-call(bf16[128,2048]{1,0:T(8,128)(2,1)S(1)} %collective-permute-done.18.refs_0_, bf16[128,2048]{1,0:T(8,128)(2,1)S(1)} %collective-permute-done.19.refs_1_, ...), custom_call_target="tpu_custom_call" | custom-call | flops 3221225472 | bytes 8388608 | tf_op jit(solution)/shard_map/experts/pallas_call | solution.py:336
  128.3 3.6 %collective-permute-done.25.refs_0_ = bf16[128,2048]{1,0:T(8,128)(2,1)S(1)} collective-permute-done((bf16[128,2048]{1,0:T(8,128)(2,1)S(1)}, bf16[128,2048]{1,0:T(8,128)(2,1)S(1)}, u32[]{:S(2)}, u32[]{:S(2)}) %collective-permute-start.25) | collective-permute-done | bytes 524320 | tf_op jit(solution)/shard_map/ppermute | solution.py:50
  131.9 4.6 %collective-permute-start.32 = (bf16[128,2048]{1,0:T(8,128)(2,1)S(1)}, bf16[128,2048]{1,0:T(8,128)(2,1)S(1)}, u32[]{:S(2)}, u32[]{:S(2)}) collective-permute-start(bf16[128,2048]{1,0:T(8,128)(2,1)S(1)} %get-tuple-element.53), channel_id=1, source_target_pairs={{0,112},{1,81},{16,64},{17,97},{32,80},{33,113},{48,96},{49,65},{6... | collective-permute-start | bytes 1572872 | tf_op jit(solution)/shard_map/ppermute | solution.py:50
  139.5 4.6 %gather.1 = (f32[256,2048]{1,0:T(8,128)}, bf16[256,2048]{1,0:T(8,128)(2,1)S(1)}) custom-call(f32[256,2048]{1,0:T(8,128)} %get-tuple-element.33.acc_ref, s32[16,256]{1,0:T(8,128)S(1)} %get-tuple-element.34.rows_ref, f32[16,256]{1,0:T(8,128)S(1)} %get-tuple-element.35.weights_ref, s32[8,256]{1,0:T(8,128)S(1)} %get-tuple-element.36.theirs_at_ref.rows2_ref, ...), custom_call_target="tpu_custom_call" | custom-call | flops 1073741824 | bytes 10485760 | tf_op jit(solution)/shard_map/gather/pallas_call | solution.py:389
  144.1 5.4 %collective-permute-start.29 = (bf16[256,2048]{1,0:T(8,128)(2,1)S(1)}, bf16[256,2048]{1,0:T(8,128)(2,1)S(1)}, u32[]{:S(2)}, u32[]{:S(2)}) collective-permute-start(bf16[256,2048]{1,0:T(8,128)(2,1)S(1)} %get-tuple-element.48), channel_id=1, source_target_pairs={{0,1},{1,0},{2,3},{3,2},{4,5},{5,4},{6,7},{7,6},{8,9},{9,8},{10,11... | collective-permute-start | bytes 3145736 | tf_op jit(solution)/shard_map/ppermute | solution.py:50
  149.9 4.1 %experts.4 = (bf16[64,2048]{1,0:T(8,128)(2,1)S(1)}, bf16[64,2048]{1,0:T(8,128)(2,1)S(1)}, bf16[64,2048]{1,0:T(8,128)(2,1)S(1)}, bf16[64,2048]{1,0:T(8,128)(2,1)S(1)}) custom-call(bf16[128,2048]{1,0:T(8,128)(2,1)S(1)} %collective-permute-done.30.refs_0_, bf16[128,2048]{1,0:T(8,128)(2,1)S(1)} %get-tuple-element.50.refs_1_, ...), custom_call_target="tpu_custom_call" | custom-call | flops 1610612736 | bytes 8388608 | tf_op jit(solution)/shard_map/experts/pallas_call | solution.py:336
  154.1 13.4 %collective-permute-start.36 = (bf16[64,2048]{1,0:T(8,128)(2,1)S(1)}, bf16[64,2048]{1,0:T(8,128)(2,1)S(1)}, u32[]{:S(2)}, u32[]{:S(2)}) collective-permute-start(bf16[64,2048]{1,0:T(8,128)(2,1)S(1)} %get-tuple-element.57), channel_id=1, source_target_pairs={{0,241},{1,32},{16,193},{17,48},{32,209},{33,0},{48,225},{49,16},{... | collective-permute-start | bytes 786440 | tf_op jit(solution)/shard_map/ppermute | solution.py:50
  167.5 4.1 %experts.5 = (bf16[64,2048]{1,0:T(8,128)(2,1)S(1)}, bf16[64,2048]{1,0:T(8,128)(2,1)S(1)}, bf16[64,2048]{1,0:T(8,128)(2,1)S(1)}, bf16[64,2048]{1,0:T(8,128)(2,1)S(1)}) custom-call(bf16[128,2048]{1,0:T(8,128)(2,1)S(1)} %collective-permute-done.32.refs_0_, bf16[128,2048]{1,0:T(8,128)(2,1)S(1)} %collective-permute-done.33.refs_1_, ...), custom_call_target="tpu_custom_call" | custom-call | flops 1610612736 | bytes 8388608 | tf_op jit(solution)/shard_map/experts/pallas_call | solution.py:336
  171.6 9.2 %collective-permute-start.34 = (bf16[64,2048]{1,0:T(8,128)(2,1)S(1)}, bf16[64,2048]{1,0:T(8,128)(2,1)S(1)}, u32[]{:S(2)}, u32[]{:S(2)}) collective-permute-start(bf16[64,2048]{1,0:T(8,128)(2,1)S(1)} %get-tuple-element.55), channel_id=1, source_target_pairs={{0,208},{1,241},{16,224},{17,193},{32,240},{33,209},{48,192},{49,2... | collective-permute-start | bytes 786440 | tf_op jit(solution)/shard_map/ppermute | solution.py:50
  190.9 6.7 %collective-permute-done.38.refs_6_ = bf16[64,2048]{1,0:T(8,128)(2,1)S(1)} collective-permute-done((bf16[64,2048]{1,0:T(8,128)(2,1)S(1)}, bf16[64,2048]{1,0:T(8,128)(2,1)S(1)}, u32[]{:S(2)}, u32[]{:S(2)}) %collective-permute-start.38) | collective-permute-done | bytes 262176 | tf_op jit(solution)/shard_map/ppermute | solution.py:50
  197.6 6.6 %collective-permute-done.39.refs_7_ = bf16[64,2048]{1,0:T(8,128)(2,1)S(1)} collective-permute-done((bf16[64,2048]{1,0:T(8,128)(2,1)S(1)}, bf16[64,2048]{1,0:T(8,128)(2,1)S(1)}, u32[]{:S(2)}, u32[]{:S(2)}) %collective-permute-start.39) | collective-permute-done | bytes 262176 | tf_op jit(solution)/shard_map/ppermute | solution.py:50
  204.2 4.6 %finish.1 = bf16[256,2048]{1,0:T(8,128)(2,1)} custom-call(f32[256,2048]{1,0:T(8,128)} %get-tuple-element.47.acc_ref, bf16[256,2048]{1,0:T(8,128)(2,1)S(1)} %collective-permute-done.29.more_ref, s32[16,256]{1,0:T(8,128)S(1)} %get-tuple-element.34.rows_ref, f32[16,256]{1,0:T(8,128)S(1)} %get-tuple-element.35.weights_ref, ...), custom_call_target="tpu_custom_call" | custom-call | flops 1073741824 | bytes 6291456 | tf_op jit(solution)/shard_map/finish/pallas_call | solution.py:430
  (105 shorter events, 56.3 us)
Async XLA Ops:
  11.0 16.3 %collective-permute-start.8 = (bf16[64,2048]{1,0:T(8,128)(2,1)}, bf16[64,2048]{1,0:T(8,128)(2,1)S(1)}, u32[]{:S(2)}, u32[]{:S(2)}) collective-permute-start(bf16[64,2048]{1,0:T(8,128)(2,1)} %refs_0_.1), channel_id=1, source_target_pairs={{0,1},{1,0},{2,3},{3,2},{4,5},{5,4},{6,7},{7,6},{8,9},{9,8},{10,11... | collective-permute-start | bytes 786440 | tf_op jit(solution)/shard_map/ppermute | solution.py:50
  12.3 23.0 %collective-permute-start.10 = (bf16[64,2048]{1,0:T(8,128)(2,1)S(1)}, bf16[64,2048]{1,0:T(8,128)(2,1)}, u32[]{:S(2)}, u32[]{:S(2)}) collective-permute-start(bf16[64,2048]{1,0:T(8,128)(2,1)S(1)} %collective-permute-done.2.refs_2_), channel_id=1, source_target_pairs={{0,1},{1,0},{2,3},{3,2},{4,5},{5,4},{6,7},{7,6},{8,9},{9,8},{10,11... | collective-permute-start | bytes 786440 | tf_op jit(solution)/shard_map/ppermute | solution.py:50
  16.5 20.8 %collective-permute-start.9 = (bf16[64,2048]{1,0:T(8,128)(2,1)S(1)}, bf16[64,2048]{1,0:T(8,128)(2,1)}, u32[]{:S(2)}, u32[]{:S(2)}) collective-permute-start(bf16[64,2048]{1,0:T(8,128)(2,1)S(1)} %collective-permute-done.1.refs_1_), channel_id=1, source_target_pairs={{0,1},{1,0},{2,3},{3,2},{4,5},{5,4},{6,7},{7,6},{8,9},{9,8},{10,11... | collective-permute-start | bytes 786440 | tf_op jit(solution)/shard_map/ppermute | solution.py:50
  16.8 23.4 %collective-permute-start.3 = (bf16[64,2048]{1,0:T(8,128)(2,1)S(1)}, bf16[64,2048]{1,0:T(8,128)(2,1)}, u32[]{:S(2)}, u32[]{:S(2)}) collective-permute-start(bf16[64,2048]{1,0:T(8,128)(2,1)S(1)} %collective-permute-done.1.refs_1_), channel_id=1, source_target_pairs={{0,2},{2,4},{4,6},{6,8},{8,10},{10,12},{12,14},{14,0},{1,3},{3,5},... | collective-permute-start | bytes 786440 | tf_op jit(solution)/shard_map/ppermute | solution.py:50
  22.4 55.0 %all-to-all-start = ((bf16[16,64,256]{2,1,0:T(8,128)(2,1)}), bf16[16,64,256]{2,1,0:T(8,128)(2,1)S(1)}, u32[]{:S(2)}, u32[]{:S(2)}) async-start(bf16[16,64,256]{2,1,0:T(8,128)(2,1)} %conv.1), calls=%async_computation | async-start | bytes 1048576 | tf_op jit(solution)/shard_map/all_to_all | solution.py:476
  28.1 72.5 %collective-permute-start.22 = (bf16[2048,512]{1,0:T(8,128)(2,1)}, bf16[2048,512]{1,0:T(8,128)(2,1)S(1)}, u32[]{:S(2)}, u32[]{:S(2)}) collective-permute-start(bf16[2048,512]{1,0:T(8,128)(2,1)} %bitcast.18), channel_id=1, source_target_pairs={{0,0},{1,161},{16,16},{17,177},{32,32},{33,129},{48,48},{49,145},{... | collective-permute-start | bytes 6291464 | tf_op jit(solution)/shard_map/ppermute | solution.py:50
  35.4 65.4 %collective-permute-start.23 = (bf16[2048,512]{1,0:T(8,128)(2,1)}, bf16[2048,512]{1,0:T(8,128)(2,1)}, u32[]{:S(2)}, u32[]{:S(2)}) collective-permute-start(bf16[2048,512]{1,0:T(8,128)(2,1)} %bitcast.19), channel_id=1, source_target_pairs={{0,0},{1,161},{16,16},{17,177},{32,32},{33,129},{48,48},{49,145},{... | collective-permute-start | bytes 6291464 | tf_op jit(solution)/shard_map/ppermute | solution.py:50
  40.3 15.4 %collective-permute-start.5 = (bf16[64,2048]{1,0:T(8,128)(2,1)}, bf16[64,2048]{1,0:T(8,128)(2,1)}, u32[]{:S(2)}, u32[]{:S(2)}) collective-permute-start(bf16[64,2048]{1,0:T(8,128)(2,1)} %collective-permute-done.3.refs_3_), channel_id=1, source_target_pairs={{0,2},{2,4},{4,6},{6,8},{8,10},{10,12},{12,14},{14,0},{1,3},{3,5},... | collective-permute-start | bytes 786440 | tf_op jit(solution)/shard_map/ppermute | solution.py:50
  41.0 15.6 %collective-permute-start.11 = (bf16[64,2048]{1,0:T(8,128)(2,1)}, bf16[64,2048]{1,0:T(8,128)(2,1)S(1)}, u32[]{:S(2)}, u32[]{:S(2)}) collective-permute-start(bf16[64,2048]{1,0:T(8,128)(2,1)} %collective-permute-done.3.refs_3_), channel_id=1, source_target_pairs={{0,1},{1,0},{2,3},{3,2},{4,5},{5,4},{6,7},{7,6},{8,9},{9,8},{10,11... | collective-permute-start | bytes 786440 | tf_op jit(solution)/shard_map/ppermute | solution.py:50
  55.7 21.6 %collective-permute-start.7 = (bf16[64,2048]{1,0:T(8,128)(2,1)}, bf16[64,2048]{1,0:T(8,128)(2,1)}, u32[]{:S(2)}, u32[]{:S(2)}) collective-permute-start(bf16[64,2048]{1,0:T(8,128)(2,1)} %collective-permute-done.5.refs_5_), channel_id=1, source_target_pairs={{0,2},{2,4},{4,6},{6,8},{8,10},{10,12},{12,14},{14,0},{1,3},{3,5},... | collective-permute-start | bytes 786440 | tf_op jit(solution)/shard_map/ppermute | solution.py:50
  57.3 51.8 %collective-permute-start.24 = (bf16[512,2048]{1,0:T(8,128)(2,1)}, bf16[512,2048]{1,0:T(8,128)(2,1)}, u32[]{:S(2)}, u32[]{:S(2)}) collective-permute-start(bf16[512,2048]{1,0:T(8,128)(2,1)} %bitcast.20), channel_id=1, source_target_pairs={{0,0},{1,161},{16,16},{17,177},{32,32},{33,129},{48,48},{49,145},{... | collective-permute-start | bytes 6291464 | tf_op jit(solution)/shard_map/ppermute | solution.py:50
  95.3 20.5 %collective-permute-start.18 = (bf16[128,2048]{1,0:T(8,128)(2,1)S(1)}, bf16[128,2048]{1,0:T(8,128)(2,1)S(1)}, u32[]{:S(2)}, u32[]{:S(2)}) collective-permute-start(bf16[128,2048]{1,0:T(8,128)(2,1)S(1)} %get-tuple-element.39), channel_id=1, source_target_pairs={{0,16},{1,49},{16,32},{17,1},{32,48},{33,17},{48,0},{49,33},{64,80... | collective-permute-start | bytes 1572872 | tf_op jit(solution)/shard_map/ppermute | solution.py:50
  97.9 17.9 %collective-permute-start.19 = (bf16[128,2048]{1,0:T(8,128)(2,1)S(1)}, bf16[128,2048]{1,0:T(8,128)(2,1)S(1)}, u32[]{:S(2)}, u32[]{:S(2)}) collective-permute-start(bf16[128,2048]{1,0:T(8,128)(2,1)S(1)} %get-tuple-element.40), channel_id=1, source_target_pairs={{0,64},{1,193},{16,80},{17,209},{32,96},{33,225},{48,112},{49,241}... | collective-permute-start | bytes 1572872 | tf_op jit(solution)/shard_map/ppermute | solution.py:50
  100.6 16.0 %collective-permute-start.20 = (bf16[128,2048]{1,0:T(8,128)(2,1)S(1)}, bf16[128,2048]{1,0:T(8,128)(2,1)S(1)}, u32[]{:S(2)}, u32[]{:S(2)}) collective-permute-start(bf16[128,2048]{1,0:T(8,128)(2,1)S(1)} %get-tuple-element.41), channel_id=1, source_target_pairs={{0,48},{1,17},{16,0},{17,33},{32,16},{33,49},{48,32},{49,1},{64,11... | collective-permute-start | bytes 1572872 | tf_op jit(solution)/shard_map/ppermute | solution.py:50
  100.8 15.8 %collective-permute-start.21 = (bf16[128,2048]{1,0:T(8,128)(2,1)S(1)}, bf16[128,2048]{1,0:T(8,128)(2,1)S(1)}, u32[]{:S(2)}, u32[]{:S(2)}) collective-permute-start(bf16[128,2048]{1,0:T(8,128)(2,1)S(1)} %get-tuple-element.42), channel_id=1, source_target_pairs={{0,192},{1,65},{16,208},{17,81},{32,224},{33,97},{48,240},{49,113}... | collective-permute-start | bytes 1572872 | tf_op jit(solution)/shard_map/ppermute | solution.py:50
  127.7 22.2 %collective-permute-start.30 = (bf16[128,2048]{1,0:T(8,128)(2,1)S(1)}, bf16[128,2048]{1,0:T(8,128)(2,1)S(1)}, u32[]{:S(2)}, u32[]{:S(2)}) collective-permute-start(bf16[128,2048]{1,0:T(8,128)(2,1)S(1)} %get-tuple-element.49), channel_id=1, source_target_pairs={{0,80},{1,33},{16,96},{17,49},{32,112},{33,1},{48,64},{49,17},{64,... | collective-permute-start | bytes 1572872 | tf_op jit(solution)/shard_map/ppermute | solution.py:50
  131.9 35.5 %collective-permute-start.32 = (bf16[128,2048]{1,0:T(8,128)(2,1)S(1)}, bf16[128,2048]{1,0:T(8,128)(2,1)S(1)}, u32[]{:S(2)}, u32[]{:S(2)}) collective-permute-start(bf16[128,2048]{1,0:T(8,128)(2,1)S(1)} %get-tuple-element.53), channel_id=1, source_target_pairs={{0,112},{1,81},{16,64},{17,97},{32,80},{33,113},{48,96},{49,65},{6... | collective-permute-start | bytes 1572872 | tf_op jit(solution)/shard_map/ppermute | solution.py:50
  144.1 60.1 %collective-permute-start.29 = (bf16[256,2048]{1,0:T(8,128)(2,1)S(1)}, bf16[256,2048]{1,0:T(8,128)(2,1)S(1)}, u32[]{:S(2)}, u32[]{:S(2)}) collective-permute-start(bf16[256,2048]{1,0:T(8,128)(2,1)S(1)} %get-tuple-element.48), channel_id=1, source_target_pairs={{0,1},{1,0},{2,3},{3,2},{4,5},{5,4},{6,7},{7,6},{8,9},{9,8},{10,11... | collective-permute-start | bytes 3145736 | tf_op jit(solution)/shard_map/ppermute | solution.py:50
  149.5 17.9 %collective-permute-start.33 = (bf16[128,2048]{1,0:T(8,128)(2,1)S(1)}, bf16[128,2048]{1,0:T(8,128)(2,1)S(1)}, u32[]{:S(2)}, u32[]{:S(2)}) collective-permute-start(bf16[128,2048]{1,0:T(8,128)(2,1)S(1)} %get-tuple-element.54), channel_id=1, source_target_pairs={{0,32},{1,113},{16,48},{17,65},{32,0},{33,81},{48,16},{49,97},{64,... | collective-permute-start | bytes 1572872 | tf_op jit(solution)/shard_map/ppermute | solution.py:50
  154.0 26.8 %collective-permute-start.31 = (bf16[64,2048]{1,0:T(8,128)(2,1)S(1)}, bf16[64,2048]{1,0:T(8,128)(2,1)S(1)}, u32[]{:S(2)}, u32[]{:S(2)}) collective-permute-start(bf16[64,2048]{1,0:T(8,128)(2,1)S(1)} %get-tuple-element.51), channel_id=1, source_target_pairs={{0,240},{1,33},{16,192},{17,49},{32,208},{33,1},{48,224},{49,17},{... | collective-permute-start | bytes 786440 | tf_op jit(solution)/shard_map/ppermute | solution.py:50
  154.1 28.7 %collective-permute-start.36 = (bf16[64,2048]{1,0:T(8,128)(2,1)S(1)}, bf16[64,2048]{1,0:T(8,128)(2,1)S(1)}, u32[]{:S(2)}, u32[]{:S(2)}) collective-permute-start(bf16[64,2048]{1,0:T(8,128)(2,1)S(1)} %get-tuple-element.57), channel_id=1, source_target_pairs={{0,241},{1,32},{16,193},{17,48},{32,209},{33,0},{48,225},{49,16},{... | collective-permute-start | bytes 786440 | tf_op jit(solution)/shard_map/ppermute | solution.py:50
  167.5 18.0 %collective-permute-start.37 = (bf16[64,2048]{1,0:T(8,128)(2,1)S(1)}, bf16[64,2048]{1,0:T(8,128)(2,1)S(1)}, u32[]{:S(2)}, u32[]{:S(2)}) collective-permute-start(bf16[64,2048]{1,0:T(8,128)(2,1)S(1)} %get-tuple-element.58), channel_id=1, source_target_pairs={{0,1},{1,0},{16,17},{17,16},{32,33},{33,32},{48,49},{49,48},{64,65... | collective-permute-start | bytes 786440 | tf_op jit(solution)/shard_map/ppermute | solution.py:50
  171.6 17.1 %collective-permute-start.34 = (bf16[64,2048]{1,0:T(8,128)(2,1)S(1)}, bf16[64,2048]{1,0:T(8,128)(2,1)S(1)}, u32[]{:S(2)}, u32[]{:S(2)}) collective-permute-start(bf16[64,2048]{1,0:T(8,128)(2,1)S(1)} %get-tuple-element.55), channel_id=1, source_target_pairs={{0,208},{1,241},{16,224},{17,193},{32,240},{33,209},{48,192},{49,2... | collective-permute-start | bytes 786440 | tf_op jit(solution)/shard_map/ppermute | solution.py:50
  185.5 18.7 %collective-permute-start.39 = (bf16[64,2048]{1,0:T(8,128)(2,1)S(1)}, bf16[64,2048]{1,0:T(8,128)(2,1)S(1)}, u32[]{:S(2)}, u32[]{:S(2)}) collective-permute-start(bf16[64,2048]{1,0:T(8,128)(2,1)S(1)} %get-tuple-element.60), channel_id=1, source_target_pairs={{0,33},{1,208},{16,49},{17,224},{32,1},{33,240},{48,17},{49,192},{... | collective-permute-start | bytes 786440 | tf_op jit(solution)/shard_map/ppermute | solution.py:50
  (33 other events, 347.8 us)

commit v4 on v3

--- a/solution.py
+++ b/solution.py
@@ -61,7 +61,11 @@
 
 
 def hosted(value):
-    return permute(value, CHIP, (4, 4, 2), lambda y, x, c: (y - 2 * c, x - 2 * c, c))
+    pairs = []
+    for y, x in np.ndindex(4, 4):
+        to = (y + 2) % 4 * 4 + (x + 2) % 4
+        pairs.append(((y * 4 + x) * 2 + 1, to * 2 + 1))
+    return lax.ppermute(value, CHIP, pairs)
 
 
 def along_z(value, step):
@@ -269,7 +273,7 @@
         compiler_params=params(16, True),
         cost_estimate=cost(1.1e9, 8 << 20),
         name="mix",
-    )(where, by_row, *own, *swapped, in_hbm(resid), gain)
+    )(where, by_row, *map(in_hbm, own), *map(in_hbm, swapped), in_hbm(resid), gain)
 
 
 def pack_kernel(mine_ref, theirs_ref, mine_at_ref, theirs_at_ref, *refs):
@@ -307,6 +311,37 @@
         cost_estimate=cost(1.1e9, 6 << 20),
         name="pack",
     )(mine, theirs, mine_at, theirs_at)
+
+
+def choose_kernel(where_ref, *refs):
+    own, received, outs, sems = refs[:3], refs[3:6], refs[6:9], refs[9]
+    c = where_ref[3]
+
+    @pl.when(c == 0)
+    def _():
+        for k in range(3):
+            pltpu.make_async_copy(own[k], outs[k], sems.at[k]).start()
+
+    @pl.when(c != 0)
+    def _():
+        for k in range(3):
+            pltpu.make_async_copy(received[k], outs[k], sems.at[k]).start()
+
+    for k in range(3):
+        pltpu.make_async_copy(own[k], outs[k], sems.at[k]).wait()
+
+
+def choose(where, own, received):
+    return pl.pallas_call(
+        choose_kernel,
+        out_shape=[jax.ShapeDtypeStruct(w.shape, w.dtype) for w in own],
+        in_specs=[SMEM] + [pl.BlockSpec(memory_space=pltpu.HBM)] * 6,
+        out_specs=[VMEM] * 3,
+        scratch_shapes=[pltpu.SemaphoreType.DMA((3,))],
+        compiler_params=params(8),
+        cost_estimate=cost(1e6, 12 << 20),
+        name="choose",
+    )(where, *map(in_hbm, own), *map(in_hbm, received))
 
 
 def expert_kernel(n, *refs):
@@ -460,9 +495,8 @@
 ):
     y, x, z, c = (lax.axis_index(a) for a in ("y", "x", "z", "c"))
 
-    wg = hosted(w_gate[0])
-    wu = hosted(w_up[0])
-    wd = hosted(w_down[0])
+    own_weights = (w_gate[0], w_up[0], w_down[0])
+    received = [hosted(w) for w in own_weights]
 
     plus, minus = [out_proj], [out_proj]
     plus.append(along_z(out_proj, 1))
@@ -492,6 +526,7 @@
     sends = pack(normed, normed_other, rows[: len(PAIRS)], rows_other)
     arrived = [displaced(s, k, 1) for k, s in enumerate(sends)]
 
+    wg, wu, wd = choose(where, own_weights, received)
     back, cross = {}, {}
     for n, group in enumerate(GROUPS):
         apart = n > 0

time: 212 us -> 203 us (0.958)
  the two profiles are of different devices: /device:TPU:1 before, /device:TPU:25 now
where the time goes in v4:
time: 203 us; the launch traced here: 202 us
  starting transfers between devices  86.7 us (43%)
  waiting for transfers between devices  77.5 us (38%)
  Pallas kernels  33.9 us (17%)
  local copies, waits for them, and re-layouts  2.76 us (1%)
    ppermute x36, starting transfers between devices, permute(): return lax.ppermute(value, axes, pairs)  64.3 us
    ppermute x36, waiting for transfers between devices, permute(): return lax.ppermute(value, axes, pairs)  42.7 us
    ppermute x3, waiting for transfers between devices, hosted(): return lax.ppermute(value, CHIP, pairs)  34.8 us
    ppermute x3, starting transfers between devices, hosted(): return lax.ppermute(value, CHIP, pairs)  13.3 us
    pallas_call x3, Pallas kernels, experts(): pl.pallas_call(functools.partial(expert_kernel, len(bufs)), out_shape=[ja...  7.21 us
    pallas_call x1, Pallas kernels, mix(): pl.pallas_call(mix_kernel, grid=(WIDTH // TILE,), out_shape=[pltpu.HBM((R...  5.97 us
    all_to_all x1, starting transfers between devices, body(): lax.all_to_all(head_normed, TP, split_axis=0, concat_axis=0, tiled=True)  5.92 us
    pallas_call x1, Pallas kernels, finish(): pl.pallas_call(functools.partial(finish_kernel, chunks), grid=(WIDTH // T...  4.56 us
  transfers between devices with their start and end apart: 41, of which 14 were waited for; matrix products, arithmetic and copies ran while one was open for 0% of the time, Pallas kernels for 13%

profile of v4, /device:TPU:25, one launch (start us, length us, event | category | flops | bytes accessed | tf_op | source)
XLA Modules:
  0.0 201.8 jit_solution(14368912718852793135)
XLA Ops:
  0.0 5.6 %collective-permute-start.2 = (bf16[64,2048]{1,0:T(8,128)(2,1)}, bf16[64,2048]{1,0:T(8,128)(2,1)S(1)}, u32[]{:S(2)}, u32[]{:S(2)}) collective-permute-start(bf16[64,2048]{1,0:T(8,128)(2,1)} %refs_0_.1), channel_id=1, source_target_pairs={{0,14},{2,0},{4,2},{6,4},{8,6},{10,8},{12,10},{14,12},{1,15},{3,1}... | collective-permute-start | bytes 786440 | tf_op jit(solution)/shard_map/ppermute | solution.py:50
  7.1 3.1 %collective-permute-start = (f32[72,128]{1,0:T(8,128)S(1)}, f32[72,128]{1,0:T(8,128)S(1)}, u32[]{:S(2)}, u32[]{:S(2)}) collective-permute-start(f32[72,128]{1,0:T(8,128)S(1)} %tail.1), channel_id=1, source_target_pairs={{0,16},{16,32},{32,48},{48,64},{64,80},{80,96},{96,112},{112,128},... | collective-permute-start | bytes 110600 | tf_op jit(solution)/shard_map/ppermute | solution.py:507
  12.4 3.3 %collective-permute-start.4 = (bf16[64,2048]{1,0:T(8,128)(2,1)S(1)}, bf16[64,2048]{1,0:T(8,128)(2,1)}, u32[]{:S(2)}, u32[]{:S(2)}) collective-permute-start(bf16[64,2048]{1,0:T(8,128)(2,1)S(1)} %collective-permute-done.2.refs_2_), channel_id=1, source_target_pairs={{0,14},{2,0},{4,2},{6,4},{8,6},{10,8},{12,10},{14,12},{1,15},{3,1}... | collective-permute-start | bytes 786440 | tf_op jit(solution)/shard_map/ppermute | solution.py:50
  17.4 4.3 %conv.1 = bf16[16,64,256]{2,1,0:T(8,128)(2,1)} custom-call(bf16[64,4096]{1,0:T(8,128)(2,1)} %a_ref.3, bf16[64,4096]{1,0:T(8,128)(2,1)} %b_ref.3, bf16[64,4096]{1,0:T(8,128)(2,1)} %o_ref.1, s32[1,4096]{1,0:T(1,128)S(1)} %bitcast.14, f32[72,128]{1,0:T(8,128)S(1)} %collective-permute-done.halo_ref, f32[8,128]{1,0:T(8,128)S(1)} %select_maximum_fusion.small_ref), custom_call_target="tpu_custom_call" | custom-call | flops 200000000 | bytes 2097152 | tf_op jit(solution)/shard_map/conv/pallas_call | solution.py:149
  21.7 5.9 %all-to-all-start = ((bf16[16,64,256]{2,1,0:T(8,128)(2,1)}), bf16[16,64,256]{2,1,0:T(8,128)(2,1)S(1)}, u32[]{:S(2)}, u32[]{:S(2)}) async-start(bf16[16,64,256]{2,1,0:T(8,128)(2,1)} %conv.1), calls=%async_computation | async-start | bytes 1048576 | tf_op jit(solution)/shard_map/all_to_all | solution.py:510
  27.9 4.1 %collective-permute-start.22 = (bf16[2048,512]{1,0:T(8,128)(2,1)S(1)}, bf16[2048,512]{1,0:T(8,128)(2,1)}, u32[]{:S(2)}, u32[]{:S(2)}) collective-permute-start(bf16[2048,512]{1,0:T(8,128)(2,1)S(1)} %bitcast.17), channel_id=1, source_target_pairs={{1,161},{17,177},{33,129},{49,145},{65,225},{81,241},{97,193},{113... | collective-permute-start | bytes 6291464 | tf_op jit(solution)/shard_map/ppermute | solution.py:68
  32.0 5.0 %collective-permute-start.23 = (bf16[2048,512]{1,0:T(8,128)(2,1)}, bf16[2048,512]{1,0:T(8,128)(2,1)}, u32[]{:S(2)}, u32[]{:S(2)}) collective-permute-start(bf16[2048,512]{1,0:T(8,128)(2,1)} %bitcast.18), channel_id=1, source_target_pairs={{1,161},{17,177},{33,129},{49,145},{65,225},{81,241},{97,193},{113... | collective-permute-start | bytes 6291464 | tf_op jit(solution)/shard_map/ppermute | solution.py:68
  37.1 2.9 %collective-permute-start.6 = (bf16[64,2048]{1,0:T(8,128)(2,1)}, bf16[64,2048]{1,0:T(8,128)(2,1)S(1)}, u32[]{:S(2)}, u32[]{:S(2)}) collective-permute-start(bf16[64,2048]{1,0:T(8,128)(2,1)} %collective-permute-done.4.refs_4_), channel_id=1, source_target_pairs={{0,14},{2,0},{4,2},{6,4},{8,6},{10,8},{12,10},{14,12},{1,15},{3,1}... | collective-permute-start | bytes 786440 | tf_op jit(solution)/shard_map/ppermute | solution.py:50
  40.2 6.7 %collective-permute-done.6.refs_6_ = bf16[64,2048]{1,0:T(8,128)(2,1)S(1)} collective-permute-done((bf16[64,2048]{1,0:T(8,128)(2,1)}, bf16[64,2048]{1,0:T(8,128)(2,1)S(1)}, u32[]{:S(2)}, u32[]{:S(2)}) %collective-permute-start.6) | collective-permute-done | bytes 262176 | tf_op jit(solution)/shard_map/ppermute | solution.py:50
  49.6 4.1 %collective-permute-start.24 = (bf16[512,2048]{1,0:T(8,128)(2,1)}, bf16[512,2048]{1,0:T(8,128)(2,1)}, u32[]{:S(2)}, u32[]{:S(2)}) collective-permute-start(bf16[512,2048]{1,0:T(8,128)(2,1)} %bitcast.20), channel_id=1, source_target_pairs={{1,161},{17,177},{33,129},{49,145},{65,225},{81,241},{97,193},{113... | collective-permute-start | bytes 6291464 | tf_op jit(solution)/shard_map/ppermute | solution.py:68
  54.5 3.4 %collective-permute-done.7.refs_7_ = bf16[64,2048]{1,0:T(8,128)(2,1)} collective-permute-done((bf16[64,2048]{1,0:T(8,128)(2,1)}, bf16[64,2048]{1,0:T(8,128)(2,1)}, u32[]{:S(2)}, u32[]{:S(2)}) %collective-permute-start.7) | collective-permute-done | bytes 262176 | tf_op jit(solution)/shard_map/ppermute | solution.py:50
  60.2 6.0 %mix.1 = (f32[256,2048]{1,0:T(8,128)}, bf16[256,2048]{1,0:T(8,128)(2,1)S(1)}) custom-call(s32[4]{0:T(128)S(1)} %pad_add_fusion.where_ref, bf16[16,64,256]{2,1,0:T(8,128)(2,1)S(1)} %all-to-all-done.by_row_ref, bf16[64,2048]{1,0:T(8,128)(2,1)} %refs_0_.1, bf16[64,2048]{1,0:T(8,128)(2,1)} %copy-done.5, bf16[64,2048]{1,0:T(8,128)(2,1)} %copy-done.4, ...), custom_call_target="tpu_custom_call" | custom-call | flops 1100000000 | bytes 8388608 | tf_op jit(solution)/shard_map/mix/pallas_call | solution.py:253
  74.3 10.6 %collective-permute-done.23.refs_4_ = bf16[2048,512]{1,0:T(8,128)(2,1)} collective-permute-done((bf16[2048,512]{1,0:T(8,128)(2,1)}, bf16[2048,512]{1,0:T(8,128)(2,1)}, u32[]{:S(2)}, u32[]{:S(2)}) %collective-permute-start.23) | collective-permute-done | bytes 2097184 | tf_op jit(solution)/shard_map/ppermute | solution.py:68
  85.1 24.2 %collective-permute-done.24.refs_5_ = bf16[512,2048]{1,0:T(8,128)(2,1)} collective-permute-done((bf16[512,2048]{1,0:T(8,128)(2,1)}, bf16[512,2048]{1,0:T(8,128)(2,1)}, u32[]{:S(2)}, u32[]{:S(2)}) %collective-permute-start.24) | collective-permute-done | bytes 2097184 | tf_op jit(solution)/shard_map/ppermute | solution.py:68
  109.3 3.4 %choose.1 = (bf16[2048,512]{1,0:T(8,128)(2,1)S(1)}, bf16[2048,512]{1,0:T(8,128)(2,1)S(1)}, bf16[512,2048]{1,0:T(8,128)(2,1)S(1)}) custom-call(s32[4]{0:T(128)S(1)} %pad_add_fusion.where_ref, bf16[2048,512]{1,0:T(8,128)(2,1)} %bitcast.16, bf16[2048,512]{1,0:T(8,128)(2,1)} %bitcast.19, bf16[512,2048]{1,0:T(8,128)(2,1)} %bitcast.21, ...), custom_call_target="tpu_custom_call" | custom-call | flops 1000000 | bytes 12582912 | tf_op jit(solution)/shard_map/choose/pallas_call | solution.py:335
  113.8 3.5 %experts.3 = (bf16[128,2048]{1,0:T(8,128)(2,1)S(1)}, bf16[128,2048]{1,0:T(8,128)(2,1)S(1)}, bf16[128,2048]{1,0:T(8,128)(2,1)S(1)}, bf16[128,2048]{1,0:T(8,128)(2,1)S(1)}) custom-call(bf16[128,2048]{1,0:T(8,128)(2,1)S(1)} %collective-permute-done.18.refs_0_, bf16[128,2048]{1,0:T(8,128)(2,1)S(1)} %collective-permute-done.19.refs_1_, ...), custom_call_target="tpu_custom_call" | custom-call | flops 3221225472 | bytes 8388608 | tf_op jit(solution)/shard_map/experts/pallas_call | solution.py:371
  122.6 6.3 %collective-permute-done.25.refs_0_ = bf16[128,2048]{1,0:T(8,128)(2,1)S(1)} collective-permute-done((bf16[128,2048]{1,0:T(8,128)(2,1)S(1)}, bf16[128,2048]{1,0:T(8,128)(2,1)S(1)}, u32[]{:S(2)}, u32[]{:S(2)}) %collective-permute-start.25) | collective-permute-done | bytes 524320 | tf_op jit(solution)/shard_map/ppermute | solution.py:50
  129.7 7.2 %collective-permute-done.27.refs_2_ = bf16[128,2048]{1,0:T(8,128)(2,1)S(1)} collective-permute-done((bf16[128,2048]{1,0:T(8,128)(2,1)S(1)}, bf16[128,2048]{1,0:T(8,128)(2,1)S(1)}, u32[]{:S(2)}, u32[]{:S(2)}) %collective-permute-start.27) | collective-permute-done | bytes 524320 | tf_op jit(solution)/shard_map/ppermute | solution.py:50
  136.9 4.5 %gather.1 = (f32[256,2048]{1,0:T(8,128)}, bf16[256,2048]{1,0:T(8,128)(2,1)S(1)}) custom-call(f32[256,2048]{1,0:T(8,128)} %get-tuple-element.36.acc_ref, s32[16,256]{1,0:T(8,128)S(1)} %get-tuple-element.37.rows_ref, f32[16,256]{1,0:T(8,128)S(1)} %get-tuple-element.38.weights_ref, s32[8,256]{1,0:T(8,128)S(1)} %get-tuple-element.39.theirs_at_ref.rows2_ref, ...), custom_call_target="tpu_custom_call" | custom-call | flops 1073741824 | bytes 10485760 | tf_op jit(solution)/shard_map/gather/pallas_call | solution.py:424
  146.6 21.5 %collective-permute-start.36 = (bf16[64,2048]{1,0:T(8,128)(2,1)S(1)}, bf16[64,2048]{1,0:T(8,128)(2,1)S(1)}, u32[]{:S(2)}, u32[]{:S(2)}) collective-permute-start(bf16[64,2048]{1,0:T(8,128)(2,1)S(1)} %get-tuple-element.63), channel_id=1, source_target_pairs={{0,241},{1,32},{16,193},{17,48},{32,209},{33,0},{48,225},{49,16},{... | collective-permute-start | bytes 786440 | tf_op jit(solution)/shard_map/ppermute | solution.py:50
  171.5 11.3 %collective-permute-start.38 = (bf16[64,2048]{1,0:T(8,128)(2,1)S(1)}, bf16[64,2048]{1,0:T(8,128)(2,1)S(1)}, u32[]{:S(2)}, u32[]{:S(2)}) collective-permute-start(bf16[64,2048]{1,0:T(8,128)(2,1)S(1)} %get-tuple-element.65), channel_id=1, source_target_pairs={{0,209},{1,240},{16,225},{17,192},{32,241},{33,208},{48,193},{49,2... | collective-permute-start | bytes 786440 | tf_op jit(solution)/shard_map/ppermute | solution.py:50
  185.6 4.7 %collective-permute-done.38.refs_6_ = bf16[64,2048]{1,0:T(8,128)(2,1)S(1)} collective-permute-done((bf16[64,2048]{1,0:T(8,128)(2,1)S(1)}, bf16[64,2048]{1,0:T(8,128)(2,1)S(1)}, u32[]{:S(2)}, u32[]{:S(2)}) %collective-permute-start.38) | collective-permute-done | bytes 262176 | tf_op jit(solution)/shard_map/ppermute | solution.py:50
  190.3 6.9 %collective-permute-done.39.refs_7_ = bf16[64,2048]{1,0:T(8,128)(2,1)S(1)} collective-permute-done((bf16[64,2048]{1,0:T(8,128)(2,1)S(1)}, bf16[64,2048]{1,0:T(8,128)(2,1)S(1)}, u32[]{:S(2)}, u32[]{:S(2)}) %collective-permute-start.39) | collective-permute-done | bytes 262176 | tf_op jit(solution)/shard_map/ppermute | solution.py:50
  197.3 4.6 %finish.1 = bf16[256,2048]{1,0:T(8,128)(2,1)} custom-call(f32[256,2048]{1,0:T(8,128)} %get-tuple-element.53.acc_ref, bf16[256,2048]{1,0:T(8,128)(2,1)S(1)} %collective-permute-done.29.more_ref, s32[16,256]{1,0:T(8,128)S(1)} %get-tuple-element.37.rows_ref, f32[16,256]{1,0:T(8,128)S(1)} %get-tuple-element.38.weights_ref, ...), custom_call_target="tpu_custom_call" | custom-call | flops 1073741824 | bytes 6291456 | tf_op jit(solution)/shard_map/finish/pallas_call | solution.py:465
  (98 shorter events, 38.3 us)
Async XLA Ops:
  10.2 17.7 %collective-permute-start.8 = (bf16[64,2048]{1,0:T(8,128)(2,1)}, bf16[64,2048]{1,0:T(8,128)(2,1)S(1)}, u32[]{:S(2)}, u32[]{:S(2)}) collective-permute-start(bf16[64,2048]{1,0:T(8,128)(2,1)} %refs_0_.1), channel_id=1, source_target_pairs={{0,1},{1,0},{2,3},{3,2},{4,5},{5,4},{6,7},{7,6},{8,9},{9,8},{10,11... | collective-permute-start | bytes 786440 | tf_op jit(solution)/shard_map/ppermute | solution.py:50
  11.5 20.5 %collective-permute-start.10 = (bf16[64,2048]{1,0:T(8,128)(2,1)S(1)}, bf16[64,2048]{1,0:T(8,128)(2,1)}, u32[]{:S(2)}, u32[]{:S(2)}) collective-permute-start(bf16[64,2048]{1,0:T(8,128)(2,1)S(1)} %collective-permute-done.2.refs_2_), channel_id=1, source_target_pairs={{0,1},{1,0},{2,3},{3,2},{4,5},{5,4},{6,7},{7,6},{8,9},{9,8},{10,11... | collective-permute-start | bytes 786440 | tf_op jit(solution)/shard_map/ppermute | solution.py:50
  12.4 15.3 %collective-permute-start.4 = (bf16[64,2048]{1,0:T(8,128)(2,1)S(1)}, bf16[64,2048]{1,0:T(8,128)(2,1)}, u32[]{:S(2)}, u32[]{:S(2)}) collective-permute-start(bf16[64,2048]{1,0:T(8,128)(2,1)S(1)} %collective-permute-done.2.refs_2_), channel_id=1, source_target_pairs={{0,14},{2,0},{4,2},{6,4},{8,6},{10,8},{12,10},{14,12},{1,15},{3,1}... | collective-permute-start | bytes 786440 | tf_op jit(solution)/shard_map/ppermute | solution.py:50
  15.7 21.4 %collective-permute-start.9 = (bf16[64,2048]{1,0:T(8,128)(2,1)S(1)}, bf16[64,2048]{1,0:T(8,128)(2,1)}, u32[]{:S(2)}, u32[]{:S(2)}) collective-permute-start(bf16[64,2048]{1,0:T(8,128)(2,1)S(1)} %collective-permute-done.1.refs_1_), channel_id=1, source_target_pairs={{0,1},{1,0},{2,3},{3,2},{4,5},{5,4},{6,7},{7,6},{8,9},{9,8},{10,11... | collective-permute-start | bytes 786440 | tf_op jit(solution)/shard_map/ppermute | solution.py:50
  16.0 24.0 %collective-permute-start.3 = (bf16[64,2048]{1,0:T(8,128)(2,1)S(1)}, bf16[64,2048]{1,0:T(8,128)(2,1)}, u32[]{:S(2)}, u32[]{:S(2)}) collective-permute-start(bf16[64,2048]{1,0:T(8,128)(2,1)S(1)} %collective-permute-done.1.refs_1_), channel_id=1, source_target_pairs={{0,2},{2,4},{4,6},{6,8},{8,10},{10,12},{12,14},{14,0},{1,3},{3,5},... | collective-permute-start | bytes 786440 | tf_op jit(solution)/shard_map/ppermute | solution.py:50
  21.7 37.0 %all-to-all-start = ((bf16[16,64,256]{2,1,0:T(8,128)(2,1)}), bf16[16,64,256]{2,1,0:T(8,128)(2,1)S(1)}, u32[]{:S(2)}, u32[]{:S(2)}) async-start(bf16[16,64,256]{2,1,0:T(8,128)(2,1)} %conv.1), calls=%async_computation | async-start | bytes 1048576 | tf_op jit(solution)/shard_map/all_to_all | solution.py:510
  27.9 46.2 %collective-permute-start.22 = (bf16[2048,512]{1,0:T(8,128)(2,1)S(1)}, bf16[2048,512]{1,0:T(8,128)(2,1)}, u32[]{:S(2)}, u32[]{:S(2)}) collective-permute-start(bf16[2048,512]{1,0:T(8,128)(2,1)S(1)} %bitcast.17), channel_id=1, source_target_pairs={{1,161},{17,177},{33,129},{49,145},{65,225},{81,241},{97,193},{113... | collective-permute-start | bytes 6291464 | tf_op jit(solution)/shard_map/ppermute | solution.py:68
  32.0 52.8 %collective-permute-start.23 = (bf16[2048,512]{1,0:T(8,128)(2,1)}, bf16[2048,512]{1,0:T(8,128)(2,1)}, u32[]{:S(2)}, u32[]{:S(2)}) collective-permute-start(bf16[2048,512]{1,0:T(8,128)(2,1)} %bitcast.18), channel_id=1, source_target_pairs={{1,161},{17,177},{33,129},{49,145},{65,225},{81,241},{97,193},{113... | collective-permute-start | bytes 6291464 | tf_op jit(solution)/shard_map/ppermute | solution.py:68
  49.6 59.7 %collective-permute-start.24 = (bf16[512,2048]{1,0:T(8,128)(2,1)}, bf16[512,2048]{1,0:T(8,128)(2,1)}, u32[]{:S(2)}, u32[]{:S(2)}) collective-permute-start(bf16[512,2048]{1,0:T(8,128)(2,1)} %bitcast.20), channel_id=1, source_target_pairs={{1,161},{17,177},{33,129},{49,145},{65,225},{81,241},{97,193},{113... | collective-permute-start | bytes 6291464 | tf_op jit(solution)/shard_map/ppermute | solution.py:68
  72.3 40.5 %collective-permute-start.18 = (bf16[128,2048]{1,0:T(8,128)(2,1)S(1)}, bf16[128,2048]{1,0:T(8,128)(2,1)S(1)}, u32[]{:S(2)}, u32[]{:S(2)}) collective-permute-start(bf16[128,2048]{1,0:T(8,128)(2,1)S(1)} %get-tuple-element.42), channel_id=1, source_target_pairs={{0,16},{1,49},{16,32},{17,1},{32,48},{33,17},{48,0},{49,33},{64,80... | collective-permute-start | bytes 1572872 | tf_op jit(solution)/shard_map/ppermute | solution.py:50
  73.7 40.2 %collective-permute-start.19 = (bf16[128,2048]{1,0:T(8,128)(2,1)S(1)}, bf16[128,2048]{1,0:T(8,128)(2,1)S(1)}, u32[]{:S(2)}, u32[]{:S(2)}) collective-permute-start(bf16[128,2048]{1,0:T(8,128)(2,1)S(1)} %get-tuple-element.43), channel_id=1, source_target_pairs={{0,64},{1,193},{16,80},{17,209},{32,96},{33,225},{48,112},{49,241}... | collective-permute-start | bytes 1572872 | tf_op jit(solution)/shard_map/ppermute | solution.py:50
  74.1 39.7 %collective-permute-start.20 = (bf16[128,2048]{1,0:T(8,128)(2,1)S(1)}, bf16[128,2048]{1,0:T(8,128)(2,1)S(1)}, u32[]{:S(2)}, u32[]{:S(2)}) collective-permute-start(bf16[128,2048]{1,0:T(8,128)(2,1)S(1)} %get-tuple-element.44), channel_id=1, source_target_pairs={{0,48},{1,17},{16,0},{17,33},{32,16},{33,49},{48,32},{49,1},{64,11... | collective-permute-start | bytes 1572872 | tf_op jit(solution)/shard_map/ppermute | solution.py:50
  84.9 29.0 %collective-permute-start.21 = (bf16[128,2048]{1,0:T(8,128)(2,1)S(1)}, bf16[128,2048]{1,0:T(8,128)(2,1)S(1)}, u32[]{:S(2)}, u32[]{:S(2)}) collective-permute-start(bf16[128,2048]{1,0:T(8,128)(2,1)S(1)} %get-tuple-element.45), channel_id=1, source_target_pairs={{0,192},{1,65},{16,208},{17,81},{32,224},{33,97},{48,240},{49,113}... | collective-permute-start | bytes 1572872 | tf_op jit(solution)/shard_map/ppermute | solution.py:50
  118.9 18.0 %collective-permute-start.27 = (bf16[128,2048]{1,0:T(8,128)(2,1)S(1)}, bf16[128,2048]{1,0:T(8,128)(2,1)S(1)}, u32[]{:S(2)}, u32[]{:S(2)}) collective-permute-start(bf16[128,2048]{1,0:T(8,128)(2,1)S(1)} %get-tuple-element.51), channel_id=1, source_target_pairs={{0,16},{1,49},{16,32},{17,1},{32,48},{33,17},{48,0},{49,33},{64,80... | collective-permute-start | bytes 1572872 | tf_op jit(solution)/shard_map/ppermute | solution.py:50
  121.1 15.8 %collective-permute-start.28 = (bf16[128,2048]{1,0:T(8,128)(2,1)S(1)}, bf16[128,2048]{1,0:T(8,128)(2,1)S(1)}, u32[]{:S(2)}, u32[]{:S(2)}) collective-permute-start(bf16[128,2048]{1,0:T(8,128)(2,1)S(1)} %get-tuple-element.52), channel_id=1, source_target_pairs={{0,64},{1,193},{16,80},{17,209},{32,96},{33,225},{48,112},{49,241}... | collective-permute-start | bytes 1572872 | tf_op jit(solution)/shard_map/ppermute | solution.py:50
  121.5 22.8 %collective-permute-start.30 = (bf16[128,2048]{1,0:T(8,128)(2,1)S(1)}, bf16[128,2048]{1,0:T(8,128)(2,1)S(1)}, u32[]{:S(2)}, u32[]{:S(2)}) collective-permute-start(bf16[128,2048]{1,0:T(8,128)(2,1)S(1)} %get-tuple-element.55), channel_id=1, source_target_pairs={{0,80},{1,33},{16,96},{17,49},{32,112},{33,1},{48,64},{49,17},{64,... | collective-permute-start | bytes 1572872 | tf_op jit(solution)/shard_map/ppermute | solution.py:50
  128.8 39.3 %collective-permute-start.32 = (bf16[128,2048]{1,0:T(8,128)(2,1)S(1)}, bf16[128,2048]{1,0:T(8,128)(2,1)S(1)}, u32[]{:S(2)}, u32[]{:S(2)}) collective-permute-start(bf16[128,2048]{1,0:T(8,128)(2,1)S(1)} %get-tuple-element.59), channel_id=1, source_target_pairs={{0,112},{1,81},{16,64},{17,97},{32,80},{33,113},{48,96},{49,65},{6... | collective-permute-start | bytes 1572872 | tf_op jit(solution)/shard_map/ppermute | solution.py:50
  141.5 55.8 %collective-permute-start.29 = (bf16[256,2048]{1,0:T(8,128)(2,1)S(1)}, bf16[256,2048]{1,0:T(8,128)(2,1)S(1)}, u32[]{:S(2)}, u32[]{:S(2)}) collective-permute-start(bf16[256,2048]{1,0:T(8,128)(2,1)S(1)} %get-tuple-element.54), channel_id=1, source_target_pairs={{0,1},{1,0},{2,3},{3,2},{4,5},{5,4},{6,7},{7,6},{8,9},{9,8},{10,11... | collective-permute-start | bytes 3145736 | tf_op jit(solution)/shard_map/ppermute | solution.py:50
  141.5 26.6 %collective-permute-start.33 = (bf16[128,2048]{1,0:T(8,128)(2,1)S(1)}, bf16[128,2048]{1,0:T(8,128)(2,1)S(1)}, u32[]{:S(2)}, u32[]{:S(2)}) collective-permute-start(bf16[128,2048]{1,0:T(8,128)(2,1)S(1)} %get-tuple-element.60), channel_id=1, source_target_pairs={{0,32},{1,113},{16,48},{17,65},{32,0},{33,81},{48,16},{49,97},{64,... | collective-permute-start | bytes 1572872 | tf_op jit(solution)/shard_map/ppermute | solution.py:50
  146.2 23.9 %collective-permute-start.31 = (bf16[64,2048]{1,0:T(8,128)(2,1)S(1)}, bf16[64,2048]{1,0:T(8,128)(2,1)S(1)}, u32[]{:S(2)}, u32[]{:S(2)}) collective-permute-start(bf16[64,2048]{1,0:T(8,128)(2,1)S(1)} %get-tuple-element.57), channel_id=1, source_target_pairs={{0,240},{1,33},{16,192},{17,49},{32,208},{33,1},{48,224},{49,17},{... | collective-permute-start | bytes 786440 | tf_op jit(solution)/shard_map/ppermute | solution.py:50
  146.6 24.9 %collective-permute-start.36 = (bf16[64,2048]{1,0:T(8,128)(2,1)S(1)}, bf16[64,2048]{1,0:T(8,128)(2,1)S(1)}, u32[]{:S(2)}, u32[]{:S(2)}) collective-permute-start(bf16[64,2048]{1,0:T(8,128)(2,1)S(1)} %get-tuple-element.63), channel_id=1, source_target_pairs={{0,241},{1,32},{16,193},{17,48},{32,209},{33,0},{48,225},{49,16},{... | collective-permute-start | bytes 786440 | tf_op jit(solution)/shard_map/ppermute | solution.py:50
  170.0 14.9 %collective-permute-start.34 = (bf16[64,2048]{1,0:T(8,128)(2,1)S(1)}, bf16[64,2048]{1,0:T(8,128)(2,1)S(1)}, u32[]{:S(2)}, u32[]{:S(2)}) collective-permute-start(bf16[64,2048]{1,0:T(8,128)(2,1)S(1)} %get-tuple-element.61), channel_id=1, source_target_pairs={{0,208},{1,241},{16,224},{17,193},{32,240},{33,209},{48,192},{49,2... | collective-permute-start | bytes 786440 | tf_op jit(solution)/shard_map/ppermute | solution.py:50
  170.1 15.6 %collective-permute-start.35 = (bf16[64,2048]{1,0:T(8,128)(2,1)S(1)}, bf16[64,2048]{1,0:T(8,128)(2,1)S(1)}, u32[]{:S(2)}, u32[]{:S(2)}) collective-permute-start(bf16[64,2048]{1,0:T(8,128)(2,1)S(1)} %get-tuple-element.62), channel_id=1, source_target_pairs={{0,32},{1,209},{16,48},{17,225},{32,0},{33,241},{48,16},{49,193},{... | collective-permute-start | bytes 786440 | tf_op jit(solution)/shard_map/ppermute | solution.py:50
  171.5 18.9 %collective-permute-start.38 = (bf16[64,2048]{1,0:T(8,128)(2,1)S(1)}, bf16[64,2048]{1,0:T(8,128)(2,1)S(1)}, u32[]{:S(2)}, u32[]{:S(2)}) collective-permute-start(bf16[64,2048]{1,0:T(8,128)(2,1)S(1)} %get-tuple-element.65), channel_id=1, source_target_pairs={{0,209},{1,240},{16,225},{17,192},{32,241},{33,208},{48,193},{49,2... | collective-permute-start | bytes 786440 | tf_op jit(solution)/shard_map/ppermute | solution.py:50
  (29 other events, 361.5 us)

commit v5 on v3

--- a/solution.py
+++ b/solution.py
@@ -61,7 +61,16 @@
 
 
 def hosted(value):
-    return permute(value, CHIP, (4, 4, 2), lambda y, x, c: (y - 2 * c, x - 2 * c, c))
+    pairs = []
+    for y, x in np.ndindex(4, 4):
+        to = (y + 2) % 4 * 4 + (x + 2) % 4
+        pairs.append(((y * 4 + x) * 2 + 1, to * 2 + 1))
+    return lax.ppermute(value, CHIP, pairs)
+
+
+def with_next_plane(value):
+    pairs = [(z * 2 + 1, (z ^ 1) * 2 + 1) for z in range(8)]
+    return lax.ppermute(value, TP, pairs)
 
 
 def along_z(value, step):
@@ -145,7 +154,7 @@
     return pl.pallas_call(
         conv_kernel,
         grid=(4,),
-        out_shape=jax.ShapeDtypeStruct((16, HEAD, ROWS), jnp.bfloat16),
+        out_shape=pltpu.HBM((16, HEAD, ROWS), jnp.bfloat16),
         in_specs=[wide] * 3
         + [pl.BlockSpec((1, 4 * ROWS), lambda i: (0, i)), whole(halo), whole(small)],
         out_specs=pl.BlockSpec((4, HEAD, ROWS), lambda i: (i, 0, 0)),
@@ -269,7 +278,7 @@
         compiler_params=params(16, True),
         cost_estimate=cost(1.1e9, 8 << 20),
         name="mix",
-    )(where, by_row, *own, *swapped, in_hbm(resid), gain)
+    )(where, by_row, *map(in_hbm, own), *map(in_hbm, swapped), in_hbm(resid), gain)
 
 
 def pack_kernel(mine_ref, theirs_ref, mine_at_ref, theirs_at_ref, *refs):
@@ -309,27 +318,103 @@
     )(mine, theirs, mine_at, theirs_at)
 
 
+BLOCK = 512
+
+
+def down_blocks(down, out):
+    return [
+        (down.at[:, pl.ds(j * BLOCK, BLOCK)], out.at[pl.ds(j * FF, FF)])
+        for j in range(WIDTH // BLOCK)
+    ]
+
+
+def row_blocks(value, out):
+    rows = [pl.ds(j * BLOCK, BLOCK) for j in range(WIDTH // BLOCK)]
+    return [(value.at[r], out.at[r]) for r in rows]
+
+
+def copy_all(copies, sems):
+    for k, (source, target) in enumerate(copies):
+        pltpu.make_async_copy(source, target, sems.at[k]).start()
+    for k, (source, target) in enumerate(copies):
+        pltpu.make_async_copy(source, target, sems.at[k]).wait()
+
+
+def pick_kernel(where_ref, gate, down, out, sems):
+    odd = lax.rem(where_ref[2], 2)
+    for which, copies in enumerate((row_blocks(gate, out), down_blocks(down, out))):
+
+        @pl.when(odd == which)
+        def _(copies=copies):
+            copy_all(copies, sems)
+
+
+def pick(where, gate, down):
+    anywhere = pl.BlockSpec(memory_space=pl.ANY)
+    return pl.pallas_call(
+        pick_kernel,
+        out_shape=jax.ShapeDtypeStruct((WIDTH, FF), gate.dtype),
+        in_specs=[SMEM] + [anywhere] * 2,
+        out_specs=VMEM,
+        scratch_shapes=[pltpu.SemaphoreType.DMA((4,))],
+        compiler_params=params(4),
+        cost_estimate=cost(1e6, 4 << 20),
+        name="pick",
+    )(where, in_hbm(gate), in_hbm(down))
+
+
+def choose_kernel(where_ref, gate, up, down, ours, traded, got_up, g_out, u_out, d_out, sems):
+    odd, c = lax.rem(where_ref[2], 2), where_ref[3]
+    own = row_blocks(gate, g_out) + row_blocks(up, u_out) + down_blocks(down, d_out)
+    got = row_blocks(got_up, u_out)
+    even_plane = row_blocks(ours, g_out) + row_blocks(traded, d_out) + got
+    odd_plane = row_blocks(traded, g_out) + row_blocks(ours, d_out) + got
+    for test, copies in (
+        (c == 0, own),
+        ((c != 0) & (odd == 0), even_plane),
+        ((c != 0) & (odd != 0), odd_plane),
+    ):
+
+        @pl.when(test)
+        def _(copies=copies):
+            copy_all(copies, sems)
+
+
+def choose(where, *weights):
+    anywhere = pl.BlockSpec(memory_space=pl.ANY)
+    return pl.pallas_call(
+        choose_kernel,
+        out_shape=[jax.ShapeDtypeStruct((WIDTH, FF), weights[0].dtype)] * 3,
+        in_specs=[SMEM] + [anywhere] * 6,
+        out_specs=[VMEM] * 3,
+        scratch_shapes=[pltpu.SemaphoreType.DMA((12,))],
+        compiler_params=params(8),
+        cost_estimate=cost(1e6, 12 << 20),
+        name="choose",
+    )(where, *weights)
+
+
 def expert_kernel(n, *refs):
-    bufs, (wg, wu, wd) = refs[:n], refs[n : n + 3]
+    bufs, (gate, up, down) = refs[:n], refs[n : n + 3]
     outs, rows = refs[n + 3 : -1], refs[-1]
     row = 0
     for ref in bufs:
         rows[pl.ds(row, ref.shape[0]), :] = ref[...]
         row += ref.shape[0]
-    x = rows[...]
-    g = jnp.dot(x, wg[...], preferred_element_type=jnp.float32)
-    u = jnp.dot(x, wu[...], preferred_element_type=jnp.float32)
+    g = jnp.dot(rows[...], gate[...], preferred_element_type=jnp.float32)
+    u = jnp.dot(rows[...], up[...], preferred_element_type=jnp.float32)
     h = (g / (1.0 + jnp.exp(-g)) * u).astype(jnp.bfloat16)
-    for n0 in range(0, WIDTH, TILE):
-        at = slice(n0, n0 + TILE)
-        y = jnp.dot(h, wd[:, at], preferred_element_type=jnp.float32).astype(jnp.bfloat16)
+    for j in range(WIDTH // BLOCK):
+        at = slice(j * BLOCK, (j + 1) * BLOCK)
+        part = down[j * FF : (j + 1) * FF]
+        y = jnp.dot(h, part, preferred_element_type=jnp.float32).astype(jnp.bfloat16)
         row = 0
         for ref in outs:
             ref[:, at] = y[row : row + ref.shape[0]]
             row += ref.shape[0]
 
 
-def experts(bufs, wg, wu, wd, apart):
+def experts(bufs, gate, up, down, apart):
     rows = sum(b.shape[0] for b in bufs)
     size = CHUNK if apart else 2 * CHUNK
     n_out = rows // size
@@ -342,7 +427,7 @@
         compiler_params=params(24),
         cost_estimate=cost(6.0 * rows * WIDTH * FF, 8 << 20),
         name="experts",
-    )(*bufs, wg, wu, wd)
+    )(*bufs, gate, up, down)
 
 
 def tables(rows_ref, weights_ref, chunks, high, low):
@@ -460,9 +545,12 @@
 ):
     y, x, z, c = (lax.axis_index(a) for a in ("y", "x", "z", "c"))
 
-    wg = hosted(w_gate[0])
-    wu = hosted(w_up[0])
-    wd = hosted(w_down[0])
+    where = jnp.stack([y, x, z, c]).astype(jnp.int32)
+    own_weights = (w_gate[0], w_up[0], w_down[0])
+    picked = pick(where, w_gate[0], w_down[0])
+    ours = hosted(picked)
+    traded = with_next_plane(ours)
+    got_up = hosted(w_up[0])
 
     plus, minus = [out_proj], [out_proj]
     plus.append(along_z(out_proj, 1))
@@ -482,7 +570,6 @@
     own = [out_proj, plus[1], minus[1], plus[2], minus[2], plus[3], minus[3], plus[4]]
     swapped = [swap_cores(w) for w in own]
 
-    where = jnp.stack([y, x, z, c]).astype(jnp.int32)
     routes = jnp.concatenate([route_ids.astype(jnp.float32), route_weight], axis=1).T
     routes_other = swap_cores(routes)
     rows, weights, rows_other, weights_other = route(where, routes, routes_other)
@@ -492,11 +579,12 @@
     sends = pack(normed, normed_other, rows[: len(PAIRS)], rows_other)
     arrived = [displaced(s, k, 1) for k, s in enumerate(sends)]
 
+    hosted_weights = choose(where, *own_weights, ours, traded, got_up)
     back, cross = {}, {}
     for n, group in enumerate(GROUPS):
         apart = n > 0
         inputs = [arrived[k] for k in group]
-        results = experts(inputs, wg, wu, wd, apart)
+        results = experts(inputs, *hosted_weights, apart)
         for i, k in enumerate(group):
             if apart:
                 back[k] = displaced(results[2 * i], k, -1)

time: 212 us -> 197 us (0.929)
  the two profiles are of different devices: /device:TPU:1 before, /device:TPU:32 now
where the time goes in v5:
time: 197 us; the launch traced here: 194 us
  starting transfers between devices  89.4 us (45%)
  waiting for transfers between devices  68.8 us (35%)
  Pallas kernels  35.5 us (18%)
    ppermute x36, waiting for transfers between devices, permute(): return lax.ppermute(value, axes, pairs)  68.8 us
    ppermute x36, starting transfers between devices, permute(): return lax.ppermute(value, axes, pairs)  55.4 us
    all_to_all x1, starting transfers between devices, body(): lax.all_to_all(head_normed, TP, split_axis=0, concat_axis=0, tiled=True)  24.5 us
    pallas_call x3, Pallas kernels, experts(): pl.pallas_call(functools.partial(expert_kernel, len(bufs)), out_shape=[ja...  7.25 us
    pallas_call x1, Pallas kernels, mix(): pl.pallas_call(mix_kernel, grid=(WIDTH // TILE,), out_shape=[pltpu.HBM((R...  6.14 us
    pallas_call x1, Pallas kernels, finish(): pl.pallas_call(functools.partial(finish_kernel, chunks), grid=(WIDTH // T...  4.55 us
    pallas_call x1, Pallas kernels, gather(): pl.pallas_call(functools.partial(gather_kernel, chunks), grid=(WIDTH // T...  4.55 us
    pallas_call x1, Pallas kernels, conv(): pl.pallas_call(conv_kernel, grid=(4,), out_shape=pltpu.HBM((16, HEAD, ROW...  4.22 us
  transfers between devices with their start and end apart: 41, of which 12 were waited for; matrix products, arithmetic and copies ran while one was open for 0% of the time, Pallas kernels for 12%

profile of v5, /device:TPU:32, one launch (start us, length us, event | category | flops | bytes accessed | tf_op | source)
XLA Modules:
  0.0 194.1 jit_solution(12546109616214883489)
XLA Ops:
  0.1 3.5 %pick.1 = bf16[2048,512]{1,0:T(8,128)(2,1)} custom-call(s32[4]{0:T(128)S(1)} %pad_add_fusion.where_ref, bf16[2048,512]{1,0:T(8,128)(2,1)} %bitcast.13, bf16[512,2048]{1,0:T(8,128)(2,1)} %bitcast.15), custom_call_target="tpu_custom_call" | custom-call | flops 1000000 | bytes 4194304 | tf_op jit(solution)/shard_map/pick/pallas_call | solution.py:354
  8.5 3.4 %collective-permute-start = (f32[72,128]{1,0:T(8,128)S(1)}, f32[72,128]{1,0:T(8,128)S(1)}, u32[]{:S(2)}, u32[]{:S(2)}) collective-permute-start(f32[72,128]{1,0:T(8,128)S(1)} %tail.1), channel_id=1, source_target_pairs={{0,16},{16,32},{32,48},{48,64},{64,80},{80,96},{96,112},{112,128},... | collective-permute-start | bytes 110600 | tf_op jit(solution)/shard_map/ppermute | solution.py:561
  11.9 3.8 %collective-permute-start.8 = (bf16[64,2048]{1,0:T(8,128)(2,1)S(1)}, bf16[64,2048]{1,0:T(8,128)(2,1)}, u32[]{:S(2)}, u32[]{:S(2)}) collective-permute-start(bf16[64,2048]{1,0:T(8,128)(2,1)S(1)} %copy-done.5), channel_id=1, source_target_pairs={{0,1},{1,0},{2,3},{3,2},{4,5},{5,4},{6,7},{7,6},{8,9},{9,8},{10,11... | collective-permute-start | bytes 786440 | tf_op jit(solution)/shard_map/ppermute | solution.py:50
  16.2 3.6 %collective-permute-start.4 = (bf16[64,2048]{1,0:T(8,128)(2,1)S(1)}, bf16[64,2048]{1,0:T(8,128)(2,1)}, u32[]{:S(2)}, u32[]{:S(2)}) collective-permute-start(bf16[64,2048]{1,0:T(8,128)(2,1)S(1)} %collective-permute-done.2.refs_2_), channel_id=1, source_target_pairs={{0,14},{2,0},{4,2},{6,4},{8,6},{10,8},{12,10},{14,12},{1,15},{3,1}... | collective-permute-start | bytes 786440 | tf_op jit(solution)/shard_map/ppermute | solution.py:50
  19.9 4.2 %conv.1 = bf16[16,64,256]{2,1,0:T(8,128)(2,1)} custom-call(bf16[64,4096]{1,0:T(8,128)(2,1)} %a_ref.3, bf16[64,4096]{1,0:T(8,128)(2,1)} %b_ref.3, bf16[64,4096]{1,0:T(8,128)(2,1)} %o_ref.1, s32[1,4096]{1,0:T(1,128)S(1)} %bitcast.20, f32[72,128]{1,0:T(8,128)S(1)} %collective-permute-done.halo_ref, f32[8,128]{1,0:T(8,128)S(1)} %select_maximum_fusion.small_ref), custom_call_target="tpu_custom_call" | custom-call | flops 200000000 | bytes 2097152 | tf_op jit(solution)/shard_map/conv/pallas_call | solution.py:154
  24.1 24.5 %all-to-all-start = ((bf16[16,64,256]{2,1,0:T(8,128)(2,1)}), bf16[16,64,256]{2,1,0:T(8,128)(2,1)S(1)}, u32[]{:S(2)}, u32[]{:S(2)}) async-start(bf16[16,64,256]{2,1,0:T(8,128)(2,1)} %conv.1), calls=%async_computation | async-start | bytes 1048576 | tf_op jit(solution)/shard_map/all_to_all | solution.py:564
  50.6 4.4 %collective-permute-start.9 = (bf16[64,2048]{1,0:T(8,128)(2,1)S(1)}, bf16[64,2048]{1,0:T(8,128)(2,1)S(1)}, u32[]{:S(2)}, u32[]{:S(2)}) collective-permute-start(bf16[64,2048]{1,0:T(8,128)(2,1)S(1)} %collective-permute-done.1.refs_1_), channel_id=1, source_target_pairs={{0,1},{1,0},{2,3},{3,2},{4,5},{5,4},{6,7},{7,6},{8,9},{9,8},{10,11... | collective-permute-start | bytes 786440 | tf_op jit(solution)/shard_map/ppermute | solution.py:50
  57.1 10.0 %collective-permute-done.5.refs_5_ = bf16[64,2048]{1,0:T(8,128)(2,1)} collective-permute-done((bf16[64,2048]{1,0:T(8,128)(2,1)}, bf16[64,2048]{1,0:T(8,128)(2,1)}, u32[]{:S(2)}, u32[]{:S(2)}) %collective-permute-start.5) | collective-permute-done | bytes 262176 | tf_op jit(solution)/shard_map/ppermute | solution.py:50
  71.3 6.1 %collective-permute-done.7.refs_7_ = bf16[64,2048]{1,0:T(8,128)(2,1)} collective-permute-done((bf16[64,2048]{1,0:T(8,128)(2,1)}, bf16[64,2048]{1,0:T(8,128)(2,1)}, u32[]{:S(2)}, u32[]{:S(2)}) %collective-permute-start.7) | collective-permute-done | bytes 262176 | tf_op jit(solution)/shard_map/ppermute | solution.py:50
  79.3 6.1 %mix.1 = (f32[256,2048]{1,0:T(8,128)}, bf16[256,2048]{1,0:T(8,128)(2,1)S(1)}) custom-call(s32[4]{0:T(128)S(1)} %pad_add_fusion.where_ref, bf16[16,64,256]{2,1,0:T(8,128)(2,1)S(1)} %all-to-all-done.by_row_ref, bf16[64,2048]{1,0:T(8,128)(2,1)} %refs_0_.1, bf16[64,2048]{1,0:T(8,128)(2,1)} %copy-done.7, bf16[64,2048]{1,0:T(8,128)(2,1)} %copy-done.6, ...), custom_call_target="tpu_custom_call" | custom-call | flops 1100000000 | bytes 8388608 | tf_op jit(solution)/shard_map/mix/pallas_call | solution.py:258
  99.4 6.6 %collective-permute-done.18.refs_0_ = bf16[128,2048]{1,0:T(8,128)(2,1)S(1)} collective-permute-done((bf16[128,2048]{1,0:T(8,128)(2,1)S(1)}, bf16[128,2048]{1,0:T(8,128)(2,1)S(1)}, u32[]{:S(2)}, u32[]{:S(2)}) %collective-permute-start.18) | collective-permute-done | bytes 524320 | tf_op jit(solution)/shard_map/ppermute | solution.py:50
  106.0 3.7 %collective-permute-done.19.refs_1_ = bf16[128,2048]{1,0:T(8,128)(2,1)S(1)} collective-permute-done((bf16[128,2048]{1,0:T(8,128)(2,1)S(1)}, bf16[128,2048]{1,0:T(8,128)(2,1)S(1)}, u32[]{:S(2)}, u32[]{:S(2)}) %collective-permute-start.19) | collective-permute-done | bytes 524320 | tf_op jit(solution)/shard_map/ppermute | solution.py:50
  109.7 3.5 %experts.3 = (bf16[128,2048]{1,0:T(8,128)(2,1)S(1)}, bf16[128,2048]{1,0:T(8,128)(2,1)S(1)}, bf16[128,2048]{1,0:T(8,128)(2,1)S(1)}, bf16[128,2048]{1,0:T(8,128)(2,1)S(1)}) custom-call(bf16[128,2048]{1,0:T(8,128)(2,1)S(1)} %collective-permute-done.18.refs_0_, bf16[128,2048]{1,0:T(8,128)(2,1)S(1)} %collective-permute-done.19.refs_1_, ...), custom_call_target="tpu_custom_call" | custom-call | flops 3221225472 | bytes 8388608 | tf_op jit(solution)/shard_map/experts/pallas_call | solution.py:421
  113.2 3.2 %collective-permute-start.26 = (bf16[128,2048]{1,0:T(8,128)(2,1)S(1)}, bf16[128,2048]{1,0:T(8,128)(2,1)S(1)}, u32[]{:S(2)}, u32[]{:S(2)}) collective-permute-start(bf16[128,2048]{1,0:T(8,128)(2,1)S(1)} %get-tuple-element.50), channel_id=1, source_target_pairs={{0,192},{1,65},{16,208},{17,81},{32,224},{33,97},{48,240},{49,113}... | collective-permute-start | bytes 1572872 | tf_op jit(solution)/shard_map/ppermute | solution.py:50
  117.4 10.5 %collective-permute-done.25.refs_0_ = bf16[128,2048]{1,0:T(8,128)(2,1)S(1)} collective-permute-done((bf16[128,2048]{1,0:T(8,128)(2,1)S(1)}, bf16[128,2048]{1,0:T(8,128)(2,1)S(1)}, u32[]{:S(2)}, u32[]{:S(2)}) %collective-permute-start.25) | collective-permute-done | bytes 524320 | tf_op jit(solution)/shard_map/ppermute | solution.py:50
  129.9 6.2 %collective-permute-done.27.refs_2_ = bf16[128,2048]{1,0:T(8,128)(2,1)S(1)} collective-permute-done((bf16[128,2048]{1,0:T(8,128)(2,1)S(1)}, bf16[128,2048]{1,0:T(8,128)(2,1)S(1)}, u32[]{:S(2)}, u32[]{:S(2)}) %collective-permute-start.27) | collective-permute-done | bytes 524320 | tf_op jit(solution)/shard_map/ppermute | solution.py:50
  136.1 4.6 %gather.1 = (f32[256,2048]{1,0:T(8,128)}, bf16[256,2048]{1,0:T(8,128)(2,1)S(1)}) custom-call(f32[256,2048]{1,0:T(8,128)} %get-tuple-element.36.acc_ref, s32[16,256]{1,0:T(8,128)S(1)} %get-tuple-element.37.rows_ref, f32[16,256]{1,0:T(8,128)S(1)} %get-tuple-element.38.weights_ref, s32[8,256]{1,0:T(8,128)S(1)} %get-tuple-element.39.theirs_at_ref.rows2_ref, ...), custom_call_target="tpu_custom_call" | custom-call | flops 1073741824 | bytes 10485760 | tf_op jit(solution)/shard_map/gather/pallas_call | solution.py:474
  140.7 9.7 %collective-permute-done.30.refs_0_ = bf16[128,2048]{1,0:T(8,128)(2,1)S(1)} collective-permute-done((bf16[128,2048]{1,0:T(8,128)(2,1)S(1)}, bf16[128,2048]{1,0:T(8,128)(2,1)S(1)}, u32[]{:S(2)}, u32[]{:S(2)}) %collective-permute-start.30) | collective-permute-done | bytes 524320 | tf_op jit(solution)/shard_map/ppermute | solution.py:50
  152.5 8.2 %collective-permute-start.37 = (bf16[64,2048]{1,0:T(8,128)(2,1)S(1)}, bf16[64,2048]{1,0:T(8,128)(2,1)S(1)}, u32[]{:S(2)}, u32[]{:S(2)}) collective-permute-start(bf16[64,2048]{1,0:T(8,128)(2,1)S(1)} %get-tuple-element.64), channel_id=1, source_target_pairs={{0,1},{1,0},{16,17},{17,16},{32,33},{33,32},{48,49},{49,48},{64,65... | collective-permute-start | bytes 786440 | tf_op jit(solution)/shard_map/ppermute | solution.py:50
  165.7 3.6 %collective-permute-start.35 = (bf16[64,2048]{1,0:T(8,128)(2,1)S(1)}, bf16[64,2048]{1,0:T(8,128)(2,1)S(1)}, u32[]{:S(2)}, u32[]{:S(2)}) collective-permute-start(bf16[64,2048]{1,0:T(8,128)(2,1)S(1)} %get-tuple-element.62), channel_id=1, source_target_pairs={{0,32},{1,209},{16,48},{17,225},{32,0},{33,241},{48,16},{49,193},{... | collective-permute-start | bytes 786440 | tf_op jit(solution)/shard_map/ppermute | solution.py:50
  169.3 9.6 %collective-permute-start.38 = (bf16[64,2048]{1,0:T(8,128)(2,1)S(1)}, bf16[64,2048]{1,0:T(8,128)(2,1)S(1)}, u32[]{:S(2)}, u32[]{:S(2)}) collective-permute-start(bf16[64,2048]{1,0:T(8,128)(2,1)S(1)} %get-tuple-element.65), channel_id=1, source_target_pairs={{0,209},{1,240},{16,225},{17,192},{32,241},{33,208},{48,193},{49,2... | collective-permute-start | bytes 786440 | tf_op jit(solution)/shard_map/ppermute | solution.py:50
  178.9 5.8 %collective-permute-done.38.refs_6_ = bf16[64,2048]{1,0:T(8,128)(2,1)S(1)} collective-permute-done((bf16[64,2048]{1,0:T(8,128)(2,1)S(1)}, bf16[64,2048]{1,0:T(8,128)(2,1)S(1)}, u32[]{:S(2)}, u32[]{:S(2)}) %collective-permute-start.38) | collective-permute-done | bytes 262176 | tf_op jit(solution)/shard_map/ppermute | solution.py:50
  184.7 4.9 %collective-permute-done.39.refs_7_ = bf16[64,2048]{1,0:T(8,128)(2,1)S(1)} collective-permute-done((bf16[64,2048]{1,0:T(8,128)(2,1)S(1)}, bf16[64,2048]{1,0:T(8,128)(2,1)S(1)}, u32[]{:S(2)}, u32[]{:S(2)}) %collective-permute-start.39) | collective-permute-done | bytes 262176 | tf_op jit(solution)/shard_map/ppermute | solution.py:50
  189.6 4.6 %finish.1 = bf16[256,2048]{1,0:T(8,128)(2,1)} custom-call(f32[256,2048]{1,0:T(8,128)} %get-tuple-element.53.acc_ref, bf16[256,2048]{1,0:T(8,128)(2,1)S(1)} %collective-permute-done.29.more_ref, s32[16,256]{1,0:T(8,128)S(1)} %get-tuple-element.37.rows_ref, f32[16,256]{1,0:T(8,128)S(1)} %get-tuple-element.38.weights_ref, ...), custom_call_target="tpu_custom_call" | custom-call | flops 1073741824 | bytes 6291456 | tf_op jit(solution)/shard_map/finish/pallas_call | solution.py:515
  (105 shorter events, 39.9 us)
Async XLA Ops:
  3.6 64.9 %collective-permute-start.22 = (bf16[2048,512]{1,0:T(8,128)(2,1)}, bf16[2048,512]{1,0:T(8,128)(2,1)}, u32[]{:S(2)}, u32[]{:S(2)}) collective-permute-start(bf16[2048,512]{1,0:T(8,128)(2,1)} %pick.1), channel_id=1, source_target_pairs={{1,161},{17,177},{33,129},{49,145},{65,225},{81,241},{97,193},{113... | collective-permute-start | bytes 6291464 | tf_op jit(solution)/shard_map/ppermute | solution.py:68
  11.9 36.6 %collective-permute-start.8 = (bf16[64,2048]{1,0:T(8,128)(2,1)S(1)}, bf16[64,2048]{1,0:T(8,128)(2,1)}, u32[]{:S(2)}, u32[]{:S(2)}) collective-permute-start(bf16[64,2048]{1,0:T(8,128)(2,1)S(1)} %copy-done.5), channel_id=1, source_target_pairs={{0,1},{1,0},{2,3},{3,2},{4,5},{5,4},{6,7},{7,6},{8,9},{9,8},{10,11... | collective-permute-start | bytes 786440 | tf_op jit(solution)/shard_map/ppermute | solution.py:50
  15.7 34.9 %collective-permute-start.10 = (bf16[64,2048]{1,0:T(8,128)(2,1)S(1)}, bf16[64,2048]{1,0:T(8,128)(2,1)}, u32[]{:S(2)}, u32[]{:S(2)}) collective-permute-start(bf16[64,2048]{1,0:T(8,128)(2,1)S(1)} %collective-permute-done.2.refs_2_), channel_id=1, source_target_pairs={{0,1},{1,0},{2,3},{3,2},{4,5},{5,4},{6,7},{7,6},{8,9},{9,8},{10,11... | collective-permute-start | bytes 786440 | tf_op jit(solution)/shard_map/ppermute | solution.py:50
  16.2 38.8 %collective-permute-start.4 = (bf16[64,2048]{1,0:T(8,128)(2,1)S(1)}, bf16[64,2048]{1,0:T(8,128)(2,1)}, u32[]{:S(2)}, u32[]{:S(2)}) collective-permute-start(bf16[64,2048]{1,0:T(8,128)(2,1)S(1)} %collective-permute-done.2.refs_2_), channel_id=1, source_target_pairs={{0,14},{2,0},{4,2},{6,4},{8,6},{10,8},{12,10},{14,12},{1,15},{3,1}... | collective-permute-start | bytes 786440 | tf_op jit(solution)/shard_map/ppermute | solution.py:50
  19.8 35.3 %collective-permute-start.3 = (bf16[64,2048]{1,0:T(8,128)(2,1)S(1)}, bf16[64,2048]{1,0:T(8,128)(2,1)}, u32[]{:S(2)}, u32[]{:S(2)}) collective-permute-start(bf16[64,2048]{1,0:T(8,128)(2,1)S(1)} %collective-permute-done.1.refs_1_), channel_id=1, source_target_pairs={{0,2},{2,4},{4,6},{6,8},{8,10},{10,12},{12,14},{14,0},{1,3},{3,5},... | collective-permute-start | bytes 786440 | tf_op jit(solution)/shard_map/ppermute | solution.py:50
  24.1 53.3 %all-to-all-start = ((bf16[16,64,256]{2,1,0:T(8,128)(2,1)}), bf16[16,64,256]{2,1,0:T(8,128)(2,1)S(1)}, u32[]{:S(2)}, u32[]{:S(2)}) async-start(bf16[16,64,256]{2,1,0:T(8,128)(2,1)} %conv.1), calls=%async_computation | async-start | bytes 1048576 | tf_op jit(solution)/shard_map/all_to_all | solution.py:564
  48.6 48.5 %collective-permute-start.24 = (bf16[2048,512]{1,0:T(8,128)(2,1)S(1)}, bf16[2048,512]{1,0:T(8,128)(2,1)}, u32[]{:S(2)}, u32[]{:S(2)}) collective-permute-start(bf16[2048,512]{1,0:T(8,128)(2,1)S(1)} %bitcast.17), channel_id=1, source_target_pairs={{1,161},{17,177},{33,129},{49,145},{65,225},{81,241},{97,193},{113... | collective-permute-start | bytes 6291464 | tf_op jit(solution)/shard_map/ppermute | solution.py:68
  57.1 14.1 %collective-permute-start.11 = (bf16[64,2048]{1,0:T(8,128)(2,1)}, bf16[64,2048]{1,0:T(8,128)(2,1)S(1)}, u32[]{:S(2)}, u32[]{:S(2)}) collective-permute-start(bf16[64,2048]{1,0:T(8,128)(2,1)} %collective-permute-done.3.refs_3_), channel_id=1, source_target_pairs={{0,1},{1,0},{2,3},{3,2},{4,5},{5,4},{6,7},{7,6},{8,9},{9,8},{10,11... | collective-permute-start | bytes 786440 | tf_op jit(solution)/shard_map/ppermute | solution.py:50
  68.5 29.6 %collective-permute-start.23 = (bf16[2048,512]{1,0:T(8,128)(2,1)}, bf16[2048,512]{1,0:T(8,128)(2,1)}, u32[]{:S(2)}, u32[]{:S(2)}) collective-permute-start(bf16[2048,512]{1,0:T(8,128)(2,1)} %collective-permute-done.22.ours), channel_id=1, source_target_pairs={{1,3},{3,1},{5,7},{7,5},{9,11},{11,9},{13,15},{15,13},{17,19},{19,... | collective-permute-start | bytes 6291464 | tf_op jit(solution)/shard_map/ppermute | solution.py:73
  91.5 14.5 %collective-permute-start.18 = (bf16[128,2048]{1,0:T(8,128)(2,1)S(1)}, bf16[128,2048]{1,0:T(8,128)(2,1)S(1)}, u32[]{:S(2)}, u32[]{:S(2)}) collective-permute-start(bf16[128,2048]{1,0:T(8,128)(2,1)S(1)} %get-tuple-element.42), channel_id=1, source_target_pairs={{0,16},{1,49},{16,32},{17,1},{32,48},{33,17},{48,0},{49,33},{64,80... | collective-permute-start | bytes 1572872 | tf_op jit(solution)/shard_map/ppermute | solution.py:50
  93.8 15.9 %collective-permute-start.19 = (bf16[128,2048]{1,0:T(8,128)(2,1)S(1)}, bf16[128,2048]{1,0:T(8,128)(2,1)S(1)}, u32[]{:S(2)}, u32[]{:S(2)}) collective-permute-start(bf16[128,2048]{1,0:T(8,128)(2,1)S(1)} %get-tuple-element.43), channel_id=1, source_target_pairs={{0,64},{1,193},{16,80},{17,209},{32,96},{33,225},{48,112},{49,241}... | collective-permute-start | bytes 1572872 | tf_op jit(solution)/shard_map/ppermute | solution.py:50
  94.5 15.2 %collective-permute-start.20 = (bf16[128,2048]{1,0:T(8,128)(2,1)S(1)}, bf16[128,2048]{1,0:T(8,128)(2,1)S(1)}, u32[]{:S(2)}, u32[]{:S(2)}) collective-permute-start(bf16[128,2048]{1,0:T(8,128)(2,1)S(1)} %get-tuple-element.44), channel_id=1, source_target_pairs={{0,48},{1,17},{16,0},{17,33},{32,16},{33,49},{48,32},{49,1},{64,11... | collective-permute-start | bytes 1572872 | tf_op jit(solution)/shard_map/ppermute | solution.py:50
  113.1 14.7 %collective-permute-start.25 = (bf16[128,2048]{1,0:T(8,128)(2,1)S(1)}, bf16[128,2048]{1,0:T(8,128)(2,1)S(1)}, u32[]{:S(2)}, u32[]{:S(2)}) collective-permute-start(bf16[128,2048]{1,0:T(8,128)(2,1)S(1)} %get-tuple-element.49), channel_id=1, source_target_pairs={{0,48},{1,17},{16,0},{17,33},{32,16},{33,49},{48,32},{49,1},{64,11... | collective-permute-start | bytes 1572872 | tf_op jit(solution)/shard_map/ppermute | solution.py:50
  113.2 16.6 %collective-permute-start.26 = (bf16[128,2048]{1,0:T(8,128)(2,1)S(1)}, bf16[128,2048]{1,0:T(8,128)(2,1)S(1)}, u32[]{:S(2)}, u32[]{:S(2)}) collective-permute-start(bf16[128,2048]{1,0:T(8,128)(2,1)S(1)} %get-tuple-element.50), channel_id=1, source_target_pairs={{0,192},{1,65},{16,208},{17,81},{32,224},{33,97},{48,240},{49,113}... | collective-permute-start | bytes 1572872 | tf_op jit(solution)/shard_map/ppermute | solution.py:50
  116.5 19.6 %collective-permute-start.27 = (bf16[128,2048]{1,0:T(8,128)(2,1)S(1)}, bf16[128,2048]{1,0:T(8,128)(2,1)S(1)}, u32[]{:S(2)}, u32[]{:S(2)}) collective-permute-start(bf16[128,2048]{1,0:T(8,128)(2,1)S(1)} %get-tuple-element.51), channel_id=1, source_target_pairs={{0,16},{1,49},{16,32},{17,1},{32,48},{33,17},{48,0},{49,33},{64,80... | collective-permute-start | bytes 1572872 | tf_op jit(solution)/shard_map/ppermute | solution.py:50
  116.5 19.6 %collective-permute-start.28 = (bf16[128,2048]{1,0:T(8,128)(2,1)S(1)}, bf16[128,2048]{1,0:T(8,128)(2,1)S(1)}, u32[]{:S(2)}, u32[]{:S(2)}) collective-permute-start(bf16[128,2048]{1,0:T(8,128)(2,1)S(1)} %get-tuple-element.52), channel_id=1, source_target_pairs={{0,64},{1,193},{16,80},{17,209},{32,96},{33,225},{48,112},{49,241}... | collective-permute-start | bytes 1572872 | tf_op jit(solution)/shard_map/ppermute | solution.py:50
  117.3 33.1 %collective-permute-start.30 = (bf16[128,2048]{1,0:T(8,128)(2,1)S(1)}, bf16[128,2048]{1,0:T(8,128)(2,1)S(1)}, u32[]{:S(2)}, u32[]{:S(2)}) collective-permute-start(bf16[128,2048]{1,0:T(8,128)(2,1)S(1)} %get-tuple-element.55), channel_id=1, source_target_pairs={{0,80},{1,33},{16,96},{17,49},{32,112},{33,1},{48,64},{49,17},{64,... | collective-permute-start | bytes 1572872 | tf_op jit(solution)/shard_map/ppermute | solution.py:50
  127.9 24.6 %collective-permute-start.32 = (bf16[128,2048]{1,0:T(8,128)(2,1)S(1)}, bf16[128,2048]{1,0:T(8,128)(2,1)S(1)}, u32[]{:S(2)}, u32[]{:S(2)}) collective-permute-start(bf16[128,2048]{1,0:T(8,128)(2,1)S(1)} %get-tuple-element.59), channel_id=1, source_target_pairs={{0,112},{1,81},{16,64},{17,97},{32,80},{33,113},{48,96},{49,65},{6... | collective-permute-start | bytes 1572872 | tf_op jit(solution)/shard_map/ppermute | solution.py:50
  140.6 48.9 %collective-permute-start.29 = (bf16[256,2048]{1,0:T(8,128)(2,1)S(1)}, bf16[256,2048]{1,0:T(8,128)(2,1)S(1)}, u32[]{:S(2)}, u32[]{:S(2)}) collective-permute-start(bf16[256,2048]{1,0:T(8,128)(2,1)S(1)} %get-tuple-element.54), channel_id=1, source_target_pairs={{0,1},{1,0},{2,3},{3,2},{4,5},{5,4},{6,7},{7,6},{8,9},{9,8},{10,11... | collective-permute-start | bytes 3145736 | tf_op jit(solution)/shard_map/ppermute | solution.py:50
  140.7 21.5 %collective-permute-start.33 = (bf16[128,2048]{1,0:T(8,128)(2,1)S(1)}, bf16[128,2048]{1,0:T(8,128)(2,1)S(1)}, u32[]{:S(2)}, u32[]{:S(2)}) collective-permute-start(bf16[128,2048]{1,0:T(8,128)(2,1)S(1)} %get-tuple-element.60), channel_id=1, source_target_pairs={{0,32},{1,113},{16,48},{17,65},{32,0},{33,81},{48,16},{49,97},{64,... | collective-permute-start | bytes 1572872 | tf_op jit(solution)/shard_map/ppermute | solution.py:50
  152.4 16.9 %collective-permute-start.36 = (bf16[64,2048]{1,0:T(8,128)(2,1)S(1)}, bf16[64,2048]{1,0:T(8,128)(2,1)S(1)}, u32[]{:S(2)}, u32[]{:S(2)}) collective-permute-start(bf16[64,2048]{1,0:T(8,128)(2,1)S(1)} %get-tuple-element.63), channel_id=1, source_target_pairs={{0,241},{1,32},{16,193},{17,48},{32,209},{33,0},{48,225},{49,16},{... | collective-permute-start | bytes 786440 | tf_op jit(solution)/shard_map/ppermute | solution.py:50
  152.5 26.4 %collective-permute-start.37 = (bf16[64,2048]{1,0:T(8,128)(2,1)S(1)}, bf16[64,2048]{1,0:T(8,128)(2,1)S(1)}, u32[]{:S(2)}, u32[]{:S(2)}) collective-permute-start(bf16[64,2048]{1,0:T(8,128)(2,1)S(1)} %get-tuple-element.64), channel_id=1, source_target_pairs={{0,1},{1,0},{16,17},{17,16},{32,33},{33,32},{48,49},{49,48},{64,65... | collective-permute-start | bytes 786440 | tf_op jit(solution)/shard_map/ppermute | solution.py:50
  164.0 14.8 %collective-permute-start.34 = (bf16[64,2048]{1,0:T(8,128)(2,1)S(1)}, bf16[64,2048]{1,0:T(8,128)(2,1)S(1)}, u32[]{:S(2)}, u32[]{:S(2)}) collective-permute-start(bf16[64,2048]{1,0:T(8,128)(2,1)S(1)} %get-tuple-element.61), channel_id=1, source_target_pairs={{0,208},{1,241},{16,224},{17,193},{32,240},{33,209},{48,192},{49,2... | collective-permute-start | bytes 786440 | tf_op jit(solution)/shard_map/ppermute | solution.py:50
  169.3 15.4 %collective-permute-start.38 = (bf16[64,2048]{1,0:T(8,128)(2,1)S(1)}, bf16[64,2048]{1,0:T(8,128)(2,1)S(1)}, u32[]{:S(2)}, u32[]{:S(2)}) collective-permute-start(bf16[64,2048]{1,0:T(8,128)(2,1)S(1)} %get-tuple-element.65), channel_id=1, source_target_pairs={{0,209},{1,240},{16,225},{17,192},{32,241},{33,208},{48,193},{49,2... | collective-permute-start | bytes 786440 | tf_op jit(solution)/shard_map/ppermute | solution.py:50
  (32 other events, 527.6 us)
